TPU v7x, 256 devices: a whole 4x4x8 slice. The times are simulated.
256 devices in a mesh: ep: 64 (over z, y, core), tp: 4 (over x).
Axes of the slice: x: 4, y: 4, z: 8, core: 2. Of those that a mesh axis runs over, the one named last changes fastest.
Arguments:
- att_queries: bfloat16 [65536, 1024], P(('ep', 'tp')), may hold values from -8 to 8
- att_keys: bfloat16 [65536, 256], P(('ep', 'tp')), may hold values from -6 to 6
- att_values: bfloat16 [65536, 256], P(('ep', 'tp')), may hold values from -6 to 6
- sink_logits: float32 [16], replicated, may hold values from 3 to 6.5
- out_weight: bfloat16 [1024, 2048], replicated, may hold values from -0.1875 to 0.1875
- att_gain: float32 [2048], replicated, may hold values from 0.1 to 1.9
- moe_in: bfloat16 [32768, 2048], P(('ep', 'tp')), may hold values from -6 to 6
- pre_gain: float32 [2048], replicated, may hold values from 0.1 to 1.9
- expert_ids: int32 [32768, 2], P(('ep', 'tp')), may hold values from 0 to 127, all different within a row; in each aligned block of 128 rows (0 to 127, 128 to 255, ...) at most 4 rows name the same one
- routed_expert_weight: float32 [32768, 2], P(('ep', 'tp')), may hold values from 0.2 to 1.5
- w_gate: bfloat16 [128, 2048, 768], P('ep', None, 'tp'), may hold values from -0.125 to 0.125
- w_up: bfloat16 [128, 2048, 768], P('ep', None, 'tp'), may hold values from -0.125 to 0.125
- w_down: bfloat16 [128, 768, 2048], P('ep', 'tp'), may hold values from -0.21875 to 0.21875
- common_expert_gate_weight: bfloat16 [2048, 512], P(None, 'tp'), may hold values from -0.125 to 0.125
- common_expert_up_weight: bfloat16 [2048, 512], P(None, 'tp'), may hold values from -0.125 to 0.125
- common_expert_down_weight: bfloat16 [512, 2048], P('tp'), may hold values from -0.25 to 0.25
- moe_gain: float32 [2048], replicated, may hold values from 0.1 to 1.9
Outputs:
- mixer_out: bfloat16 [65536, 2048], P(('ep', 'tp'))
- experts_out: bfloat16 [32768, 2048], P(('ep', 'tp'))
Inputs may be any that keep to these rules, and one draw needn't show every extreme that they name: `expert_ids`: each row names 2 different experts; within the rows of one device no expert is named more than 4 times, and in every draw some expert is named exactly 4 times by the rows of some device.
All inputs are finite; a program needn't handle non-finite values.
Results may differ from a plain program's by a relative error of at most 0.012.
Values may be sent and summed in bfloat16 or wider, within the bound.
No kernel may reach another device: no remote copies, remote signals or barrier semaphores. Data moves between devices by JAX's collectives and lax.ppermute only.
A program may use at most 128 MiB of HBM per device.

v0:
```python
import math

import jax
import jax.numpy as jnp
from jax import lax
from jax.sharding import Mesh
from jax.sharding import PartitionSpec as P

HEADS = 16
KV_HEADS = 4
HEAD_DIM = 64
WINDOW = 128
EP_TP = ("ep_0", "ep_1", "ep_2", "tp")
EP = ("ep_0", "ep_1", "ep_2")


EPS = 1e-06
NEGATIVE = -1e30


def from_behind(block, axis, distance):
    devices = range(lax.axis_size(axis))
    route = [(i - distance, i) for i in devices if i - distance in devices]
    return lax.ppermute(block, axis, route)


def in_blocks(x, dim, count):
    dims = x.shape
    blocks = x.reshape(*dims[:dim], count, dims[dim] // count, *dims[dim + 1 :])
    return jnp.moveaxis(blocks, dim, 0)


def laid_out(blocks, dim):
    blocks = jnp.moveaxis(blocks, 0, dim)
    dims = blocks.shape
    return blocks.reshape(*dims[:dim], dims[dim] * dims[dim + 1], *dims[dim + 2 :])


def turned_blocks(blocks, axes, order):
    inside = blocks.shape[1:]
    out = blocks.reshape(*(lax.axis_size(a) for a in axes), *inside)
    for k in order:
        out = lax.all_to_all(out, axes[k], k, k, tiled=True)
    return out.reshape(-1, *inside)


def exchange_by_chip(x, groups, order, split_dim, concat_dim):
    count = lax.axis_size(groups[0]) * lax.axis_size(groups[1])
    blocks = in_blocks(x, split_dim, count)
    return laid_out(turned_blocks(blocks, groups, order), concat_dim)


def one_gather(arrays, axis, dims):
    ravelled = jnp.concatenate([a.reshape(-1) for a in arrays])
    lines, at, done = (lax.all_gather(ravelled, axis), 0, [])
    for a, dim in zip(arrays, dims):
        blocks = lines[:, at : at + a.size].reshape(-1, *a.shape)
        done.append(laid_out(blocks, dim))
        at += a.size
    return tuple(done)


def rms_scale(inputs, gain_vec):
    mean_sq = jnp.mean(inputs * inputs, axis=-1, keepdims=True)
    return inputs * lax.rsqrt(mean_sq + EPS) * gain_vec


def slot_table(route_ids, slot_cap):
    flat_ids = route_ids.reshape(-1)
    assigned = flat_ids.shape[0]
    earlier = jnp.arange(assigned)[None, :] < jnp.arange(assigned)[:, None]
    position = jnp.sum((flat_ids[:, None] == flat_ids[None, :]) & earlier, axis=1)
    return (flat_ids * slot_cap + position).reshape(route_ids.shape)


def pack_rows(token_rows, slot_ids, slot_total):
    numbers = jnp.arange(slot_total, dtype=jnp.int32)
    chosen = jnp.any(slot_ids[None, :, :] == numbers[:, None, None], axis=2).astype(jnp.bfloat16)
    return jnp.dot(chosen, token_rows, preferred_element_type=jnp.float32).astype(jnp.bfloat16)


def body(
    att_queries,
    att_keys,
    att_values,
    sink_logits,
    out_weight,
    att_gain,
    moe_in,
    pre_gain,
    expert_ids,
    routed_expert_weight,
    w_gate,
    w_up,
    w_down,
    common_expert_gate_weight,
    common_expert_up_weight,
    common_expert_down_weight,
    moe_gain,
):
    tok_rows = att_queries.shape[0]
    group_size = HEADS // KV_HEADS
    blocks = tok_rows // WINDOW
    kv_rows = jnp.stack([att_keys, att_values])
    rim_rows = from_behind(kv_rows[:, tok_rows - WINDOW :], EP_TP, 1)
    kv_all = jnp.concatenate([rim_rows, kv_rows], axis=1).reshape(
        2, blocks + 1, WINDOW, KV_HEADS, HEAD_DIM
    )
    kv_band = jnp.concatenate([kv_all[:, :-1], kv_all[:, 1:]], axis=2)
    query_blocks = att_queries.reshape(blocks, WINDOW, KV_HEADS, group_size, HEAD_DIM)
    scores = jnp.einsum(
        "nqgjd,nkgd->ngjqk", query_blocks, kv_band[0], preferred_element_type=jnp.float32
    ) * (1.0 / math.sqrt(HEAD_DIM))
    distance = jnp.arange(WINDOW)[:, None] + WINDOW - jnp.arange(2 * WINDOW)[None, :]
    inside = (distance >= 0) & (distance < WINDOW)
    first_pos = lax.axis_index(EP_TP) * tok_rows
    key_pos = (
        first_pos + jnp.arange(blocks)[:, None] * WINDOW - WINDOW + jnp.arange(2 * WINDOW)[None, :]
    )
    is_valid = inside[None] & (key_pos >= 0)[:, None, :]
    scores = jnp.where(is_valid[:, None, None], scores, NEGATIVE)
    sink_grid = sink_logits.reshape(KV_HEADS, group_size)[None, :, :, None, None]
    row_top = jnp.maximum(jnp.max(scores, axis=-1, keepdims=True), sink_grid)
    exp_scores = jnp.exp(scores - row_top)
    denominator = jnp.sum(exp_scores, axis=-1, keepdims=True) + jnp.exp(sink_grid - row_top)
    probs = (exp_scores / denominator).astype(jnp.bfloat16)
    head_mix = jnp.einsum(
        "ngjqk,nkgd->nqgjd", probs, kv_band[1], preferred_element_type=jnp.float32
    )
    head_mix = head_mix.astype(jnp.bfloat16).reshape(tok_rows, HEADS * HEAD_DIM)
    projected = jnp.dot(head_mix, out_weight, preferred_element_type=jnp.float32)
    mixer_out = rms_scale(projected, att_gain).astype(jnp.bfloat16)
    tokens = moe_in.shape[0]
    top_count = expert_ids.shape[1]
    local_experts = w_gate.shape[0]
    ep_size = lax.axis_size(EP)
    tp_size = lax.axis_size("tp")
    experts = local_experts * ep_size
    slot_cap = 2 * tokens * top_count // experts
    slot_total = experts * slot_cap
    normed = rms_scale(moe_in.astype(jnp.float32), pre_gain).astype(jnp.bfloat16)
    own_slots = slot_table(expert_ids, slot_cap)
    packed = pack_rows(normed, own_slots, slot_total)[None]
    arrived = exchange_by_chip(packed, (("ep_0", "ep_1"), "ep_2"), (0, 1), 1, 1)
    arrived_all, tokens_all = one_gather((arrived[0], normed), "tp", (0, 0))
    arrived = arrived_all.reshape(tp_size, slot_total, normed.shape[1])
    token_block = tokens_all.reshape(tp_size, tokens, normed.shape[1])
    routed = arrived
    routed = routed.reshape(
        1 * lax.axis_size("tp"), ep_size, local_experts, slot_cap, normed.shape[1]
    )
    gate_act = jnp.einsum("tsjcd,jdf->tsjcf", routed, w_gate, preferred_element_type=jnp.float32)
    up_act = jnp.einsum("tsjcd,jdf->tsjcf", routed, w_up, preferred_element_type=jnp.float32)
    hidden = (jax.nn.silu(gate_act) * up_act).astype(jnp.bfloat16)
    routed_part = jnp.einsum("tsjcf,jfd->tsjcd", hidden, w_down, preferred_element_type=jnp.float32)
    routed_part = routed_part.reshape(1 * lax.axis_size("tp"), slot_total, normed.shape[1])
    common_gate_activation = jnp.einsum(
        "spz,zv->spv", token_block, common_expert_gate_weight, preferred_element_type=jnp.float32
    )
    shared_up_act = jnp.einsum(
        "spz,zv->spv", token_block, common_expert_up_weight, preferred_element_type=jnp.float32
    )
    common_expert_hidden = (jax.nn.silu(common_gate_activation) * shared_up_act).astype(
        jnp.bfloat16
    )
    shared_part = jnp.einsum(
        "nsq,ql->nsl",
        common_expert_hidden,
        common_expert_down_weight,
        preferred_element_type=jnp.float32,
    )
    summed = lax.psum_scatter(
        jnp.concatenate([routed_part, shared_part], axis=1).astype(jnp.bfloat16),
        "tp",
        scatter_dimension=0,
        tiled=True,
    ).astype(jnp.float32)
    routed_out = summed[0, :slot_total].astype(jnp.bfloat16)
    shared_sum = summed[0, slot_total:]
    returned = lax.all_to_all(routed_out, EP, split_axis=0, concat_axis=0, tiled=True)
    picked = returned[own_slots.reshape(-1)].reshape(tokens, top_count, normed.shape[1])
    combined = (
        jnp.sum(routed_expert_weight[:, :, None] * picked.astype(jnp.float32), axis=1) + shared_sum
    )
    experts_out = rms_scale(combined, moe_gain).astype(jnp.bfloat16)
    return (mixer_out, experts_out)


def solution(mesh):
    split = Mesh(mesh.devices.reshape(8, 4, 2, mesh.shape["tp"]), ("ep_0", "ep_1", "ep_2", "tp"))
    placed = (
        P(EP_TP, None),
        P(EP_TP, None),
        P(EP_TP, None),
        P(),
        P(),
        P(),
        P(EP_TP, None),
        P(),
        P(EP_TP, None),
        P(EP_TP, None),
        P(EP, None, "tp"),
        P(EP, None, "tp"),
        P(EP, "tp", None),
        P(None, "tp"),
        P(None, "tp"),
        P("tp", None),
        P(),
    )
    return jax.shard_map(
        body,
        mesh=split,
        in_specs=placed,
        out_specs=(P(EP_TP, None), P(EP_TP, None)),
        check_vma=False,
    )
```

profile of v0, /device:TPU:8, one launch (start us, length us, event | category | flops | bytes accessed | tf_op | source)
XLA Modules:
  0.0 497.6 jit_solution(8483960690266620586)
XLA Ops:
  7.2 1.3 fusion.35
  10.0 3.1 convolution_convert_fusion.1
  13.1 11.9 %all-to-all-start = ((bf16[32,2,1,8,2048]{4,3,1,2,0:T(8,128)(2,1)}), bf16[32,2,1,8,2048]{4,3,1,2,0:T(8,128)(2,1)}, u32[]{:S(2)}, u32[]{:S(2)}) async-start(bf16[32,2,1,8,2048]{4,3,1,2,0:T(8,128)(2,1)} %bitcast.127), calls=%async_computation | async-start | bytes 4194304 | tf_op jit(solution)/shard_map/all_to_all | solution.py:43
  25.4 48.9 %all-to-all-done = bf16[32,2,1,8,2048]{4,3,1,2,0:T(8,128)(2,1)} async-done(((bf16[32,2,1,8,2048]{4,3,1,2,0:T(8,128)(2,1)}), bf16[32,2,1,8,2048]{4,3,1,2,0:T(8,128)(2,1)}, u32[]{:S(2)}, u32[]{:S(2)}) %all-to-all-start) | async-done | bytes 2097184 | tf_op jit(solution)/shard_map/all_to_all | solution.py:43
  74.3 1.7 copy.97
  76.0 5.4 %all_to_all.19 = bf16[32,2,1,8,2048]{4,3,0,2,1:T(8,128)(2,1)S(1)} all-to-all(bf16[32,2,1,8,2048]{4,3,0,2,1:T(8,128)(2,1)S(1)} %copy.97), channel_id=1, replica_groups=mesh['ep_0'=8,'ep_1'=4,'ep_2'=2,'tp'=4] {'ep_2'}, dimensions={1} | all-to-all | bytes 4194304 | tf_op jit(solution)/shard_map/all_to_all | solution.py:43
  82.3 7.6 %pad_maximum_fusion.1 = bf16[1310720]{0:T(1024)(128)(2,1)} fusion(bf16[262144]{0:T(1024)(128)(2,1)S(1)} %bitcast.130, bf16[1048576]{0:T(1024)(128)(2,1)S(1)} %bitcast.128), kind=kLoop, calls=%fused_computation.14 | loop fusion | flops 5242880 | bytes 5242880 | tf_op jit(solution)/shard_map/concatenate | solution.py:54
  90.0 101.5 %all-gather.3.cloned.1.call-done = bf16[5242880]{0:T(1024)(128)(2,1)} async-done(((bf16[1310720]{0:T(1024)(128)(2,1)}), bf16[5242880]{0:T(1024)(128)(2,1)}) %all-gather.3.cloned.1.call-update) | async-done | bytes 10485776 | tf_op jit(solution)/shard_map/all_gather | solution.py:55
  191.5 13.5 %reshape.179 = bf16[4,1310720]{1,0:T(4,128)(2,1)} reshape(bf16[5242880]{0:T(1024)(128)(2,1)} %all-gather.3.cloned.1.call-done) | data formatting | bytes 20971520 | tf_op jit(solution)/shard_map/all_gather | solution.py:55
  205.0 2.0 slice.45
  207.0 9.1 %slice.44 = bf16[4,1048576]{1,0:T(4,128)(2,1)} slice(bf16[4,1310720]{1,0:T(4,128)(2,1)} %reshape.179), slice={[0:4], [0:1048576]} | slice | bytes 16777216 | tf_op jit(solution)/shard_map/slice | solution.py:57
  216.1 3.0 fusion.8
  219.1 6.4 %convolution_convert_fusion = bf16[4,128,2048]{2,1,0:T(8,128)(2,1)} fusion(bf16[1,4,128,2048]{3,1,2,0:T(4,128)(2,1)} %bitcast.132, bf16[128,2048]{1,0:T(8,128)(2,1)S(1)} %copy-done.15, bf16[2048,128]{1,0:T(8,128)(2,1)S(1)} %copy-done.16, f32[4,128,128]{2,1,0:T(8,128)} %fusion.8), kind=kOutput, calls=%fused_computation.12 | convolution fusion | flops 538312704 | bytes 5505024 | tf_op jit(solution)/shard_map/nsq,ql->nsl/dot_general | solution.py:166
  225.5 4.5 copy.102
  230.0 13.3 %reshape_reshape_reshape_reshape.3 = bf16[4,64,2,4,2048]{4,3,2,1,0:T(4,128)(2,1)} reshape(bf16[4,1048576]{1,0:T(4,128)(2,1)} %slice.44) | data formatting | bytes 16777216 | tf_op jit(solution)/shard_map/reshape;reshape;reshape;reshape | solution.py:149
  243.3 14.2 %fusion.2 = f32[2,4,64,4,192]{4,2,3,1,0:T(8,128)} fusion(bf16[4,64,2,4,2048]{4,3,2,1,0:T(4,128)(2,1)} %reshape_reshape_reshape_reshape.3, bf16[2,2048,192]{1,2,0:T(8,128)(2,1)} %param.27), kind=kOutput, calls=%fused_computation.5 | convolution fusion | flops 1610612736 | bytes 11534336 | tf_op jit(solution)/shard_map/tsjcd,jdf->tsjcf/dot_general | solution.py:152
  257.4 16.0 %convert_bitcast_fusion = bf16[4,64,2,4,2048]{4,1,3,0,2:T(8,128)(2,1)} fusion(f32[2,4,64,4,192]{4,2,3,1,0:T(8,128)} %fusion.2, bf16[4,64,2,4,2048]{4,3,2,1,0:T(4,128)(2,1)} %reshape_reshape_reshape_reshape.3, bf16[2,192,2048]{2,1,0:T(8,128)(2,1)S(1)} %copy-done, bf16[2,2048,192]{1,2,0:T(8,128)(2,1)} %param.28), kind=kOutput, calls=%fused_computation.2 | convolution fusion | flops 3227779072 | bytes 21495808 | tf_op jit(solution)/shard_map/tsjcf,jfd->tsjcd/dot_general | solution.py:155
  273.4 10.2 %copy.101 = bf16[4,64,2,4,2048]{4,0,3,2,1:T(4,128)(2,1)S(1)} copy(bf16[4,64,2,4,2048]{4,1,3,0,2:T(8,128)(2,1)} %convert_bitcast_fusion) | data formatting | bytes 16777216 | tf_op jit(solution)/shard_map/tsjcf,jfd->tsjcd/transpose | solution.py:155
  283.7 14.4 %pad_maximum_fusion = bf16[4,640,2048]{2,0,1:T(4,128)(2,1)} fusion(bf16[4,128,2048]{2,0,1:T(4,128)(2,1)S(1)} %copy-done.2, bf16[4,512,2048]{2,0,1:T(4,128)(2,1)S(1)} %bitcast.126), kind=kLoop, calls=%fused_computation.1 | loop fusion | flops 5242880 | bytes 20971520 | tf_op jit(solution)/shard_map/concatenate | solution.py:173
  298.1 13.8 %copy.103 = bf16[4,640,2048]{2,1,0:T(8,128)(2,1)} copy(bf16[4,640,2048]{2,0,1:T(4,128)(2,1)} %pad_maximum_fusion) | data formatting | bytes 20971520 | tf_op jit(solution)/shard_map/concatenate | solution.py:173
  312.8 3.4 collective-permute-start
  316.3 96.8 %reduce-scatter.2.cloned.1.call-done = bf16[1,640,2048]{2,1,0:T(8,128)(2,1)} async-done(((bf16[4,640,2048]{2,1,0:T(8,128)(2,1)}), bf16[1,640,2048]{2,1,0:T(8,128)(2,1)}) %reduce-scatter.2.cloned.1.call-update) | async-done | bytes 2621456 | tf_op jit(solution)/shard_map/reduce_scatter | solution.py:172
  413.1 3.2 slice_bitcast_fusion
  416.3 11.0 %all-to-all-start.2 = ((bf16[64,8,2048]{2,1,0:T(8,128)(2,1)}), bf16[64,8,2048]{2,1,0:T(8,128)(2,1)S(1)}, u32[]{:S(2)}, u32[]{:S(2)}) async-start(bf16[64,8,2048]{2,1,0:T(8,128)(2,1)} %slice_bitcast_fusion), calls=%async_computation.3 | async-start | bytes 4194304 | tf_op jit(solution)/shard_map/all_to_all | solution.py:180
  427.7 1.6 reshape.188
  433.5 2.1 fusion.5
  438.9 1.4 multiply_reduce_fusion.1
  441.5 36.9 %all-to-all-done.2 = bf16[64,8,2048]{2,1,0:T(8,128)(2,1)S(1)} async-done(((bf16[64,8,2048]{2,1,0:T(8,128)(2,1)}), bf16[64,8,2048]{2,1,0:T(8,128)(2,1)S(1)}, u32[]{:S(2)}, u32[]{:S(2)}) %all-to-all-start.2) | async-done | bytes 2097184 | tf_op jit(solution)/shard_map/all_to_all | solution.py:180
  478.4 1.4 gather_fusion
  479.8 2.4 reshape.169
  482.1 4.9 multiply_reduce_fusion
  488.3 2.0 multiply_convert_fusion.1
  (76 shorter events, 14.1 us)
Async XLA Ops:
  7.2 250.3 %copy-start = (bf16[2,192,2048]{2,1,0:T(8,128)(2,1)S(1)}, bf16[2,192,2048]{2,1,0:T(8,128)(2,1)}, u32[]{:S(2)}) copy-start(bf16[2,192,2048]{2,1,0:T(8,128)(2,1)} %param.29) | copy-start | bytes 4718596
  13.1 12.0 %copy-start.3 = (bf16[128,2048]{1,0:T(8,128)(2,1)S(1)}, bf16[128,2048]{1,0:T(8,128)(2,1)}, u32[]{:S(2)}) copy-start(bf16[128,2048]{1,0:T(8,128)(2,1)} %param.23) | copy-start | bytes 1572868
  13.1 12.0 %copy-start.8 = (f32[2048]{0:T(1024)S(1)}, f32[2048]{0:T(1024)}, u32[]{:S(2)}) copy-start(f32[2048]{0:T(1024)} %param.24) | copy-start | bytes 24580
  13.1 61.2 %all-to-all-start = ((bf16[32,2,1,8,2048]{4,3,1,2,0:T(8,128)(2,1)}), bf16[32,2,1,8,2048]{4,3,1,2,0:T(8,128)(2,1)}, u32[]{:S(2)}, u32[]{:S(2)}) async-start(bf16[32,2,1,8,2048]{4,3,1,2,0:T(8,128)(2,1)} %bitcast.127), calls=%async_computation | async-start | bytes 4194304 | tf_op jit(solution)/shard_map/all_to_all | solution.py:43
  25.0 166.5 %all-gather.3.cloned.1.call-start = ((), (), s32[]{:S(2)}) async-start(), calls=%async_computation.5 | async-start | bytes 13107200 | tf_op jit(solution)/shard_map/all_gather | solution.py:55
  89.9 323.1 %reduce-scatter.2.cloned.1.call-start = ((), (), s32[]{:S(2)}) async-start(), calls=%async_computation.4 | async-start | bytes 13107200 | tf_op jit(solution)/shard_map/reduce_scatter | solution.py:172
  206.9 9.1 %copy-start.4 = (bf16[4,262144]{1,0:T(4,128)(2,1)}, bf16[4,262144]{1,0:T(4,128)(2,1)S(1)}, u32[]{:S(2)}) copy-start(bf16[4,262144]{1,0:T(4,128)(2,1)S(1)} %slice.45) | copy-start | bytes 6291460
  207.0 9.1 %copy-start.14 = (bf16[2048,128]{1,0:T(8,128)(2,1)S(1)}, bf16[2048,128]{1,0:T(8,128)(2,1)}, u32[]{:S(2)}) copy-start(bf16[2048,128]{1,0:T(8,128)(2,1)} %param.30) | copy-start | bytes 1572868
  216.1 3.1 copy-start.15
  216.1 3.1 copy-start.16
  273.4 10.2 %copy-start.2 = (bf16[4,128,2048]{2,0,1:T(4,128)(2,1)S(1)}, bf16[4,128,2048]{2,0,1:T(4,128)(2,1)}, u32[]{:S(2)}) copy-start(bf16[4,128,2048]{2,0,1:T(4,128)(2,1)} %copy.102) | copy-start | bytes 6291460
  311.8 0.9 copy-start.6
  311.8 1.0 copy-start.7
  312.8 116.7 %collective-permute-start = (bf16[2,128,256]{2,1,0:T(8,128)(2,1)S(1)}, bf16[2,128,256]{2,1,0:T(8,128)(2,1)}, u32[]{:S(2)}, u32[]{:S(2)}) collective-permute-start(bf16[2,128,256]{2,1,0:T(8,128)(2,1)S(1)} %pad_maximum_fusion.3), channel_id=1, source_target_pairs={{0,1},{1,2},{2,3},{3,4},{4,5},{5,6},{6,7},{7,8},{8,9},{9,10},{10,1... | collective-permute-start | bytes 393224 | tf_op jit(solution)/shard_map/ppermute | solution.py:24
  416.3 11.4 %copy-start.5 = (bf16[256,1024]{1,0:T(8,128)(2,1)S(1)}, bf16[256,1024]{1,0:T(8,128)(2,1)}, u32[]{:S(2)}) copy-start(bf16[256,1024]{1,0:T(8,128)(2,1)} %param.17) | copy-start | bytes 1572868
  416.3 13.0 %copy-start.12 = (f32[16]{0:T(128)S(1)}, f32[16]{0:T(128)}, u32[]{:S(2)}) copy-start(f32[16]{0:T(128)} %param.20) | copy-start | bytes 196
  416.3 13.1 %copy-start.11 = (f32[128,2]{0,1:T(2,128)S(1)}, f32[128,2]{0,1:T(2,128)}, u32[]{:S(2)}) copy-start(f32[128,2]{0,1:T(2,128)} %param.26) | copy-start | bytes 3076
  416.3 62.1 %all-to-all-start.2 = ((bf16[64,8,2048]{2,1,0:T(8,128)(2,1)}), bf16[64,8,2048]{2,1,0:T(8,128)(2,1)S(1)}, u32[]{:S(2)}, u32[]{:S(2)}) async-start(bf16[64,8,2048]{2,1,0:T(8,128)(2,1)} %slice_bitcast_fusion), calls=%async_computation.3 | async-start | bytes 4194304 | tf_op jit(solution)/shard_map/all_to_all | solution.py:180
  436.7 2.2 copy-start.13
  438.9 1.4 copy-start.9
  482.1 6.2 %copy-start.10 = (f32[2048]{0:T(1024)S(1)}, f32[2048]{0:T(1024)}, u32[]{:S(2)}) copy-start(f32[2048]{0:T(1024)} %param.33) | copy-start | bytes 24580
  482.1 8.3 %copy-start.1 = (bf16[2,192,2048]{2,1,0:T(8,128)(2,1)S(1)}, bf16[2,192,2048]{2,1,0:T(8,128)(2,1)}, u32[]{:S(2)}) copy-start(bf16[2,192,2048]{2,1,0:T(8,128)(2,1)} %param.29) | copy-start | bytes 4718596
Sparse Core Ops, SparseCore 0:
  90.0 101.3 all-gather.2
  312.0 101.0 reduce-scatter.1
where the time goes:
time: 506 us; the launch traced here: 498 us
  waiting for transfers between devices  284 us (56%)
  local copies, waits for them, and re-layouts  84 us (17%)
  matrix products  47.4 us (9%)
  other arithmetic  35.6 us (7%)
  starting transfers between devices  26.4 us (5%)
  between operations  14.8 us (3%)
  blocking collectives  5.42 us (1%)
    all_gather x1, waiting for transfers between devices, one_gather(): lines, at, done = (lax.all_gather(ravelled, axis), 0, [])  101 us
    reduce_scatter x1, waiting for transfers between devices, body(): lax.psum_scatter(jnp.concatenate([routed_part, shared_part], axis=1).asty...  96.8 us
    all_to_all x1, waiting for transfers between devices, turned_blocks(): out = lax.all_to_all(out, axes[k], k, k, tiled=True)  48.9 us
    all_to_all x1, waiting for transfers between devices, body(): lax.all_to_all(routed_out, EP, split_axis=0, concat_axis=0, tiled=True)  36.9 us
    dot_general x1, matrix products, body(): jnp.einsum('tsjcf,jfd->tsjcd', hidden, w_down, preferred_element_type=jnp...  16 us
    concatenate x1, other arithmetic, body(): jnp.concatenate([routed_part, shared_part], axis=1).astype(jnp.bfloat16)  14.4 us
    dot_general x1, matrix products, body(): jnp.einsum('tsjcd,jdf->tsjcf', routed, w_gate, preferred_element_type=jnp...  14.2 us
    concatenate x1, local copies, waits for them, and re-layouts, body(): jnp.concatenate([routed_part, shared_part], axis=1).astype(jnp.bfloat16)  13.8 us
  transfers between devices with their start and end apart: 5, of which 4 were waited for; matrix products, arithmetic and copies ran while one was open for 3% of the time, Pallas kernels for 0%

commit v1 on v0

v1 whole, which is shorter than its diff:
```python
import math

import jax
import jax.numpy as jnp
from jax import lax
from jax.experimental import pallas as pl
from jax.experimental.pallas import tpu as pltpu
from jax.sharding import Mesh
from jax.sharding import PartitionSpec as P


HEADS = 16
KV_HEADS = 4
HEAD_DIM = 64
WINDOW = 128
CAP = 4
BLOCK = 256
EP = ("z", "y", "c")
EP_TP = ("z", "y", "c", "tp")
CHIPS = ("z", "y", "tp")
CORE_TP = ("c", "tp")
EPS = 1e-06
NEGATIVE = -1e30


f32 = jnp.float32
bf16 = jnp.bfloat16
VMEM = pltpu.VMEM
ANY = pl.ANY


def iota(shape, dim):
    return lax.broadcasted_iota(jnp.int32, shape, dim)


def dot(a, b):
    return jnp.dot(a, b, preferred_element_type=f32)


def dot_t(a, b):
    return lax.dot_general(a, b, (((1,), (1,)), ((), ())), preferred_element_type=f32)


def in_vmem(count):
    return [pl.BlockSpec(memory_space=VMEM)] * count


def from_behind(block, axis, distance):
    devices = range(lax.axis_size(axis))
    route = [(i - distance, i) for i in devices if i - distance in devices]
    return lax.ppermute(block, axis, route)


def rms_scale(inputs, gain_vec):
    mean_sq = jnp.mean(inputs * inputs, axis=-1, keepdims=True)
    return inputs * lax.rsqrt(mean_sq + EPS) * gain_vec


def slot_rows(ids, lanes):
    tokens = ids.shape[1]
    shape = (tokens, tokens)
    eye = iota(shape, 0) == iota(shape, 1)
    across = [ids[k : k + 1, :] for k in range(2)]
    down = [jnp.sum(jnp.where(eye, a, 0.0), axis=1, keepdims=True) for a in across]
    if lanes:
        mine, theirs, axis, earlier = across, down, 0, iota(shape, 0) < iota(shape, 1)
    else:
        mine, theirs, axis, earlier = down, across, 1, iota(shape, 1) < iota(shape, 0)
    rows = []
    for k in range(2):
        place = sum(
            jnp.sum(jnp.where((mine[k] == other) & earlier, 1.0, 0.0), axis=axis, keepdims=True)
            for other in theirs
        )
        rows.append((mine[k] * (2 * CAP) + place).astype(jnp.int32))
    return rows


def pack_kernel(x_ref, gain_ref, ids_ref, packed_ref, normed_ref, stacked):
    half = x_ref.shape[1] // 2
    tokens = x_ref.shape[0]
    step = pl.program_id(0)
    block = packed_ref.shape[0]

    @pl.when(step == 0)
    def _():
        x = x_ref[...].astype(f32)
        normed = rms_scale(x, gain_ref[...]).astype(bf16)
        normed_ref[...] = normed
        stacked[:tokens, :] = normed[:, :half]
        stacked[tokens:, :] = normed[:, half:]

    rows = slot_rows(ids_ref[...].astype(f32), True)
    r = iota((block, tokens), 0) + step * block
    chosen = jnp.concatenate(
        [
            jnp.where((r == rows[0] + h * CAP) | (r == rows[1] + h * CAP), 1.0, 0.0).astype(bf16)
            for h in range(2)
        ],
        axis=1,
    )
    packed_ref[...] = dot(chosen, stacked[...]).astype(bf16)


def pack(x, gain, ids, slots):
    tokens, width = x.shape
    steps = 4
    total = 2 * slots
    return pl.pallas_call(
        pack_kernel,
        grid=(steps,),
        in_specs=[
            pl.BlockSpec((tokens, width), lambda i: (0, 0)),
            pl.BlockSpec((1, width), lambda i: (0, 0)),
            pl.BlockSpec((2, tokens), lambda i: (0, 0)),
        ],
        out_specs=[
            pl.BlockSpec((total // steps, width // 2), lambda i: (i, 0)),
            pl.BlockSpec((tokens, width), lambda i: (0, 0)),
        ],
        out_shape=[
            jax.ShapeDtypeStruct((total, width // 2), bf16),
            jax.ShapeDtypeStruct((tokens, width), bf16),
        ],
        scratch_shapes=[VMEM((2 * tokens, width // 2), bf16)],
        cost_estimate=pl.CostEstimate(
            flops=2 * total * tokens * width, bytes_accessed=6 * tokens * width, transcendentals=0
        ),
        name="pack",
    )(x, gain, ids)


def expert_kernel(own_ref, recv, *refs):
    own, other = refs[:4], refs[4:8]
    out_ref, arrived, gate, up, down, rows, hidden, sem, sems = refs[8:]
    part = own[0].shape[0] // 3
    half = recv.shape[1]
    groups = recv.shape[0] // BLOCK

    def fill(k, m, piece):
        into = (gate, up, down)[m]
        return pltpu.make_async_copy(
            piece.at[pl.ds(m * part, part)], into.at[pl.ds(k * part, part)], sems.at[m, k]
        )

    rows_in = pltpu.make_async_copy(recv, arrived, sem)
    rows_in.start()
    for mine, pieces in ((1, own), (0, other)):

        @pl.when(own_ref[0] == mine)
        def _():
            for m in range(3):
                for k, piece in enumerate(pieces):
                    fill(k, m, piece).start()

    def wait(m):
        for k in range(4):
            fill(k, m, own[k]).wait()

    a, b = iota((BLOCK // 2, BLOCK), 0), iota((BLOCK // 2, BLOCK), 1)
    first = (a // CAP) * (2 * CAP) + a % CAP
    picks = [jnp.where(b == first + h * CAP, 1.0, 0.0).astype(bf16) for h in range(2)]
    rows_in.wait()

    def sort_rows(i, carry):
        block = arrived[pl.ds(pl.multiple_of(i * BLOCK, BLOCK), BLOCK), :]
        at = pl.ds(pl.multiple_of(i * (BLOCK // 2), BLOCK // 2), BLOCK // 2)
        for h in range(2):
            rows[at, h * half : (h + 1) * half] = dot(picks[h], block).astype(bf16)
        return carry

    lax.fori_loop(0, groups, sort_rows, 0)
    wait(0)
    wait(1)

    def units(n, carry):
        at = pl.ds(pl.multiple_of(n * BLOCK, BLOCK), BLOCK)
        x = rows[...]
        g = dot_t(x, gate[at, :])
        u = dot_t(x, up[at, :])
        hidden[:, at] = (g / (1.0 + jnp.exp(-g)) * u).astype(bf16)
        return carry

    lax.fori_loop(0, hidden.shape[1] // BLOCK, units, 0)
    wait(2)
    a, b = iota((BLOCK, BLOCK), 0), iota((BLOCK, BLOCK), 1)
    b, h = b % (BLOCK // 2), b // (BLOCK // 2)
    back = jnp.where(a == (b // CAP) * (2 * CAP) + b % CAP + h * CAP, 1.0, 0.0).astype(bf16)

    def columns(n, carry):
        at = pl.multiple_of(n * BLOCK, BLOCK)
        x = hidden[...]
        left = dot(x, down[:, pl.ds(at, BLOCK)]).astype(bf16)
        right = dot(x, down[:, pl.ds(half + at, BLOCK)]).astype(bf16)
        for i in range(groups):
            mine = slice(i * (BLOCK // 2), (i + 1) * (BLOCK // 2))
            both = jnp.concatenate([left[mine], right[mine]], axis=0)
            out_ref[i * BLOCK : (i + 1) * BLOCK, pl.ds(at, BLOCK)] = dot(back, both).astype(bf16)
        return carry

    lax.fori_loop(0, half // BLOCK, columns, 0)


def expert(own, recv, mine, others):
    total, half = recv.shape
    units = 4 * mine[0].shape[0] // 3
    return pl.pallas_call(
        expert_kernel,
        in_specs=[pl.BlockSpec(memory_space=pltpu.SMEM)] + [pl.BlockSpec(memory_space=ANY)] * 9,
        out_specs=pl.BlockSpec(memory_space=VMEM),
        out_shape=jax.ShapeDtypeStruct((total, half), bf16),
        scratch_shapes=[
            VMEM((total, half), bf16),
            VMEM((units, 2 * half), bf16),
            VMEM((units, 2 * half), bf16),
            VMEM((units, 2 * half), bf16),
            VMEM((total // 2, 2 * half), bf16),
            VMEM((total // 2, units), bf16),
            pltpu.SemaphoreType.DMA,
            pltpu.SemaphoreType.DMA((3, 4)),
        ],
        cost_estimate=pl.CostEstimate(
            flops=6 * total * half * units,
            bytes_accessed=4 * total * half + 12 * half * units,
            transcendentals=total * units // 2,
        ),
        name="expert",
    )(own, recv, *mine, *others)


def shared_prep_kernel(core_ref, gate_ref, up_ref, down_ref, out_ref):
    depth = gate_ref.shape[0] // 2
    units = gate_ref.shape[1]
    core = core_ref[0]
    at = pl.ds(pl.multiple_of(core * depth, depth), depth)
    out_ref[:depth, :] = gate_ref[at, :]
    out_ref[depth : 2 * depth, :] = up_ref[at, :]
    for t in range(depth // 128):
        lane = pl.multiple_of(core * depth + t * 128, 128)
        out_ref[2 * depth + t * units : 2 * depth + (t + 1) * units, :] = down_ref[
            :, pl.ds(lane, 128)
        ]


def shared_prep(core, gate, up, down):
    return pl.pallas_call(
        shared_prep_kernel,
        in_specs=[pl.BlockSpec(memory_space=pltpu.SMEM)] + in_vmem(3),
        out_specs=pl.BlockSpec(memory_space=VMEM),
        out_shape=jax.ShapeDtypeStruct((gate.shape[0] // 2 * 3, gate.shape[1]), bf16),
        cost_estimate=pl.CostEstimate(flops=1000, bytes_accessed=12 * gate.size, transcendentals=0),
        name="shared_prep",
    )(core, gate, up, down)


def shared_kernel(core_ref, x_ref, *refs):
    mine, theirs = refs[:4], refs[4:8]
    out_ref, into, down = refs[8:]
    depth = x_ref.shape[1] // 2
    units = mine[0].shape[1]
    core = core_ref[0]
    for side, pieces in ((core, mine), (1 - core, theirs)):
        top = pl.multiple_of(side * depth, depth)
        for k, piece in enumerate(pieces):
            for m in range(2):
                lane = (m * 4 + k) * units
                into[pl.ds(top, depth), lane : lane + units] = piece[m * depth : (m + 1) * depth, :]
            for t in range(depth // 128):
                lane = pl.multiple_of(side * depth + t * 128, 128)
                at = 2 * depth + t * units
                down[k * units : (k + 1) * units, pl.ds(lane, 128)] = piece[at : at + units, :]
    both = dot(x_ref[...], into[...])
    g, u = both[:, : 4 * units], both[:, 4 * units :]
    hidden = (g / (1.0 + jnp.exp(-g)) * u).astype(bf16)
    out_ref[...] = dot(hidden, down[...])


def shared_expert(core, normed, mine, theirs):
    tokens, width = normed.shape
    units = 4 * mine[0].shape[1]
    return pl.pallas_call(
        shared_kernel,
        in_specs=[pl.BlockSpec(memory_space=pltpu.SMEM)] + in_vmem(9),
        out_specs=pl.BlockSpec(memory_space=VMEM),
        out_shape=jax.ShapeDtypeStruct((tokens, width), f32),
        scratch_shapes=[VMEM((width, 2 * units), bf16), VMEM((units, width), bf16)],
        cost_estimate=pl.CostEstimate(
            flops=6 * tokens * width * units,
            bytes_accessed=6 * width * units,
            transcendentals=tokens * units,
        ),
        name="shared_expert",
    )(core, normed, *mine, *theirs)


def combine_kernel(back_ref, ids_ref, weight_ref, shared_ref, gain_ref, out_ref):
    tokens = out_ref.shape[0]
    slots, half = back_ref.shape
    first = slot_rows(ids_ref[...].astype(f32), False)
    eye = iota((tokens, tokens), 0) == iota((tokens, tokens), 1)
    weights = [
        jnp.sum(jnp.where(eye, weight_ref[k : k + 1, :], 0.0), axis=1, keepdims=True)
        for k in range(2)
    ]
    r = iota((tokens, slots), 1)
    back = back_ref[...]
    halves = []
    for h in range(2):
        spread = jnp.where(r == first[0] + h * CAP, weights[0], 0.0) + jnp.where(
            r == first[1] + h * CAP, weights[1], 0.0
        )
        coarse = spread.astype(bf16)
        fine = (spread - coarse.astype(f32)).astype(bf16)
        summed = dot(jnp.concatenate([coarse, fine], axis=0), back)
        halves.append(
            summed[:tokens] + summed[tokens:] + shared_ref[:, h * half : (h + 1) * half]
        )
    square = sum(jnp.sum(v * v, axis=1, keepdims=True) for v in halves)
    scale = lax.rsqrt(square / (2 * half) + EPS)
    for h, v in enumerate(halves):
        at = slice(h * half, (h + 1) * half)
        out_ref[:, at] = (v * scale * gain_ref[:, at]).astype(bf16)


def combine(back, ids, weights, shared, gain):
    slots, half = back.shape
    tokens = ids.shape[1]
    return pl.pallas_call(
        combine_kernel,
        in_specs=in_vmem(5),
        out_specs=pl.BlockSpec(memory_space=VMEM),
        out_shape=jax.ShapeDtypeStruct((tokens, 2 * half), bf16),
        cost_estimate=pl.CostEstimate(
            flops=8 * tokens * slots * half, bytes_accessed=2 * slots * half, transcendentals=0
        ),
        name="combine",
    )(back, ids, weights, shared, gain)


def attention_kernel(
    first_ref, sink_ref, q_ref, k_ref, v_ref, rim_ref, weight_ref, gain_ref, out_ref, keys, values, mix, wide
):
    tokens = q_ref.shape[0]
    lanes = 2 * HEAD_DIM
    group = HEADS // KV_HEADS
    tiles = k_ref.shape[1] // lanes
    for into, rim, own in ((keys, 0, k_ref), (values, 1, v_ref)):
        for t in range(tiles):
            at = slice(t * lanes, (t + 1) * lanes)
            rows = jnp.concatenate([rim_ref[rim, :, at], own[:, at]], axis=0)
            into[2 * t] = rows
            into[2 * t + 1] = jnp.concatenate([rows[:, HEAD_DIM:], rows[:, :HEAD_DIM]], axis=1)
    i, j = iota((WINDOW, 2 * WINDOW), 0), iota((WINDOW, 2 * WINDOW), 1)
    low = iota((WINDOW, lanes), 1) < HEAD_DIM

    for n in range(tokens // WINDOW):
        band = slice(n * WINDOW, (n + 2) * WINDOW)
        at = slice(n * WINDOW, (n + 1) * WINDOW)
        inside = (j > i) & (j <= i + WINDOW)
        if n == 0:
            inside = inside & (j >= first_ref[0] * WINDOW)
        for g in range(KV_HEADS):
            kt = [2 * (g // 2) + (g + s) % 2 for s in range(2)]
            for t in range(group // 2):
                tile = g * (group // 2) + t
                q = q_ref[at, tile * lanes : (tile + 1) * lanes]
                mixed = []
                for s in range(2):
                    mine = jnp.where(low if s == 0 else ~low, q, jnp.zeros_like(q))
                    score = dot_t(mine, keys[kt[s], band, :]) * (1.0 / math.sqrt(HEAD_DIM))
                    score = jnp.where(inside, score, NEGATIVE)
                    sink = sink_ref[2 * tile + s]
                    top = jnp.maximum(jnp.max(score, axis=1, keepdims=True), sink)
                    e = jnp.exp(score - top)
                    below = jnp.sum(e, axis=1, keepdims=True) + jnp.exp(sink - top)
                    mixed.append(dot((e / below).astype(bf16), values[kt[s], band, :]))
                mix[at, tile * lanes : (tile + 1) * lanes] = jnp.where(
                    low, mixed[0], mixed[1]
                ).astype(bf16)

    width = 512
    square = jnp.zeros((tokens, 1), f32)
    for n in range(out_ref.shape[1] // width):
        at = slice(n * width, (n + 1) * width)
        p = dot(mix[...], weight_ref[:, at])
        wide[:, at] = p
        square = square + jnp.sum(p * p, axis=1, keepdims=True)
    scale = lax.rsqrt(square / out_ref.shape[1] + EPS)
    for n in range(out_ref.shape[1] // width):
        at = slice(n * width, (n + 1) * width)
        out_ref[:, at] = (wide[:, at] * scale * gain_ref[:, at]).astype(bf16)


def attention(first, sinks, queries, keys, values, rim, weight, gain):
    tokens, wide = queries.shape[0], weight.shape[1]
    lanes = 2 * HEAD_DIM
    rows = tokens + WINDOW
    return pl.pallas_call(
        attention_kernel,
        in_specs=[pl.BlockSpec(memory_space=pltpu.SMEM)] * 2 + in_vmem(6),
        out_specs=pl.BlockSpec(memory_space=VMEM),
        out_shape=jax.ShapeDtypeStruct((tokens, wide), bf16),
        scratch_shapes=[
            VMEM((KV_HEADS, rows, lanes), bf16),
            VMEM((KV_HEADS, rows, lanes), bf16),
            VMEM((tokens, HEADS * HEAD_DIM), bf16),
            VMEM((tokens, wide), f32),
        ],
        cost_estimate=pl.CostEstimate(
            flops=2 * tokens * HEADS * HEAD_DIM * (wide + 8 * WINDOW),
            bytes_accessed=2 * weight.size + 4 * tokens * wide,
            transcendentals=tokens * HEADS * 2 * WINDOW,
        ),
        name="attention",
    )(first, sinks, queries, keys, values, rim, weight, gain)


def body(
    att_queries,
    att_keys,
    att_values,
    sink_logits,
    out_weight,
    att_gain,
    moe_in,
    pre_gain,
    expert_ids,
    routed_expert_weight,
    w_gate,
    w_up,
    w_down,
    common_expert_gate_weight,
    common_expert_up_weight,
    common_expert_down_weight,
    moe_gain,
):
    x, core = lax.axis_index("tp"), lax.axis_index("c")
    tp = lax.axis_size("tp")
    homes = [(i // 2, i) for i in range(tp)]
    to_home = {
        k: [(c * tp + (i - k) % tp, c * tp + i) for c, i in homes] for k in range(1, tp)
    }
    to_other = [(c * tp + i, (1 - c) * tp + i) for c, i in homes]
    own = (core == x // 2).astype(jnp.int32).reshape(1)
    core_at = core.astype(jnp.int32).reshape(1)

    kv_rows = jnp.stack([att_keys, att_values])
    rim_rows = from_behind(kv_rows[:, att_keys.shape[0] - WINDOW :], EP_TP, 1)
    first = (lax.axis_index(EP_TP) == 0).astype(jnp.int32).reshape(1)

    gate_t, up_t = w_gate.transpose(0, 2, 1), w_up.transpose(0, 2, 1)

    def expert_of(parity, arrays):
        j = (x + parity) % 2
        return jnp.concatenate(
            [lax.dynamic_index_in_dim(a, j, 0, keepdims=False) for a in arrays], axis=0
        )

    def homeward(k, piece):
        return lax.ppermute(piece, CORE_TP, to_home[k])

    def across(pieces):
        return [lax.ppermute(v, CORE_TP, to_other) for v in pieces]

    pieces = {p: expert_of(p, (gate_t, up_t, w_down)) for p in (1, 0)}
    mine = [pieces[0]] + [homeward(k, pieces[k % 2]) for k in (1, 3, 2)]
    mine[2], mine[3] = mine[3], mine[2]
    others = across(mine)

    ids_t = expert_ids.T
    packed, normed = pack(moe_in, pre_gain.reshape(1, -1), ids_t, 128 * CAP)
    chips = packed.shape[0] // (2 * CAP)
    arrived = lax.all_to_all(
        packed.reshape(chips, 2 * CAP, -1), CHIPS, split_axis=0, concat_axis=0, tiled=True
    ).reshape(packed.shape)

    mixer_out = attention(
        first,
        sink_logits,
        att_queries,
        att_keys,
        att_values,
        rim_rows,
        out_weight,
        att_gain.reshape(1, -1),
    )

    out = expert(own, arrived, mine, others)
    returned = lax.all_to_all(
        out.reshape(chips, 2 * CAP, -1), CHIPS, split_axis=0, concat_axis=0, tiled=True
    ).reshape(out.shape)

    prepared = shared_prep(
        core_at,
        common_expert_gate_weight,
        common_expert_up_weight,
        common_expert_down_weight,
    )
    blocks = [prepared]
    for k in range(1, tp):
        blocks.append(lax.ppermute(prepared, "tp", [(i, (i + k) % tp) for i in range(tp)]))
    theirs = [lax.ppermute(v, "c", [(0, 1), (1, 0)]) for v in blocks]
    shared_sum = shared_expert(core_at, normed, blocks, theirs)
    experts_out = combine(
        returned, ids_t, routed_expert_weight.T, shared_sum, moe_gain.reshape(1, -1)
    )
    return (mixer_out, experts_out)


def solution(mesh):
    split = Mesh(mesh.devices.reshape(8, 4, 2, mesh.shape["tp"]), ("z", "y", "c", "tp"))
    placed = (
        P(EP_TP, None),
        P(EP_TP, None),
        P(EP_TP, None),
        P(),
        P(),
        P(),
        P(EP_TP, None),
        P(),
        P(EP_TP, None),
        P(EP_TP, None),
        P(EP, None, "tp"),
        P(EP, None, "tp"),
        P(EP, "tp", None),
        P(None, "tp"),
        P(None, "tp"),
        P("tp", None),
        P(),
    )
    return jax.shard_map(
        body,
        mesh=split,
        in_specs=placed,
        out_specs=(P(EP_TP, None), P(EP_TP, None)),
        check_vma=False,
    )
```

time: 506 us -> 215 us (0.42); the launches traced: 498 us -> 214 us
  waiting for transfers between devices: 284 us -> 108 us
  local copies, waits for them, and re-layouts: 84 us -> 4.53 us
  matrix products: 47.4 us -> 0 us
  Pallas kernels: 0 us -> 39.7 us
  other arithmetic: 35.6 us -> 1.84 us
  starting transfers between devices: 26.4 us -> 58.4 us
  between operations: 14.8 us -> 0.85 us
  blocking collectives: 5.42 us -> 0 us
    all_gather x1 -> x0, waiting for transfers between devices: 101 us -> none  [one_gather(): lines, at, done = (lax.all_gather(ravelled, axis), 0, [])]
    ppermute x0 -> x14, waiting for transfers between devices: none -> 101 us  [the longest x3 51.2 us: body(): lax.ppermute(prepared, 'tp', [(i, (i + k) % tp) for i in range(tp)])]
    reduce_scatter x1 -> x0, waiting for transfers between devices: 96.8 us -> none  [body(): lax.psum_scatter(jnp.concatenate([routed_part, shared_part], axis=1).asty...]
    all_to_all x2, waiting for transfers between devices: 85.7 us -> 0.01 us  [the longest x1 0.01 us: body(): lax.all_to_all(packed.reshape(chips, 2 * CAP, -1), CHIPS, split_axis=0, c...]
    dot_general x8 -> x0, matrix products: 47.4 us -> none  [the longest x1 16 us: body(): jnp.einsum('tsjcf,jfd->tsjcd', hidden, w_down, preferred_element_type=jnp...]
    pallas_call x0 -> x6, Pallas kernels: none -> 39.7 us  [the longest x1 14.2 us: expert(): pl.pallas_call(expert_kernel, in_specs=[pl.BlockSpec(memory_space=pltpu.S...]
    ppermute x0 -> x14, starting transfers between devices: none -> 22.9 us  [the longest x4 10.8 us: across(): return [lax.ppermute(v, CORE_TP, to_other) for v in pieces]]
    concatenate x3 -> x2, other arithmetic: 22.9 us -> 1.83 us  [expert_of(): jnp.concatenate([lax.dynamic_index_in_dim(a, j, 0, keepdims=False) for a...]
  transfers between devices with their start and end apart: 5 -> 17, of which waited for: 4 -> 6; matrix products, arithmetic and copies ran while one was open for 3% -> 0% of each run, Pallas kernels for 0% -> 10%
where the time goes in v1:
time: 215 us; the launch traced here: 214 us
  waiting for transfers between devices  108 us (50%)
  starting transfers between devices  58.4 us (27%)
  Pallas kernels  39.7 us (18%)
  local copies, waits for them, and re-layouts  4.53 us (2%)
    ppermute x3, waiting for transfers between devices, body(): lax.ppermute(prepared, 'tp', [(i, (i + k) % tp) for i in range(tp)])  51.2 us
    ppermute x3, waiting for transfers between devices, homeward(): return lax.ppermute(piece, CORE_TP, to_home[k])  45.2 us
    all_to_all x1, starting transfers between devices, body(): lax.all_to_all(packed.reshape(chips, 2 * CAP, -1), CHIPS, split_axis=0, c...  20.1 us
    pallas_call x1, Pallas kernels, expert(): pl.pallas_call(expert_kernel, in_specs=[pl.BlockSpec(memory_space=pltpu.S...  14.2 us
    all_to_all x1, starting transfers between devices, body(): lax.all_to_all(out.reshape(chips, 2 * CAP, -1), CHIPS, split_axis=0, conc...  13.3 us
    ppermute x4, starting transfers between devices, across(): return [lax.ppermute(v, CORE_TP, to_other) for v in pieces]  10.8 us
    pallas_call x1, Pallas kernels, attention(): pl.pallas_call(attention_kernel, in_specs=[pl.BlockSpec(memory_space=pltp...  7.94 us
    ppermute x1, waiting for transfers between devices, from_behind(): return lax.ppermute(block, axis, route)  7.59 us
  transfers between devices with their start and end apart: 17, of which 6 were waited for; matrix products, arithmetic and copies ran while one was open for 0% of the time, Pallas kernels for 10%

profile of v1, /device:TPU:8, one launch (start us, length us, event | category | flops | bytes accessed | tf_op | source)
XLA Modules:
  0.0 213.7 jit_solution(11226588407565812547)
XLA Ops:
  0.7 1.7 dynamic-slice_bitcast_fusion
  2.5 0.5 copy-done.2
  3.0 0.2 dynamic-slice_bitcast_fusion.1
  3.2 1.7 pad_maximum_fusion.1
  4.9 3.4 %collective-permute-start.1 = (bf16[576,2048]{1,0:T(8,128)(2,1)}, bf16[576,2048]{1,0:T(8,128)(2,1)}, u32[]{:S(2)}, u32[]{:S(2)}) collective-permute-start(bf16[576,2048]{1,0:T(8,128)(2,1)} %pad_maximum_fusion.1), channel_id=1, source_target_pairs={{3,0},{0,1},{5,6},{6,7},{11,8},{8,9},{13,14},{14,15},{19,16},{16,1... | collective-permute-start | bytes 7077896 | tf_op jit(solution)/shard_map/ppermute | solution.py:460
  8.3 1.3 collective-permute-start.3
  9.8 1.3 collective-permute-start.2
  11.1 4.1 %pack.1 = (bf16[1024,1024]{1,0:T(8,128)(2,1)}, bf16[128,2048]{1,0:T(8,128)(2,1)}) custom-call(bf16[128,2048]{1,0:T(8,128)(2,1)} %x_ref.1, f32[1,2048]{1,0:T(1,128)} %bitcast.40, s32[2,128]{1,0:T(2,128)} %bitcast.42), custom_call_target="tpu_custom_call" | custom-call | flops 536870912 | bytes 1572864 | tf_op jit(solution)/shard_map/pack/pallas_call | solution.py:109
  15.2 20.1 %all-to-all-start = ((bf16[128,8,1024]{2,1,0:T(8,128)(2,1)}), bf16[128,8,1024]{2,1,0:T(8,128)(2,1)}, u32[]{:S(2)}, u32[]{:S(2)}) async-start(bf16[128,8,1024]{2,1,0:T(8,128)(2,1)} %bitcast.36), calls=%async_computation | async-start | bytes 4194304 | tf_op jit(solution)/shard_map/all_to_all | solution.py:473
  35.3 2.7 %collective-permute-start.4 = (bf16[576,2048]{1,0:T(8,128)(2,1)S(1)}, bf16[576,2048]{1,0:T(8,128)(2,1)}, u32[]{:S(2)}, u32[]{:S(2)}) collective-permute-start(bf16[576,2048]{1,0:T(8,128)(2,1)S(1)} %pad_maximum_fusion.refs_0_), channel_id=1, source_target_pairs={{0,4},{1,5},{6,2},{7,3},{8,12},{9,13},{14,10},{15,11},{16,20},{17,... | collective-permute-start | bytes 7077896 | tf_op jit(solution)/shard_map/ppermute | solution.py:463
  38.0 45.2 %collective-permute-done.1.refs_1_ = bf16[576,2048]{1,0:T(8,128)(2,1)} collective-permute-done((bf16[576,2048]{1,0:T(8,128)(2,1)}, bf16[576,2048]{1,0:T(8,128)(2,1)}, u32[]{:S(2)}, u32[]{:S(2)}) %collective-permute-start.1) | collective-permute-done | bytes 2359328 | tf_op jit(solution)/shard_map/ppermute | solution.py:460
  83.2 2.7 %collective-permute-start.5 = (bf16[576,2048]{1,0:T(8,128)(2,1)}, bf16[576,2048]{1,0:T(8,128)(2,1)}, u32[]{:S(2)}, u32[]{:S(2)}) collective-permute-start(bf16[576,2048]{1,0:T(8,128)(2,1)} %collective-permute-done.1.refs_1_), channel_id=1, source_target_pairs={{0,4},{1,5},{6,2},{7,3},{8,12},{9,13},{14,10},{15,11},{16,20},{17,... | collective-permute-start | bytes 7077896 | tf_op jit(solution)/shard_map/ppermute | solution.py:463
  85.9 2.7 %collective-permute-start.7 = (bf16[576,2048]{1,0:T(8,128)(2,1)}, bf16[576,2048]{1,0:T(8,128)(2,1)}, u32[]{:S(2)}, u32[]{:S(2)}) collective-permute-start(bf16[576,2048]{1,0:T(8,128)(2,1)} %collective-permute-done.3.refs_3_), channel_id=1, source_target_pairs={{0,4},{1,5},{6,2},{7,3},{8,12},{9,13},{14,10},{15,11},{16,20},{17,... | collective-permute-start | bytes 7077896 | tf_op jit(solution)/shard_map/ppermute | solution.py:463
  88.6 2.7 %collective-permute-start.6 = (bf16[576,2048]{1,0:T(8,128)(2,1)}, bf16[576,2048]{1,0:T(8,128)(2,1)}, u32[]{:S(2)}, u32[]{:S(2)}) collective-permute-start(bf16[576,2048]{1,0:T(8,128)(2,1)} %collective-permute-done.2.refs_2_), channel_id=1, source_target_pairs={{0,4},{1,5},{6,2},{7,3},{8,12},{9,13},{14,10},{15,11},{16,20},{17,... | collective-permute-start | bytes 7077896 | tf_op jit(solution)/shard_map/ppermute | solution.py:463
  91.3 1.0 collective-permute-done.7.refs_7_
  92.3 3.4 %collective-permute-done.6.refs_6_ = bf16[576,2048]{1,0:T(8,128)(2,1)} collective-permute-done((bf16[576,2048]{1,0:T(8,128)(2,1)}, bf16[576,2048]{1,0:T(8,128)(2,1)}, u32[]{:S(2)}, u32[]{:S(2)}) %collective-permute-start.6) | collective-permute-done | bytes 2359328 | tf_op jit(solution)/shard_map/ppermute | solution.py:463
  95.7 14.2 %expert.1 = bf16[1024,1024]{1,0:T(8,128)(2,1)} custom-call(s32[1]{0:T(128)} %bitcast.4.own_ref, bf16[1024,1024]{1,0:T(8,128)(2,1)} %bitcast.8.recv, bf16[576,2048]{1,0:T(8,128)(2,1)} %copy-done, bf16[576,2048]{1,0:T(8,128)(2,1)} %collective-permute-done.1.refs_1_, bf16[576,2048]{1,0:T(8,128)(2,1)} %collective-permute-done.2.refs_2_, ...), custom_call_target="tpu_custom_call" | custom-call | flops 4831838208 | bytes 13631488 | tf_op jit(solution)/shard_map/expert/pallas_call | solution.py:207
  110.0 13.3 %all-to-all-start.1 = ((bf16[128,8,1024]{2,1,0:T(8,128)(2,1)}), bf16[128,8,1024]{2,1,0:T(8,128)(2,1)S(1)}, u32[]{:S(2)}, u32[]{:S(2)}) async-start(bf16[128,8,1024]{2,1,0:T(8,128)(2,1)} %bitcast.34), calls=%async_computation.1 | async-start | bytes 4194304 | tf_op jit(solution)/shard_map/all_to_all | solution.py:489
  123.3 2.4 %shared_prep.1.refs_0_ = bf16[3072,128]{1,0:T(8,128)(2,1)} custom-call(s32[1]{0:T(128)} %bitcast.22.core_ref, bf16[2048,128]{1,0:T(8,128)(2,1)} %gate_ref.1, bf16[2048,128]{1,0:T(8,128)(2,1)} %up_ref.1, bf16[128,2048]{1,0:T(8,128)(2,1)} %down_ref.1), custom_call_target="tpu_custom_call" | custom-call | flops 1000 | bytes 3145728 | tf_op jit(solution)/shard_map/shared_prep/pallas_call | solution.py:246
  125.6 1.5 collective-permute-start.8
  127.1 2.7 %collective-permute-start.9 = (bf16[3072,128]{1,0:T(8,128)(2,1)}, bf16[3072,128]{1,0:T(8,128)(2,1)}, u32[]{:S(2)}, u32[]{:S(2)}) collective-permute-start(bf16[3072,128]{1,0:T(8,128)(2,1)} %shared_prep.1.refs_0_), channel_id=1, source_target_pairs={{0,2},{1,3},{2,0},{3,1},{4,6},{5,7},{6,4},{7,5},{8,10},{9,11},{10,... | collective-permute-start | bytes 2359304 | tf_op jit(solution)/shard_map/ppermute | solution.py:501
  129.8 1.5 collective-permute-start.10
  131.2 28.9 %collective-permute-done.8.refs_1_ = bf16[3072,128]{1,0:T(8,128)(2,1)S(1)} collective-permute-done((bf16[3072,128]{1,0:T(8,128)(2,1)}, bf16[3072,128]{1,0:T(8,128)(2,1)S(1)}, u32[]{:S(2)}, u32[]{:S(2)}) %collective-permute-start.8) | collective-permute-done | bytes 786464 | tf_op jit(solution)/shard_map/ppermute | solution.py:501
  160.2 22.2 %collective-permute-done.9.refs_2_ = bf16[3072,128]{1,0:T(8,128)(2,1)} collective-permute-done((bf16[3072,128]{1,0:T(8,128)(2,1)}, bf16[3072,128]{1,0:T(8,128)(2,1)}, u32[]{:S(2)}, u32[]{:S(2)}) %collective-permute-start.9) | collective-permute-done | bytes 786464 | tf_op jit(solution)/shard_map/ppermute | solution.py:501
  182.4 0.5 collective-permute-start.14
  182.9 2.1 collective-permute-start
  185.1 7.6 %collective-permute-done.rim_ref = bf16[2,128,256]{2,1,0:T(8,128)(2,1)S(1)} collective-permute-done((bf16[2,128,256]{2,1,0:T(8,128)(2,1)S(1)}, bf16[2,128,256]{2,1,0:T(8,128)(2,1)S(1)}, u32[]{:S(2)}, u32[]{:S(2)}) %collective-permute-start) | collective-permute-done | bytes 131104 | tf_op jit(solution)/shard_map/ppermute | solution.py:51
  192.7 0.7 copy-done.7
  193.3 7.9 %attention.1 = bf16[256,2048]{1,0:T(8,128)(2,1)} custom-call(s32[1]{0:T(128)} %bitcast.first_ref, f32[16]{0:T(128)} %sink_ref.1, bf16[256,1024]{1,0:T(8,128)(2,1)} %q_ref.1, bf16[256,256]{1,0:T(8,128)(2,1)} %k_ref.1, bf16[256,256]{1,0:T(8,128)(2,1)} %v_ref.1, bf16[2,128,256]{2,1,0:T(8,128)(2,1)} %copy-done.7, bf16[1024,2048]{1,0:T(8,128)(2,1)} %weight_ref.1, ...), custom_call_target="tpu_custom_call" | custom-call | flops 1610612736 | bytes 6291456 | tf_op jit(solution)/shard_map/attention/pallas_call | solution.py:398
  201.3 6.7 %shared_expert.1.shared_ref = f32[128,2048]{1,0:T(8,128)} custom-call(s32[1]{0:T(128)} %bitcast.22.core_ref, bf16[128,2048]{1,0:T(8,128)(2,1)} %get-tuple-element.5.x_ref, bf16[3072,128]{1,0:T(8,128)(2,1)} %shared_prep.1.refs_0_, bf16[3072,128]{1,0:T(8,128)(2,1)} %copy-done.4, bf16[3072,128]{1,0:T(8,128)(2,1)} %collective-permute-done.9.refs_2_, ...), custom_call_target="tpu_custom_call" | custom-call | flops 805306368 | bytes 6291456 | tf_op jit(solution)/shard_map/shared_expert/pallas_call | solution.py:281
  208.0 1.3 copy-done.1
  209.3 4.4 %combine.1 = bf16[128,2048]{1,0:T(8,128)(2,1)} custom-call(bf16[1024,1024]{1,0:T(8,128)(2,1)} %bitcast.35, s32[2,128]{1,0:T(2,128)} %bitcast.43, f32[2,128]{1,0:T(2,128)} %bitcast.44, f32[128,2048]{1,0:T(8,128)} %shared_expert.1.shared_ref, f32[1,2048]{1,0:T(1,128)} %bitcast.41), custom_call_target="tpu_custom_call" | custom-call | flops 1073741824 | bytes 2097152 | tf_op jit(solution)/shard_map/combine/pallas_call | solution.py:328
  (29 shorter events, 0.4 us)
Async XLA Ops:
  0.6 1.9 copy-start.3
  0.6 2.3 %copy-start.2 = (bf16[2,2048,192]{1,2,0:T(8,128)(2,1)S(1)}, bf16[2,2048,192]{1,2,0:T(8,128)(2,1)}, u32[]{:S(2)}) copy-start(bf16[2,2048,192]{1,2,0:T(8,128)(2,1)} %param.28) | copy-start | bytes 4718596
  4.9 78.3 %collective-permute-start.1 = (bf16[576,2048]{1,0:T(8,128)(2,1)}, bf16[576,2048]{1,0:T(8,128)(2,1)}, u32[]{:S(2)}, u32[]{:S(2)}) collective-permute-start(bf16[576,2048]{1,0:T(8,128)(2,1)} %pad_maximum_fusion.1), channel_id=1, source_target_pairs={{3,0},{0,1},{5,6},{6,7},{11,8},{8,9},{13,14},{14,15},{19,16},{16,1... | collective-permute-start | bytes 7077896 | tf_op jit(solution)/shard_map/ppermute | solution.py:460
  8.3 77.7 %collective-permute-start.3 = (bf16[576,2048]{1,0:T(8,128)(2,1)}, bf16[576,2048]{1,0:T(8,128)(2,1)}, u32[]{:S(2)}, u32[]{:S(2)}) collective-permute-start(bf16[576,2048]{1,0:T(8,128)(2,1)} %pad_maximum_fusion.1), channel_id=1, source_target_pairs={{1,0},{2,1},{7,6},{4,7},{9,8},{10,9},{15,14},{12,15},{17,16},{18,1... | collective-permute-start | bytes 7077896 | tf_op jit(solution)/shard_map/ppermute | solution.py:460
  9.7 25.6 %copy-start = (bf16[576,2048]{1,0:T(8,128)(2,1)}, bf16[576,2048]{1,0:T(8,128)(2,1)S(1)}, u32[]{:S(2)}) copy-start(bf16[576,2048]{1,0:T(8,128)(2,1)S(1)} %pad_maximum_fusion.refs_0_) | copy-start | bytes 7077892
  9.8 78.9 %collective-permute-start.2 = (bf16[576,2048]{1,0:T(8,128)(2,1)S(1)}, bf16[576,2048]{1,0:T(8,128)(2,1)}, u32[]{:S(2)}, u32[]{:S(2)}) collective-permute-start(bf16[576,2048]{1,0:T(8,128)(2,1)S(1)} %pad_maximum_fusion.refs_0_), channel_id=1, source_target_pairs={{2,0},{3,1},{4,6},{5,7},{10,8},{11,9},{12,14},{13,15},{18,16},{19,... | collective-permute-start | bytes 7077896 | tf_op jit(solution)/shard_map/ppermute | solution.py:460
  15.2 76.1 %all-to-all-start = ((bf16[128,8,1024]{2,1,0:T(8,128)(2,1)}), bf16[128,8,1024]{2,1,0:T(8,128)(2,1)}, u32[]{:S(2)}, u32[]{:S(2)}) async-start(bf16[128,8,1024]{2,1,0:T(8,128)(2,1)} %bitcast.36), calls=%async_computation | async-start | bytes 4194304 | tf_op jit(solution)/shard_map/all_to_all | solution.py:473
  35.3 56.0 %collective-permute-start.4 = (bf16[576,2048]{1,0:T(8,128)(2,1)S(1)}, bf16[576,2048]{1,0:T(8,128)(2,1)}, u32[]{:S(2)}, u32[]{:S(2)}) collective-permute-start(bf16[576,2048]{1,0:T(8,128)(2,1)S(1)} %pad_maximum_fusion.refs_0_), channel_id=1, source_target_pairs={{0,4},{1,5},{6,2},{7,3},{8,12},{9,13},{14,10},{15,11},{16,20},{17,... | collective-permute-start | bytes 7077896 | tf_op jit(solution)/shard_map/ppermute | solution.py:463
  83.2 8.1 %collective-permute-start.5 = (bf16[576,2048]{1,0:T(8,128)(2,1)}, bf16[576,2048]{1,0:T(8,128)(2,1)}, u32[]{:S(2)}, u32[]{:S(2)}) collective-permute-start(bf16[576,2048]{1,0:T(8,128)(2,1)} %collective-permute-done.1.refs_1_), channel_id=1, source_target_pairs={{0,4},{1,5},{6,2},{7,3},{8,12},{9,13},{14,10},{15,11},{16,20},{17,... | collective-permute-start | bytes 7077896 | tf_op jit(solution)/shard_map/ppermute | solution.py:463
  85.9 6.4 %collective-permute-start.7 = (bf16[576,2048]{1,0:T(8,128)(2,1)}, bf16[576,2048]{1,0:T(8,128)(2,1)}, u32[]{:S(2)}, u32[]{:S(2)}) collective-permute-start(bf16[576,2048]{1,0:T(8,128)(2,1)} %collective-permute-done.3.refs_3_), channel_id=1, source_target_pairs={{0,4},{1,5},{6,2},{7,3},{8,12},{9,13},{14,10},{15,11},{16,20},{17,... | collective-permute-start | bytes 7077896 | tf_op jit(solution)/shard_map/ppermute | solution.py:463
  88.6 7.1 %collective-permute-start.6 = (bf16[576,2048]{1,0:T(8,128)(2,1)}, bf16[576,2048]{1,0:T(8,128)(2,1)}, u32[]{:S(2)}, u32[]{:S(2)}) collective-permute-start(bf16[576,2048]{1,0:T(8,128)(2,1)} %collective-permute-done.2.refs_2_), channel_id=1, source_target_pairs={{0,4},{1,5},{6,2},{7,3},{8,12},{9,13},{14,10},{15,11},{16,20},{17,... | collective-permute-start | bytes 7077896 | tf_op jit(solution)/shard_map/ppermute | solution.py:463
  109.9 73.0 %copy-start.5 = (bf16[256,256]{1,0:T(8,128)(2,1)S(1)}, bf16[256,256]{1,0:T(8,128)(2,1)}, u32[]{:S(2)}) copy-start(bf16[256,256]{1,0:T(8,128)(2,1)} %k_ref.1) | copy-start | bytes 393220
  110.0 73.0 %copy-start.6 = (bf16[256,256]{1,0:T(8,128)(2,1)S(1)}, bf16[256,256]{1,0:T(8,128)(2,1)}, u32[]{:S(2)}) copy-start(bf16[256,256]{1,0:T(8,128)(2,1)} %v_ref.1) | copy-start | bytes 393220
  110.0 98.0 %all-to-all-start.1 = ((bf16[128,8,1024]{2,1,0:T(8,128)(2,1)}), bf16[128,8,1024]{2,1,0:T(8,128)(2,1)S(1)}, u32[]{:S(2)}, u32[]{:S(2)}) async-start(bf16[128,8,1024]{2,1,0:T(8,128)(2,1)} %bitcast.34), calls=%async_computation.1 | async-start | bytes 4194304 | tf_op jit(solution)/shard_map/all_to_all | solution.py:489
  125.6 34.5 %collective-permute-start.8 = (bf16[3072,128]{1,0:T(8,128)(2,1)}, bf16[3072,128]{1,0:T(8,128)(2,1)S(1)}, u32[]{:S(2)}, u32[]{:S(2)}) collective-permute-start(bf16[3072,128]{1,0:T(8,128)(2,1)} %shared_prep.1.refs_0_), channel_id=1, source_target_pairs={{0,1},{1,2},{2,3},{3,0},{4,5},{5,6},{6,7},{7,4},{8,9},{9,10},{10,1... | collective-permute-start | bytes 2359304 | tf_op jit(solution)/shard_map/ppermute | solution.py:501
  127.1 55.3 %collective-permute-start.9 = (bf16[3072,128]{1,0:T(8,128)(2,1)}, bf16[3072,128]{1,0:T(8,128)(2,1)}, u32[]{:S(2)}, u32[]{:S(2)}) collective-permute-start(bf16[3072,128]{1,0:T(8,128)(2,1)} %shared_prep.1.refs_0_), channel_id=1, source_target_pairs={{0,2},{1,3},{2,0},{3,1},{4,6},{5,7},{6,4},{7,5},{8,10},{9,11},{10,... | collective-permute-start | bytes 2359304 | tf_op jit(solution)/shard_map/ppermute | solution.py:501
  129.8 52.6 %collective-permute-start.10 = (bf16[3072,128]{1,0:T(8,128)(2,1)}, bf16[3072,128]{1,0:T(8,128)(2,1)}, u32[]{:S(2)}, u32[]{:S(2)}) collective-permute-start(bf16[3072,128]{1,0:T(8,128)(2,1)} %shared_prep.1.refs_0_), channel_id=1, source_target_pairs={{0,3},{1,0},{2,1},{3,2},{4,7},{5,4},{6,5},{7,6},{8,11},{9,8},{10,9... | collective-permute-start | bytes 2359304 | tf_op jit(solution)/shard_map/ppermute | solution.py:501
  131.2 70.0 %collective-permute-start.11 = (bf16[3072,128]{1,0:T(8,128)(2,1)}, bf16[3072,128]{1,0:T(8,128)(2,1)}, u32[]{:S(2)}, u32[]{:S(2)}) collective-permute-start(bf16[3072,128]{1,0:T(8,128)(2,1)} %shared_prep.1.refs_0_), channel_id=1, source_target_pairs={{0,4},{4,0},{1,5},{5,1},{2,6},{6,2},{3,7},{7,3},{8,12},{12,8},{9,1... | collective-permute-start | bytes 2359304 | tf_op jit(solution)/shard_map/ppermute | solution.py:502
  160.2 41.1 %copy-start.4 = (bf16[3072,128]{1,0:T(8,128)(2,1)}, bf16[3072,128]{1,0:T(8,128)(2,1)S(1)}, u32[]{:S(2)}) copy-start(bf16[3072,128]{1,0:T(8,128)(2,1)S(1)} %collective-permute-done.8.refs_1_) | copy-start | bytes 2359300
  160.2 41.1 %collective-permute-start.12 = (bf16[3072,128]{1,0:T(8,128)(2,1)S(1)}, bf16[3072,128]{1,0:T(8,128)(2,1)}, u32[]{:S(2)}, u32[]{:S(2)}) collective-permute-start(bf16[3072,128]{1,0:T(8,128)(2,1)S(1)} %collective-permute-done.8.refs_1_), channel_id=1, source_target_pairs={{0,4},{4,0},{1,5},{5,1},{2,6},{6,2},{3,7},{7,3},{8,12},{12,8},{9,1... | collective-permute-start | bytes 2359304 | tf_op jit(solution)/shard_map/ppermute | solution.py:502
  182.4 18.9 %collective-permute-start.13 = (bf16[3072,128]{1,0:T(8,128)(2,1)}, bf16[3072,128]{1,0:T(8,128)(2,1)}, u32[]{:S(2)}, u32[]{:S(2)}) collective-permute-start(bf16[3072,128]{1,0:T(8,128)(2,1)} %collective-permute-done.9.refs_2_), channel_id=1, source_target_pairs={{0,4},{4,0},{1,5},{5,1},{2,6},{6,2},{3,7},{7,3},{8,12},{12,8},{9,1... | collective-permute-start | bytes 2359304 | tf_op jit(solution)/shard_map/ppermute | solution.py:502
  182.4 18.9 %collective-permute-start.14 = (bf16[3072,128]{1,0:T(8,128)(2,1)}, bf16[3072,128]{1,0:T(8,128)(2,1)}, u32[]{:S(2)}, u32[]{:S(2)}) collective-permute-start(bf16[3072,128]{1,0:T(8,128)(2,1)} %collective-permute-done.10.refs_3_), channel_id=1, source_target_pairs={{0,4},{4,0},{1,5},{5,1},{2,6},{6,2},{3,7},{7,3},{8,12},{12,8},{9,1... | collective-permute-start | bytes 2359304 | tf_op jit(solution)/shard_map/ppermute | solution.py:502
  182.9 9.7 %collective-permute-start = (bf16[2,128,256]{2,1,0:T(8,128)(2,1)S(1)}, bf16[2,128,256]{2,1,0:T(8,128)(2,1)S(1)}, u32[]{:S(2)}, u32[]{:S(2)}) collective-permute-start(bf16[2,128,256]{2,1,0:T(8,128)(2,1)S(1)} %pad_maximum_fusion.2), channel_id=1, source_target_pairs={{0,1},{1,2},{2,3},{3,4},{4,5},{5,6},{6,7},{7,8},{8,9},{9,10},{10,1... | collective-permute-start | bytes 393224 | tf_op jit(solution)/shard_map/ppermute | solution.py:51
  192.7 0.7 copy-start.7
  208.0 1.3 copy-start.1

commit v2 on v1

--- a/solution.py
+++ b/solution.py
@@ -15,6 +15,11 @@
 WINDOW = 128
 CAP = 4
 BLOCK = 256
+MIB = 1 << 20
+PARTS = 4
+COMBINE_LIMIT = 16
+UP_LIMIT = 24
+DOWN_LIMIT = 16
 EP = ("z", "y", "c")
 EP_TP = ("z", "y", "c", "tp")
 CHIPS = ("z", "y", "tp")
@@ -130,33 +135,73 @@
     )(x, gain, ids)
 
 
-def expert_kernel(own_ref, recv, *refs):
+def pick_kernel(parity_ref, *refs):
+    arrays, outs, held, sems = refs[:-4], refs[-4:-2], refs[-2], refs[-1]
+    rows = arrays[0].shape[1]
+    steps = []
+    for p, out in enumerate(outs):
+        j = lax.rem(parity_ref[0] + p, 2)
+        for m, array in enumerate(arrays):
+            at = pl.ds(m * rows, rows)
+            steps.append(
+                (
+                    pltpu.make_async_copy(array.at[j], held.at[p, at], sems.at[0, p, m]),
+                    pltpu.make_async_copy(held.at[p, at], out.at[at], sems.at[1, p, m]),
+                )
+            )
+    for c, _ in steps:
+        c.start()
+    for c, d in steps:
+        c.wait()
+        d.start()
+    for _, d in steps:
+        d.wait()
+
+
+def pick(parity, arrays, limit):
+    rows, width = arrays[0].shape[1:]
+    count = len(arrays)
+    return pl.pallas_call(
+        pick_kernel,
+        in_specs=[pl.BlockSpec(memory_space=pltpu.SMEM)] + [pl.BlockSpec(memory_space=ANY)] * count,
+        out_specs=[pl.BlockSpec(memory_space=ANY)] * 2,
+        out_shape=[jax.ShapeDtypeStruct((count * rows, width), bf16)] * 2,
+        scratch_shapes=[
+            VMEM((2, count * rows, width), bf16),
+            pltpu.SemaphoreType.DMA((2, 2, count)),
+        ],
+        compiler_params=pltpu.CompilerParams(vmem_limit_bytes=limit * MIB),
+        cost_estimate=pl.CostEstimate(
+            flops=1000, bytes_accessed=8 * count * rows * width, transcendentals=0
+        ),
+        name="pick",
+    )(parity, *arrays)
+
+
+def start_pieces(own_ref, own, other, copy, parts):
+    for mine, pieces in ((1, own), (0, other)):
+
+        @pl.when(own_ref[0] == mine)
+        def _():
+            for m in range(parts):
+                for k, piece in enumerate(pieces):
+                    copy(k, m, piece).start()
+
+
+def up_kernel(own_ref, recv, *refs):
     own, other = refs[:4], refs[4:8]
-    out_ref, arrived, gate, up, down, rows, hidden, sem, sems = refs[8:]
-    part = own[0].shape[0] // 3
+    hidden_ref, arrived, gate, up, rows, sem, sems = refs[8:]
+    part = own[0].shape[0] // 2
     half = recv.shape[1]
-    groups = recv.shape[0] // BLOCK
-
-    def fill(k, m, piece):
-        into = (gate, up, down)[m]
+
+    def copy(k, m, piece):
         return pltpu.make_async_copy(
-            piece.at[pl.ds(m * part, part)], into.at[pl.ds(k * part, part)], sems.at[m, k]
+            piece.at[pl.ds(m * part, part)], (gate, up)[m].at[pl.ds(k * part, part)], sems.at[m, k]
         )
 
     rows_in = pltpu.make_async_copy(recv, arrived, sem)
     rows_in.start()
-    for mine, pieces in ((1, own), (0, other)):
-
-        @pl.when(own_ref[0] == mine)
-        def _():
-            for m in range(3):
-                for k, piece in enumerate(pieces):
-                    fill(k, m, piece).start()
-
-    def wait(m):
-        for k in range(4):
-            fill(k, m, own[k]).wait()
-
+    start_pieces(own_ref, own, other, copy, 2)
     a, b = iota((BLOCK // 2, BLOCK), 0), iota((BLOCK // 2, BLOCK), 1)
     first = (a // CAP) * (2 * CAP) + a % CAP
     picks = [jnp.where(b == first + h * CAP, 1.0, 0.0).astype(bf16) for h in range(2)]
@@ -169,152 +214,234 @@
             rows[at, h * half : (h + 1) * half] = dot(picks[h], block).astype(bf16)
         return carry
 
-    lax.fori_loop(0, groups, sort_rows, 0)
-    wait(0)
-    wait(1)
+    lax.fori_loop(0, recv.shape[0] // BLOCK, sort_rows, 0)
+    for m in range(2):
+        for k in range(4):
+            copy(k, m, own[k]).wait()
 
     def units(n, carry):
         at = pl.ds(pl.multiple_of(n * BLOCK, BLOCK), BLOCK)
         x = rows[...]
         g = dot_t(x, gate[at, :])
         u = dot_t(x, up[at, :])
-        hidden[:, at] = (g / (1.0 + jnp.exp(-g)) * u).astype(bf16)
+        hidden_ref[:, at] = (g / (1.0 + jnp.exp(-g)) * u).astype(bf16)
         return carry
 
-    lax.fori_loop(0, hidden.shape[1] // BLOCK, units, 0)
-    wait(2)
-    a, b = iota((BLOCK, BLOCK), 0), iota((BLOCK, BLOCK), 1)
-    b, h = b % (BLOCK // 2), b // (BLOCK // 2)
-    back = jnp.where(a == (b // CAP) * (2 * CAP) + b % CAP + h * CAP, 1.0, 0.0).astype(bf16)
-
-    def columns(n, carry):
-        at = pl.multiple_of(n * BLOCK, BLOCK)
-        x = hidden[...]
-        left = dot(x, down[:, pl.ds(at, BLOCK)]).astype(bf16)
-        right = dot(x, down[:, pl.ds(half + at, BLOCK)]).astype(bf16)
-        for i in range(groups):
-            mine = slice(i * (BLOCK // 2), (i + 1) * (BLOCK // 2))
-            both = jnp.concatenate([left[mine], right[mine]], axis=0)
-            out_ref[i * BLOCK : (i + 1) * BLOCK, pl.ds(at, BLOCK)] = dot(back, both).astype(bf16)
-        return carry
-
-    lax.fori_loop(0, half // BLOCK, columns, 0)
-
-
-def expert(own, recv, mine, others):
+    lax.fori_loop(0, hidden_ref.shape[1] // BLOCK, units, 0)
+
+
+def expert_up(own, recv, mine, others):
     total, half = recv.shape
-    units = 4 * mine[0].shape[0] // 3
-    return pl.pallas_call(
-        expert_kernel,
+    units = 2 * mine[0].shape[0]
+    return pl.pallas_call(
+        up_kernel,
         in_specs=[pl.BlockSpec(memory_space=pltpu.SMEM)] + [pl.BlockSpec(memory_space=ANY)] * 9,
         out_specs=pl.BlockSpec(memory_space=VMEM),
-        out_shape=jax.ShapeDtypeStruct((total, half), bf16),
+        out_shape=jax.ShapeDtypeStruct((total // 2, units), bf16),
         scratch_shapes=[
             VMEM((total, half), bf16),
             VMEM((units, 2 * half), bf16),
             VMEM((units, 2 * half), bf16),
-            VMEM((units, 2 * half), bf16),
             VMEM((total // 2, 2 * half), bf16),
-            VMEM((total // 2, units), bf16),
             pltpu.SemaphoreType.DMA,
-            pltpu.SemaphoreType.DMA((3, 4)),
-        ],
+            pltpu.SemaphoreType.DMA((2, 4)),
+        ],
+        compiler_params=pltpu.CompilerParams(vmem_limit_bytes=UP_LIMIT * MIB),
         cost_estimate=pl.CostEstimate(
-            flops=6 * total * half * units,
-            bytes_accessed=4 * total * half + 12 * half * units,
+            flops=4 * total * half * units,
+            bytes_accessed=2 * total * half + 8 * half * units,
             transcendentals=total * units // 2,
         ),
-        name="expert",
+        name="expert_up",
     )(own, recv, *mine, *others)
 
 
-def shared_prep_kernel(core_ref, gate_ref, up_ref, down_ref, out_ref):
-    depth = gate_ref.shape[0] // 2
+def down_kernel(own_ref, hidden, *refs):
+    own, other = refs[:4], refs[4:8]
+    out_ref, down, made, sems, out_sems = refs[8:]
+    part = own[0].shape[0]
+    half = out_ref.shape[1]
+    groups = out_ref.shape[0] // BLOCK
+    count = half // BLOCK
+
+    def copies(n, pieces):
+        return [
+            pltpu.make_async_copy(
+                piece.at[:, pl.ds(h * half + n * BLOCK, BLOCK)],
+                down.at[pl.ds(k * part, part), pl.ds(h * half + n * BLOCK, BLOCK)],
+                sems.at[n, h, k],
+            )
+            for h in range(2)
+            for k, piece in enumerate(pieces)
+        ]
+
+    for mine, pieces in ((1, own), (0, other)):
+
+        @pl.when(own_ref[0] == mine)
+        def _():
+            for n in range(count):
+                for c in copies(n, pieces):
+                    c.start()
+
+    a, b = iota((BLOCK, BLOCK), 0), iota((BLOCK, BLOCK), 1)
+    b, h = b % (BLOCK // 2), b // (BLOCK // 2)
+    back = jnp.where(a == (b // CAP) * (2 * CAP) + b % CAP + h * CAP, 1.0, 0.0).astype(bf16)
+    for n in range(count):
+        for c in copies(n, own):
+            c.wait()
+        at = n * BLOCK
+        x = hidden[...]
+        left = dot(x, down[:, at : at + BLOCK]).astype(bf16)
+        right = dot(x, down[:, half + at : half + at + BLOCK]).astype(bf16)
+        for i in range(groups):
+            mine = slice(i * (BLOCK // 2), (i + 1) * (BLOCK // 2))
+            both = jnp.concatenate([left[mine], right[mine]], axis=0)
+            made[i * BLOCK : (i + 1) * BLOCK, at : at + BLOCK] = dot(back, both).astype(bf16)
+        columns = pl.ds(at, BLOCK)
+        pltpu.make_async_copy(made.at[:, columns], out_ref.at[:, columns], out_sems.at[n]).start()
+    for n in range(count):
+        columns = pl.ds(n * BLOCK, BLOCK)
+        pltpu.make_async_copy(made.at[:, columns], out_ref.at[:, columns], out_sems.at[n]).wait()
+
+
+def expert_down(own, hidden, mine, others):
+    rows, units = hidden.shape
+    width = mine[0].shape[1]
+    count = width // 2 // BLOCK
+    return pl.pallas_call(
+        down_kernel,
+        in_specs=[pl.BlockSpec(memory_space=pltpu.SMEM)]
+        + in_vmem(1)
+        + [pl.BlockSpec(memory_space=ANY)] * 8,
+        out_specs=pl.BlockSpec(memory_space=ANY),
+        out_shape=jax.ShapeDtypeStruct((2 * rows, width // 2), bf16),
+        scratch_shapes=[
+            VMEM((units, width), bf16),
+            VMEM((2 * rows, width // 2), bf16),
+            pltpu.SemaphoreType.DMA((count, 2, 4)),
+            pltpu.SemaphoreType.DMA((count,)),
+        ],
+        compiler_params=pltpu.CompilerParams(vmem_limit_bytes=DOWN_LIMIT * MIB),
+        cost_estimate=pl.CostEstimate(
+            flops=2 * rows * units * width,
+            bytes_accessed=2 * (rows * (units + width) + units * width),
+            transcendentals=0,
+        ),
+        name="expert_down",
+    )(own, hidden, *mine, *others)
+
+
+def shared_prep_kernel(part_ref, gate_ref, up_ref, down_ref, out_ref):
+    depth = gate_ref.shape[0] // PARTS
     units = gate_ref.shape[1]
-    core = core_ref[0]
-    at = pl.ds(pl.multiple_of(core * depth, depth), depth)
+    first = pl.multiple_of(part_ref[0] * depth, depth)
+    at = pl.ds(first, depth)
     out_ref[:depth, :] = gate_ref[at, :]
     out_ref[depth : 2 * depth, :] = up_ref[at, :]
     for t in range(depth // 128):
-        lane = pl.multiple_of(core * depth + t * 128, 128)
+        lane = pl.multiple_of(first + t * 128, 128)
         out_ref[2 * depth + t * units : 2 * depth + (t + 1) * units, :] = down_ref[
             :, pl.ds(lane, 128)
         ]
 
 
-def shared_prep(core, gate, up, down):
+def shared_prep(part, gate, up, down):
     return pl.pallas_call(
         shared_prep_kernel,
         in_specs=[pl.BlockSpec(memory_space=pltpu.SMEM)] + in_vmem(3),
         out_specs=pl.BlockSpec(memory_space=VMEM),
-        out_shape=jax.ShapeDtypeStruct((gate.shape[0] // 2 * 3, gate.shape[1]), bf16),
-        cost_estimate=pl.CostEstimate(flops=1000, bytes_accessed=12 * gate.size, transcendentals=0),
+        out_shape=jax.ShapeDtypeStruct((gate.shape[0] // PARTS * 3, gate.shape[1]), bf16),
+        compiler_params=pltpu.CompilerParams(vmem_limit_bytes=8 * MIB),
+        cost_estimate=pl.CostEstimate(flops=1000, bytes_accessed=8 * gate.size, transcendentals=0),
         name="shared_prep",
-    )(core, gate, up, down)
-
-
-def shared_kernel(core_ref, x_ref, *refs):
-    mine, theirs = refs[:4], refs[4:8]
-    out_ref, into, down = refs[8:]
-    depth = x_ref.shape[1] // 2
-    units = mine[0].shape[1]
-    core = core_ref[0]
-    for side, pieces in ((core, mine), (1 - core, theirs)):
-        top = pl.multiple_of(side * depth, depth)
-        for k, piece in enumerate(pieces):
+    )(part, gate, up, down)
+
+
+def slot_columns(ids, weights):
+    tokens = ids.shape[1]
+    first = slot_rows(ids.astype(f32), False)
+    eye = iota((tokens, tokens), 0) == iota((tokens, tokens), 1)
+    lane = iota((tokens, 128), 1)
+    out = jnp.zeros((tokens, 128), f32)
+    for k in range(2):
+        weight = jnp.sum(jnp.where(eye, weights[k : k + 1, :], 0.0), axis=1, keepdims=True)
+        out = jnp.where(lane == k, first[k].astype(f32), out)
+        out = jnp.where(lane == 2 + k, weight, out)
+    return out
+
+
+def shared_kernel(part_ref, ids_ref, weight_ref, x_ref, *refs):
+    parts, (out_ref, columns_ref, into, down) = refs[:PARTS], refs[PARTS:]
+    depth = x_ref.shape[1] // PARTS
+    units = parts[0].shape[1]
+    for p, ref in enumerate(parts):
+        first = pl.multiple_of(part_ref[p] * depth, depth)
+        for k in range(4):
+            base = 3 * k * depth
             for m in range(2):
                 lane = (m * 4 + k) * units
-                into[pl.ds(top, depth), lane : lane + units] = piece[m * depth : (m + 1) * depth, :]
+                into[pl.ds(first, depth), lane : lane + units] = ref[
+                    base + m * depth : base + (m + 1) * depth, :
+                ]
             for t in range(depth // 128):
-                lane = pl.multiple_of(side * depth + t * 128, 128)
-                at = 2 * depth + t * units
-                down[k * units : (k + 1) * units, pl.ds(lane, 128)] = piece[at : at + units, :]
+                lane = pl.multiple_of(first + t * 128, 128)
+                at = base + 2 * depth + t * units
+                down[k * units : (k + 1) * units, pl.ds(lane, 128)] = ref[at : at + units, :]
     both = dot(x_ref[...], into[...])
     g, u = both[:, : 4 * units], both[:, 4 * units :]
     hidden = (g / (1.0 + jnp.exp(-g)) * u).astype(bf16)
     out_ref[...] = dot(hidden, down[...])
-
-
-def shared_expert(core, normed, mine, theirs):
+    columns_ref[...] = slot_columns(ids_ref[...], weight_ref[...])
+
+
+def shared_expert(part, ids, weights, normed, parts):
     tokens, width = normed.shape
-    units = 4 * mine[0].shape[1]
+    units = 4 * parts[0].shape[1]
     return pl.pallas_call(
         shared_kernel,
-        in_specs=[pl.BlockSpec(memory_space=pltpu.SMEM)] + in_vmem(9),
-        out_specs=pl.BlockSpec(memory_space=VMEM),
-        out_shape=jax.ShapeDtypeStruct((tokens, width), f32),
+        in_specs=[pl.BlockSpec(memory_space=pltpu.SMEM)] + in_vmem(3 + PARTS),
+        out_specs=[pl.BlockSpec(memory_space=VMEM)] * 2,
+        out_shape=[
+            jax.ShapeDtypeStruct((tokens, width), f32),
+            jax.ShapeDtypeStruct((tokens, 128), f32),
+        ],
         scratch_shapes=[VMEM((width, 2 * units), bf16), VMEM((units, width), bf16)],
+        compiler_params=pltpu.CompilerParams(vmem_limit_bytes=24 * MIB),
         cost_estimate=pl.CostEstimate(
             flops=6 * tokens * width * units,
             bytes_accessed=6 * width * units,
             transcendentals=tokens * units,
         ),
         name="shared_expert",
-    )(core, normed, *mine, *theirs)
-
-
-def combine_kernel(back_ref, ids_ref, weight_ref, shared_ref, gain_ref, out_ref):
-    tokens = out_ref.shape[0]
-    slots, half = back_ref.shape
-    first = slot_rows(ids_ref[...].astype(f32), False)
-    eye = iota((tokens, tokens), 0) == iota((tokens, tokens), 1)
-    weights = [
-        jnp.sum(jnp.where(eye, weight_ref[k : k + 1, :], 0.0), axis=1, keepdims=True)
-        for k in range(2)
-    ]
-    r = iota((tokens, slots), 1)
-    back = back_ref[...]
-    halves = []
+    )(part, ids, weights, normed, *parts)
+
+
+def combine_kernel(back_ref, shared_ref, columns_ref, gain_ref, out_ref, came, common, sems):
+    tokens, half = out_ref.shape[0], back_ref.shape[1]
+    back_in = pltpu.make_async_copy(back_ref, came, sems.at[0])
+    shared_in = pltpu.make_async_copy(shared_ref, common, sems.at[1])
+    back_in.start()
+    shared_in.start()
+    r = iota((tokens, back_ref.shape[0]), 1)
+    first = [columns_ref[:, k : k + 1].astype(jnp.int32) for k in range(2)]
+    weights = [columns_ref[:, 2 + k : 3 + k] for k in range(2)]
+    spreads = []
     for h in range(2):
         spread = jnp.where(r == first[0] + h * CAP, weights[0], 0.0) + jnp.where(
             r == first[1] + h * CAP, weights[1], 0.0
         )
         coarse = spread.astype(bf16)
         fine = (spread - coarse.astype(f32)).astype(bf16)
-        summed = dot(jnp.concatenate([coarse, fine], axis=0), back)
-        halves.append(
-            summed[:tokens] + summed[tokens:] + shared_ref[:, h * half : (h + 1) * half]
-        )
+        spreads += [coarse, fine]
+    back_in.wait()
+    summed = dot(jnp.concatenate(spreads, axis=0), came[...])
+    shared_in.wait()
+    halves = [
+        summed[2 * h * tokens : (2 * h + 1) * tokens]
+        + summed[(2 * h + 1) * tokens : (2 * h + 2) * tokens]
+        + common[:, h * half : (h + 1) * half]
+        for h in range(2)
+    ]
     square = sum(jnp.sum(v * v, axis=1, keepdims=True) for v in halves)
     scale = lax.rsqrt(square / (2 * half) + EPS)
     for h, v in enumerate(halves):
@@ -322,19 +449,25 @@
         out_ref[:, at] = (v * scale * gain_ref[:, at]).astype(bf16)
 
 
-def combine(back, ids, weights, shared, gain):
+def combine(back, shared, columns, gain):
     slots, half = back.shape
-    tokens = ids.shape[1]
+    tokens = shared.shape[0]
     return pl.pallas_call(
         combine_kernel,
-        in_specs=in_vmem(5),
+        in_specs=[pl.BlockSpec(memory_space=ANY)] * 2 + in_vmem(2),
         out_specs=pl.BlockSpec(memory_space=VMEM),
         out_shape=jax.ShapeDtypeStruct((tokens, 2 * half), bf16),
+        scratch_shapes=[
+            VMEM((slots, half), bf16),
+            VMEM((tokens, 2 * half), f32),
+            pltpu.SemaphoreType.DMA((2,)),
+        ],
+        compiler_params=pltpu.CompilerParams(vmem_limit_bytes=COMBINE_LIMIT * MIB),
         cost_estimate=pl.CostEstimate(
             flops=8 * tokens * slots * half, bytes_accessed=2 * slots * half, transcendentals=0
         ),
         name="combine",
-    )(back, ids, weights, shared, gain)
+    )(back, shared, columns, gain)
 
 
 def attention_kernel(
@@ -411,6 +544,7 @@
             bytes_accessed=2 * weight.size + 4 * tokens * wide,
             transcendentals=tokens * HEADS * 2 * WINDOW,
         ),
+        compiler_params=pltpu.CompilerParams(vmem_limit_bytes=24 * MIB),
         name="attention",
     )(first, sinks, queries, keys, values, rim, weight, gain)
 
@@ -436,13 +570,13 @@
 ):
     x, core = lax.axis_index("tp"), lax.axis_index("c")
     tp = lax.axis_size("tp")
-    homes = [(i // 2, i) for i in range(tp)]
-    to_home = {
-        k: [(c * tp + (i - k) % tp, c * tp + i) for c, i in homes] for k in range(1, tp)
-    }
-    to_other = [(c * tp + i, (1 - c) * tp + i) for c, i in homes]
+    near, far = [], []
+    for i in range(tp):
+        c = i // 2
+        near += [(c * tp + (i - 1) % tp, c * tp + i), (c * tp + (i + 1) % tp, (1 - c) * tp + i)]
+        far += [(c * tp + (i + 2) % tp, c * tp + i), (c * tp + i, (1 - c) * tp + i)]
+    swapped = [(i, (i + tp) % (2 * tp)) for i in range(2 * tp)]
     own = (core == x // 2).astype(jnp.int32).reshape(1)
-    core_at = core.astype(jnp.int32).reshape(1)
 
     kv_rows = jnp.stack([att_keys, att_values])
     rim_rows = from_behind(kv_rows[:, att_keys.shape[0] - WINDOW :], EP_TP, 1)
@@ -450,22 +584,21 @@
 
     gate_t, up_t = w_gate.transpose(0, 2, 1), w_up.transpose(0, 2, 1)
 
-    def expert_of(parity, arrays):
-        j = (x + parity) % 2
-        return jnp.concatenate(
-            [lax.dynamic_index_in_dim(a, j, 0, keepdims=False) for a in arrays], axis=0
+    parity = (x % 2).astype(jnp.int32).reshape(1)
+
+    def moved(piece, route):
+        return lax.ppermute(piece, CORE_TP, route)
+
+    def gathered(came_near, came_far, other_near, other_far):
+        return (other_far, came_near, came_far, other_near), (
+            came_far,
+            other_near,
+            other_far,
+            came_near,
         )
 
-    def homeward(k, piece):
-        return lax.ppermute(piece, CORE_TP, to_home[k])
-
-    def across(pieces):
-        return [lax.ppermute(v, CORE_TP, to_other) for v in pieces]
-
-    pieces = {p: expert_of(p, (gate_t, up_t, w_down)) for p in (1, 0)}
-    mine = [pieces[0]] + [homeward(k, pieces[k % 2]) for k in (1, 3, 2)]
-    mine[2], mine[3] = mine[3], mine[2]
-    others = across(mine)
+    even, odd = pick(parity, (gate_t, up_t), 63)
+    near_in, far_in = moved(odd, near), moved(even, far)
 
     ids_t = expert_ids.T
     packed, normed = pack(moe_in, pre_gain.reshape(1, -1), ids_t, 128 * CAP)
@@ -473,6 +606,11 @@
     arrived = lax.all_to_all(
         packed.reshape(chips, 2 * CAP, -1), CHIPS, split_axis=0, concat_axis=0, tiled=True
     ).reshape(packed.shape)
+
+    even_out, odd_out = pick(parity, (w_down,), 8)
+    near_out, far_out = moved(odd_out, near), moved(even_out, far)
+    up_pieces = gathered(near_in, far_in, moved(near_in, swapped), moved(far_in, swapped))
+    down_pieces = gathered(near_out, far_out, moved(near_out, swapped), moved(far_out, swapped))
 
     mixer_out = attention(
         first,
@@ -485,13 +623,17 @@
         att_gain.reshape(1, -1),
     )
 
-    out = expert(own, arrived, mine, others)
+    hidden = expert_up(own, arrived, *up_pieces)
+    out = expert_down(own, hidden, *down_pieces)
     returned = lax.all_to_all(
         out.reshape(chips, 2 * CAP, -1), CHIPS, split_axis=0, concat_axis=0, tiled=True
     ).reshape(out.shape)
 
+    y, ys = lax.axis_index("y"), lax.axis_size("y")
+    part = jnp.stack([2 * c + v for c in (core, 1 - core) for v in (y % 2, 1 - y % 2)])
+    part = part.astype(jnp.int32)
     prepared = shared_prep(
-        core_at,
+        part,
         common_expert_gate_weight,
         common_expert_up_weight,
         common_expert_down_weight,
@@ -499,11 +641,16 @@
     blocks = [prepared]
     for k in range(1, tp):
         blocks.append(lax.ppermute(prepared, "tp", [(i, (i + k) % tp) for i in range(tp)]))
-    theirs = [lax.ppermute(v, "c", [(0, 1), (1, 0)]) for v in blocks]
-    shared_sum = shared_expert(core_at, normed, blocks, theirs)
-    experts_out = combine(
-        returned, ids_t, routed_expert_weight.T, shared_sum, moe_gain.reshape(1, -1)
+    quarters = [jnp.concatenate(blocks, axis=0)]
+    beside = [
+        (2 * i + c, 2 * ((i + 1 - 2 * ((i + c) % 2)) % ys) + c) for i in range(ys) for c in range(2)
+    ]
+    quarters.append(lax.ppermute(quarters[0], ("y", "c"), beside))
+    quarters += [lax.ppermute(v, "c", [(0, 1), (1, 0)]) for v in quarters]
+    shared_sum, columns = shared_expert(
+        part, ids_t, routed_expert_weight.T, normed, quarters
     )
+    experts_out = combine(returned, shared_sum, columns, moe_gain.reshape(1, -1))
     return (mixer_out, experts_out)
 
 

time: 215 us -> 210 us (0.977); the launches traced: 214 us -> 206 us
  starting transfers between devices: 58.4 us -> 39.2 us
  waiting for transfers between devices: 108 us -> 118 us
  local copies, waits for them, and re-layouts: 4.53 us -> 11.8 us
  Pallas kernels: 39.7 us -> 34.9 us
    ppermute x11, waiting for transfers between devices: 49.6 us -> 110 us  [the longest x8 76.6 us: moved(): return lax.ppermute(piece, CORE_TP, route)]
    ppermute x3, waiting for transfers between devices: 51.2 us -> 0.01 us  [body(): lax.ppermute(prepared, 'tp', [(i, (i + k) % tp) for i in range(tp)])]
    ppermute x11, starting transfers between devices: 17.3 us -> 3.75 us  [the longest x8 2.69 us: moved(): return lax.ppermute(piece, CORE_TP, route)]
    unnamed x16 -> x36, local copies, waits for them, and re-layouts: 2.62 us -> 11.8 us
    all_to_all x1, starting transfers between devices: 20.1 us -> 15.8 us  [body(): lax.all_to_all(packed.reshape(chips, 2 * CAP, -1), CHIPS, split_axis=0, c...]
    ppermute x3, starting transfers between devices: 5.6 us -> 3.07 us  [body(): lax.ppermute(prepared, 'tp', [(i, (i + k) % tp) for i in range(tp)])]
    pallas_call x2 -> x5, Pallas kernels: 18.6 us -> 19.5 us  [the longest x1 6.86 us: expert_up(): pl.pallas_call(up_kernel, in_specs=[pl.BlockSpec(memory_space=pltpu.SMEM)...]
  transfers between devices with their start and end apart: 17 -> 17, of which waited for: 6 -> 6; matrix products, arithmetic and copies ran while one was open for 0% -> 1% of each run, Pallas kernels for 10% -> 13%
where the time goes in v2:
time: 210 us; the launch traced here: 206 us
  waiting for transfers between devices  118 us (56%)
  starting transfers between devices  39.2 us (19%)
  Pallas kernels  34.9 us (17%)
  local copies, waits for them, and re-layouts  11.8 us (6%)
    ppermute x8, waiting for transfers between devices, moved(): return lax.ppermute(piece, CORE_TP, route)  76.6 us
    ppermute x1, waiting for transfers between devices, body(): quarters.append(lax.ppermute(quarters[0], ('y', 'c'), beside))  33.7 us
    all_to_all x1, starting transfers between devices, body(): lax.all_to_all(packed.reshape(chips, 2 * CAP, -1), CHIPS, split_axis=0, c...  15.8 us
    all_to_all x1, starting transfers between devices, body(): lax.all_to_all(out.reshape(chips, 2 * CAP, -1), CHIPS, split_axis=0, conc...  13.5 us
    unnamed x36, local copies, waits for them, and re-layouts  11.8 us
    ppermute x1, waiting for transfers between devices, from_behind(): return lax.ppermute(block, axis, route)  7.28 us
    pallas_call x1, Pallas kernels, expert_up(): pl.pallas_call(up_kernel, in_specs=[pl.BlockSpec(memory_space=pltpu.SMEM)...  6.86 us
    pallas_call x1, Pallas kernels, attention(): pl.pallas_call(attention_kernel, in_specs=[pl.BlockSpec(memory_space=pltp...  5.94 us
  transfers between devices with their start and end apart: 17, of which 6 were waited for; matrix products, arithmetic and copies ran while one was open for 1% of the time, Pallas kernels for 13%

profile of v2, /device:TPU:8, one launch (start us, length us, event | category | flops | bytes accessed | tf_op | source)
XLA Modules:
  0.0 206.1 jit_solution(7224639969705183249)
XLA Ops:
  0.6 4.1 %pack.1 = (bf16[1024,1024]{1,0:T(8,128)(2,1)}, bf16[128,2048]{1,0:T(8,128)(2,1)}) custom-call(bf16[128,2048]{1,0:T(8,128)(2,1)} %x_ref.1, f32[1,2048]{1,0:T(1,128)} %bitcast.30, s32[2,128]{1,0:T(2,128)} %bitcast.23), custom_call_target="tpu_custom_call" | custom-call | flops 536870912 | bytes 1572864 | tf_op jit(solution)/shard_map/pack/pallas_call | solution.py:114
  4.8 15.8 %all-to-all-start = ((bf16[128,8,1024]{2,1,0:T(8,128)(2,1)}), bf16[128,8,1024]{2,1,0:T(8,128)(2,1)}, u32[]{:S(2)}, u32[]{:S(2)}) async-start(bf16[128,8,1024]{2,1,0:T(8,128)(2,1)} %bitcast.27), calls=%async_computation | async-start | bytes 4194304 | tf_op jit(solution)/shard_map/all_to_all | solution.py:606
  20.6 2.8 %pick.2 = (bf16[384,2048]{1,0:T(8,128)(2,1)}, bf16[384,2048]{1,0:T(8,128)(2,1)}) custom-call(s32[1]{0:T(128)} %bitcast.9.parity_ref, bf16[2,192,2048]{2,1,0:T(8,128)(2,1)} %bitcast.28, bf16[2,192,2048]{2,1,0:T(8,128)(2,1)} %bitcast.29), custom_call_target="tpu_custom_call" | custom-call | flops 1000 | bytes 6291456 | tf_op jit(solution)/shard_map/pick/pallas_call | solution.py:164
  23.6 1.5 collective-permute-start.3
  25.1 55.1 %collective-permute-done.1.refs_2_.refs_4_ = bf16[384,2048]{1,0:T(8,128)(2,1)S(1)} collective-permute-done((bf16[384,2048]{1,0:T(8,128)(2,1)}, bf16[384,2048]{1,0:T(8,128)(2,1)S(1)}, u32[]{:S(2)}, u32[]{:S(2)}) %collective-permute-start.1) | collective-permute-done | bytes 1572896 | tf_op jit(solution)/shard_map/ppermute | solution.py:590
  80.7 1.4 copy-done.1
  82.4 0.4 collective-permute-start.5
  82.7 0.4 collective-permute-start.7
  83.2 19.2 %collective-permute-done.5.refs_2_.refs_4_ = bf16[192,2048]{1,0:T(8,128)(2,1)} collective-permute-done((bf16[192,2048]{1,0:T(8,128)(2,1)S(1)}, bf16[192,2048]{1,0:T(8,128)(2,1)}, u32[]{:S(2)}, u32[]{:S(2)}) %collective-permute-start.5) | collective-permute-done | bytes 786464 | tf_op jit(solution)/shard_map/ppermute | solution.py:590
  102.3 2.1 %collective-permute-done.7.refs_1_.refs_7_ = bf16[192,2048]{1,0:T(8,128)(2,1)} collective-permute-done((bf16[192,2048]{1,0:T(8,128)(2,1)S(1)}, bf16[192,2048]{1,0:T(8,128)(2,1)}, u32[]{:S(2)}, u32[]{:S(2)}) %collective-permute-start.7) | collective-permute-done | bytes 786464 | tf_op jit(solution)/shard_map/ppermute | solution.py:590
  104.5 1.0 copy-done.2
  105.6 1.0 copy-done.3
  106.6 1.0 copy-done.4
  107.6 0.6 shared_prep.1
  108.6 2.7 %collective-permute-start.10 = (bf16[1536,128]{1,0:T(8,128)(2,1)S(1)}, bf16[1536,128]{1,0:T(8,128)(2,1)}, u32[]{:S(2)}, u32[]{:S(2)}) collective-permute-start(bf16[1536,128]{1,0:T(8,128)(2,1)S(1)} %shared_prep.1), channel_id=1, source_target_pairs={{0,2},{1,3},{2,0},{3,1},{4,6},{5,7},{6,4},{7,5},{8,10},{9,11},{10,... | collective-permute-start | bytes 1179656 | tf_op jit(solution)/shard_map/ppermute | solution.py:643
  111.3 6.9 %expert_up.1.hidden = bf16[512,768]{1,0:T(8,128)(2,1)S(1)} custom-call(s32[1]{0:T(128)} %bitcast.4.own_ref, bf16[1024,1024]{1,0:T(8,128)(2,1)} %bitcast.8.recv, bf16[384,2048]{1,0:T(8,128)(2,1)} %collective-permute-done.2.refs_0_.refs_6_, bf16[384,2048]{1,0:T(8,128)(2,1)S(1)} %collective-permute-done.3.refs_1_.refs_7_, ...), custom_call_target="tpu_custom_call" | custom-call | flops 3221225472 | bytes 8388608 | tf_op jit(solution)/shard_map/expert_up/pallas_call | solution.py:236
  118.2 5.6 %expert_down.1 = bf16[1024,1024]{1,0:T(8,128)(2,1)} custom-call(s32[1]{0:T(128)} %bitcast.4.own_ref, bf16[512,768]{1,0:T(8,128)(2,1)S(1)} %expert_up.1.hidden, bf16[192,2048]{1,0:T(8,128)(2,1)} %collective-permute-done.6.refs_0_.refs_6_, bf16[192,2048]{1,0:T(8,128)(2,1)} %collective-permute-done.7.refs_1_.refs_7_, ...), custom_call_target="tpu_custom_call" | custom-call | flops 1610612736 | bytes 6029312 | tf_op jit(solution)/shard_map/expert_down/pallas_call | solution.py:311
  123.9 13.5 %all-to-all-start.1 = ((bf16[128,8,1024]{2,1,0:T(8,128)(2,1)}), bf16[128,8,1024]{2,1,0:T(8,128)(2,1)}, u32[]{:S(2)}, u32[]{:S(2)}) async-start(bf16[128,8,1024]{2,1,0:T(8,128)(2,1)} %bitcast.12), calls=%async_computation.1 | async-start | bytes 4194304 | tf_op jit(solution)/shard_map/all_to_all | solution.py:628
  137.4 1.4 pad_maximum_fusion.refs_0_
  138.8 1.1 collective-permute-start.12
  139.9 33.7 %collective-permute-done.12.refs_1_ = bf16[6144,128]{1,0:T(8,128)(2,1)S(1)} collective-permute-done((bf16[6144,128]{1,0:T(8,128)(2,1)S(1)}, bf16[6144,128]{1,0:T(8,128)(2,1)S(1)}, u32[]{:S(2)}, u32[]{:S(2)}) %collective-permute-start.12) | collective-permute-done | bytes 1572896 | tf_op jit(solution)/shard_map/ppermute | solution.py:648
  173.6 3.1 %collective-permute-start = (bf16[2,128,256]{2,1,0:T(8,128)(2,1)S(1)}, bf16[2,128,256]{2,1,0:T(8,128)(2,1)S(1)}, u32[]{:S(2)}, u32[]{:S(2)}) collective-permute-start(bf16[2,128,256]{2,1,0:T(8,128)(2,1)S(1)} %pad_maximum_fusion.1), channel_id=1, source_target_pairs={{0,1},{1,2},{2,3},{3,4},{4,5},{5,6},{6,7},{7,8},{8,9},{9,10},{10,1... | collective-permute-start | bytes 393224 | tf_op jit(solution)/shard_map/ppermute | solution.py:56
  176.7 7.3 %collective-permute-done.rim_ref = bf16[2,128,256]{2,1,0:T(8,128)(2,1)S(1)} collective-permute-done((bf16[2,128,256]{2,1,0:T(8,128)(2,1)S(1)}, bf16[2,128,256]{2,1,0:T(8,128)(2,1)S(1)}, u32[]{:S(2)}, u32[]{:S(2)}) %collective-permute-start) | collective-permute-done | bytes 131104 | tf_op jit(solution)/shard_map/ppermute | solution.py:56
  184.0 2.2 %copy-done = bf16[1024,2048]{1,0:T(8,128)(2,1)S(1)} copy-done((bf16[1024,2048]{1,0:T(8,128)(2,1)S(1)}, bf16[1024,2048]{1,0:T(8,128)(2,1)}, u32[]{:S(2)}) %copy-start) | copy-done | bytes 4194328
  186.2 1.0 copy-done.5
  187.2 0.9 copy-done.8
  188.1 0.9 copy-done.10
  189.1 5.9 %attention.1 = bf16[256,2048]{1,0:T(8,128)(2,1)} custom-call(s32[1]{0:T(128)} %bitcast.first_ref, f32[16]{0:T(128)S(1)} %copy-done.14, bf16[256,1024]{1,0:T(8,128)(2,1)S(1)} %copy-done.5, bf16[256,256]{1,0:T(8,128)(2,1)S(1)} %copy-done.8, bf16[256,256]{1,0:T(8,128)(2,1)S(1)} %copy-done.10, bf16[2,128,256]{2,1,0:T(8,128)(2,1)S(1)} %collective-permute-done.rim_ref, ...), custom_call_target="tpu_custom_call" | custom-call | flops 1610612736 | bytes 6291456 | tf_op jit(solution)/shard_map/attention/pallas_call | solution.py:531
  195.0 4.7 %shared_expert.1 = (f32[128,2048]{1,0:T(8,128)S(1)}, f32[128,128]{1,0:T(8,128)S(1)}) custom-call(s32[4]{0:T(128)S(1)} %pad_add_fusion.part_ref, s32[2,128]{1,0:T(2,128)S(1)} %bitcast.24, f32[2,128]{1,0:T(2,128)S(1)} %bitcast.25, bf16[128,2048]{1,0:T(8,128)(2,1)S(1)} %copy-done.6, bf16[6144,128]{1,0:T(8,128)(2,1)S(1)} %pad_maximum_fusion.refs_0_, ...), custom_call_target="tpu_custom_call" | custom-call | flops 805306368 | bytes 6291456 | tf_op jit(solution)/shard_map/shared_expert/pallas_call | solution.py:400
  199.8 1.0 copy-done.15
  200.8 1.2 copy-done.16
  202.0 3.9 %combine.1 = bf16[128,2048]{1,0:T(8,128)(2,1)} custom-call(bf16[1024,1024]{1,0:T(8,128)(2,1)} %bitcast.13.back_ref, f32[128,2048]{1,0:T(8,128)S(1)} %copy-done.16, f32[128,128]{1,0:T(8,128)S(1)} %get-tuple-element.17.columns_ref, f32[1,2048]{1,0:T(1,128)S(1)} %bitcast.26), custom_call_target="tpu_custom_call" | custom-call | flops 1073741824 | bytes 2097152 | tf_op jit(solution)/shard_map/combine/pallas_call | solution.py:455
  (50 shorter events, 1.4 us)
Async XLA Ops:
  4.8 106.6 %all-to-all-start = ((bf16[128,8,1024]{2,1,0:T(8,128)(2,1)}), bf16[128,8,1024]{2,1,0:T(8,128)(2,1)}, u32[]{:S(2)}, u32[]{:S(2)}) async-start(bf16[128,8,1024]{2,1,0:T(8,128)(2,1)} %bitcast.27), calls=%async_computation | async-start | bytes 4194304 | tf_op jit(solution)/shard_map/all_to_all | solution.py:606
  23.5 56.7 %collective-permute-start.1 = (bf16[384,2048]{1,0:T(8,128)(2,1)}, bf16[384,2048]{1,0:T(8,128)(2,1)S(1)}, u32[]{:S(2)}, u32[]{:S(2)}) collective-permute-start(bf16[384,2048]{1,0:T(8,128)(2,1)} %get-tuple-element.11), channel_id=1, source_target_pairs={{2,0},{0,4},{3,1},{1,5},{4,6},{6,2},{5,7},{7,3},{10,8},{8,12},{11,... | collective-permute-start | bytes 4718600 | tf_op jit(solution)/shard_map/ppermute | solution.py:590
  23.6 56.9 %collective-permute-start.3 = (bf16[384,2048]{1,0:T(8,128)(2,1)}, bf16[384,2048]{1,0:T(8,128)(2,1)S(1)}, u32[]{:S(2)}, u32[]{:S(2)}) collective-permute-start(bf16[384,2048]{1,0:T(8,128)(2,1)} %get-tuple-element.12), channel_id=1, source_target_pairs={{3,0},{1,4},{0,1},{2,5},{5,6},{7,2},{6,7},{4,3},{11,8},{9,12},{8,9... | collective-permute-start | bytes 4718600 | tf_op jit(solution)/shard_map/ppermute | solution.py:590
  80.2 28.4 %collective-permute-start.2 = (bf16[384,2048]{1,0:T(8,128)(2,1)S(1)}, bf16[384,2048]{1,0:T(8,128)(2,1)}, u32[]{:S(2)}, u32[]{:S(2)}) collective-permute-start(bf16[384,2048]{1,0:T(8,128)(2,1)S(1)} %collective-permute-done.1.refs_2_.refs_4_), channel_id=1, source_target_pairs={{0,4},{1,5},{2,6},{3,7},{4,0},{5,1},{6,2},{7,3},{8,12},{9,13},{10,... | collective-permute-start | bytes 4718600 | tf_op jit(solution)/shard_map/ppermute | solution.py:590
  80.4 30.9 %collective-permute-start.4 = (bf16[384,2048]{1,0:T(8,128)(2,1)S(1)}, bf16[384,2048]{1,0:T(8,128)(2,1)}, u32[]{:S(2)}, u32[]{:S(2)}) collective-permute-start(bf16[384,2048]{1,0:T(8,128)(2,1)S(1)} %collective-permute-done.3.refs_1_.refs_7_), channel_id=1, source_target_pairs={{0,4},{1,5},{2,6},{3,7},{4,0},{5,1},{6,2},{7,3},{8,12},{9,13},{10,... | collective-permute-start | bytes 4718600 | tf_op jit(solution)/shard_map/ppermute | solution.py:590
  80.7 1.4 copy-start.1
  82.4 20.0 %collective-permute-start.5 = (bf16[192,2048]{1,0:T(8,128)(2,1)S(1)}, bf16[192,2048]{1,0:T(8,128)(2,1)}, u32[]{:S(2)}, u32[]{:S(2)}) collective-permute-start(bf16[192,2048]{1,0:T(8,128)(2,1)S(1)} %get-tuple-element.13), channel_id=1, source_target_pairs={{2,0},{0,4},{3,1},{1,5},{4,6},{6,2},{5,7},{7,3},{10,8},{8,12},{11,... | collective-permute-start | bytes 2359304 | tf_op jit(solution)/shard_map/ppermute | solution.py:590
  82.7 21.7 %collective-permute-start.7 = (bf16[192,2048]{1,0:T(8,128)(2,1)S(1)}, bf16[192,2048]{1,0:T(8,128)(2,1)}, u32[]{:S(2)}, u32[]{:S(2)}) collective-permute-start(bf16[192,2048]{1,0:T(8,128)(2,1)S(1)} %get-tuple-element.14), channel_id=1, source_target_pairs={{3,0},{1,4},{0,1},{2,5},{5,6},{7,2},{6,7},{4,3},{11,8},{9,12},{8,9... | collective-permute-start | bytes 2359304 | tf_op jit(solution)/shard_map/ppermute | solution.py:590
  102.3 15.9 %collective-permute-start.6 = (bf16[192,2048]{1,0:T(8,128)(2,1)}, bf16[192,2048]{1,0:T(8,128)(2,1)}, u32[]{:S(2)}, u32[]{:S(2)}) collective-permute-start(bf16[192,2048]{1,0:T(8,128)(2,1)} %collective-permute-done.5.refs_2_.refs_4_), channel_id=1, source_target_pairs={{0,4},{1,5},{2,6},{3,7},{4,0},{5,1},{6,2},{7,3},{8,12},{9,13},{10,... | collective-permute-start | bytes 2359304 | tf_op jit(solution)/shard_map/ppermute | solution.py:590
  104.4 13.8 %collective-permute-start.8 = (bf16[192,2048]{1,0:T(8,128)(2,1)}, bf16[192,2048]{1,0:T(8,128)(2,1)}, u32[]{:S(2)}, u32[]{:S(2)}) collective-permute-start(bf16[192,2048]{1,0:T(8,128)(2,1)} %collective-permute-done.7.refs_1_.refs_7_), channel_id=1, source_target_pairs={{0,4},{1,5},{2,6},{3,7},{4,0},{5,1},{6,2},{7,3},{8,12},{9,13},{10,... | collective-permute-start | bytes 2359304 | tf_op jit(solution)/shard_map/ppermute | solution.py:590
  104.5 1.0 copy-start.2
  105.6 1.0 copy-start.3
  106.6 1.0 copy-start.4
  108.3 29.1 %collective-permute-start.11 = (bf16[1536,128]{1,0:T(8,128)(2,1)S(1)}, bf16[1536,128]{1,0:T(8,128)(2,1)}, u32[]{:S(2)}, u32[]{:S(2)}) collective-permute-start(bf16[1536,128]{1,0:T(8,128)(2,1)S(1)} %shared_prep.1), channel_id=1, source_target_pairs={{0,3},{1,0},{2,1},{3,2},{4,7},{5,4},{6,5},{7,6},{8,11},{9,8},{10,9... | collective-permute-start | bytes 1179656 | tf_op jit(solution)/shard_map/ppermute | solution.py:643
  108.6 28.8 %collective-permute-start.10 = (bf16[1536,128]{1,0:T(8,128)(2,1)S(1)}, bf16[1536,128]{1,0:T(8,128)(2,1)}, u32[]{:S(2)}, u32[]{:S(2)}) collective-permute-start(bf16[1536,128]{1,0:T(8,128)(2,1)S(1)} %shared_prep.1), channel_id=1, source_target_pairs={{0,2},{1,3},{2,0},{3,1},{4,6},{5,7},{6,4},{7,5},{8,10},{9,11},{10,... | collective-permute-start | bytes 1179656 | tf_op jit(solution)/shard_map/ppermute | solution.py:643
  111.3 26.1 %collective-permute-start.9 = (bf16[1536,128]{1,0:T(8,128)(2,1)S(1)}, bf16[1536,128]{1,0:T(8,128)(2,1)}, u32[]{:S(2)}, u32[]{:S(2)}) collective-permute-start(bf16[1536,128]{1,0:T(8,128)(2,1)S(1)} %shared_prep.1), channel_id=1, source_target_pairs={{0,1},{1,2},{2,3},{3,0},{4,5},{5,6},{6,7},{7,4},{8,9},{9,10},{10,1... | collective-permute-start | bytes 1179656 | tf_op jit(solution)/shard_map/ppermute | solution.py:643
  123.9 76.9 %all-to-all-start.1 = ((bf16[128,8,1024]{2,1,0:T(8,128)(2,1)}), bf16[128,8,1024]{2,1,0:T(8,128)(2,1)}, u32[]{:S(2)}, u32[]{:S(2)}) async-start(bf16[128,8,1024]{2,1,0:T(8,128)(2,1)} %bitcast.12), calls=%async_computation.1 | async-start | bytes 4194304 | tf_op jit(solution)/shard_map/all_to_all | solution.py:628
  137.3 36.2 %copy-start.7 = (bf16[256,256]{1,0:T(8,128)(2,1)S(1)}, bf16[256,256]{1,0:T(8,128)(2,1)}, u32[]{:S(2)}) copy-start(bf16[256,256]{1,0:T(8,128)(2,1)} %k_ref.1) | copy-start | bytes 393220
  137.3 36.2 %copy-start.9 = (bf16[256,256]{1,0:T(8,128)(2,1)S(1)}, bf16[256,256]{1,0:T(8,128)(2,1)}, u32[]{:S(2)}) copy-start(bf16[256,256]{1,0:T(8,128)(2,1)} %v_ref.1) | copy-start | bytes 393220
  137.4 46.7 %copy-start.11 = (f32[2048]{0:T(1024)S(1)}, f32[2048]{0:T(1024)}, u32[]{:S(2)}) copy-start(f32[2048]{0:T(1024)} %param.22) | copy-start | bytes 24580
  137.4 46.6 %copy-start.14 = (f32[16]{0:T(128)S(1)}, f32[16]{0:T(128)}, u32[]{:S(2)}) copy-start(f32[16]{0:T(128)} %sink_ref.1) | copy-start | bytes 196
  138.8 34.7 %collective-permute-start.12 = (bf16[6144,128]{1,0:T(8,128)(2,1)S(1)}, bf16[6144,128]{1,0:T(8,128)(2,1)S(1)}, u32[]{:S(2)}, u32[]{:S(2)}) collective-permute-start(bf16[6144,128]{1,0:T(8,128)(2,1)S(1)} %pad_maximum_fusion.refs_0_), channel_id=1, source_target_pairs={{0,8},{4,28},{8,0},{12,20},{16,24},{20,12},{24,16},{28,4},{1,9},{5... | collective-permute-start | bytes 4718600 | tf_op jit(solution)/shard_map/ppermute | solution.py:648
  139.9 55.1 %collective-permute-start.13 = (bf16[6144,128]{1,0:T(8,128)(2,1)S(1)}, bf16[6144,128]{1,0:T(8,128)(2,1)}, u32[]{:S(2)}, u32[]{:S(2)}) collective-permute-start(bf16[6144,128]{1,0:T(8,128)(2,1)S(1)} %pad_maximum_fusion.refs_0_), channel_id=1, source_target_pairs={{0,4},{4,0},{1,5},{5,1},{2,6},{6,2},{3,7},{7,3},{8,12},{12,8},{9,1... | collective-permute-start | bytes 4718600 | tf_op jit(solution)/shard_map/ppermute | solution.py:649
  173.6 21.4 %collective-permute-start.14 = (bf16[6144,128]{1,0:T(8,128)(2,1)S(1)}, bf16[6144,128]{1,0:T(8,128)(2,1)}, u32[]{:S(2)}, u32[]{:S(2)}) collective-permute-start(bf16[6144,128]{1,0:T(8,128)(2,1)S(1)} %collective-permute-done.12.refs_1_), channel_id=1, source_target_pairs={{0,4},{4,0},{1,5},{5,1},{2,6},{6,2},{3,7},{7,3},{8,12},{12,8},{9,1... | collective-permute-start | bytes 4718600 | tf_op jit(solution)/shard_map/ppermute | solution.py:649
  173.6 10.4 %collective-permute-start = (bf16[2,128,256]{2,1,0:T(8,128)(2,1)S(1)}, bf16[2,128,256]{2,1,0:T(8,128)(2,1)S(1)}, u32[]{:S(2)}, u32[]{:S(2)}) collective-permute-start(bf16[2,128,256]{2,1,0:T(8,128)(2,1)S(1)} %pad_maximum_fusion.1), channel_id=1, source_target_pairs={{0,1},{1,2},{2,3},{3,4},{4,5},{5,6},{6,7},{7,8},{8,9},{9,10},{10,1... | collective-permute-start | bytes 393224 | tf_op jit(solution)/shard_map/ppermute | solution.py:56
  184.0 2.2 %copy-start = (bf16[1024,2048]{1,0:T(8,128)(2,1)S(1)}, bf16[1024,2048]{1,0:T(8,128)(2,1)}, u32[]{:S(2)}) copy-start(bf16[1024,2048]{1,0:T(8,128)(2,1)} %weight_ref.1) | copy-start | bytes 12582916
  186.2 1.0 copy-start.5
  189.1 6.0 %copy-start.6 = (bf16[128,2048]{1,0:T(8,128)(2,1)S(1)}, bf16[128,2048]{1,0:T(8,128)(2,1)}, u32[]{:S(2)}) copy-start(bf16[128,2048]{1,0:T(8,128)(2,1)} %get-tuple-element.15.x_ref) | copy-start | bytes 1572868
  189.1 6.0 %copy-start.12 = (s32[128,2]{0,1:T(2,128)S(1)}, s32[128,2]{0,1:T(2,128)}, u32[]{:S(2)}) copy-start(s32[128,2]{0,1:T(2,128)} %param.25) | copy-start | bytes 3076
  189.1 6.0 %copy-start.13 = (f32[128,2]{0,1:T(2,128)S(1)}, f32[128,2]{0,1:T(2,128)}, u32[]{:S(2)}) copy-start(f32[128,2]{0,1:T(2,128)} %param.26) | copy-start | bytes 3076
  195.0 5.7 %copy-start.17 = (f32[2048]{0:T(1024)S(1)}, f32[2048]{0:T(1024)}, u32[]{:S(2)}) copy-start(f32[2048]{0:T(1024)} %param.33) | copy-start | bytes 24580
  200.8 1.2 copy-start.16
  (3 other events, 2.8 us)

commit v3 on v2

--- a/solution.py
+++ b/solution.py
@@ -17,7 +17,7 @@
 BLOCK = 256
 MIB = 1 << 20
 PARTS = 4
-COMBINE_LIMIT = 16
+COMBINE_LIMIT = 62
 UP_LIMIT = 24
 DOWN_LIMIT = 16
 EP = ("z", "y", "c")
@@ -81,101 +81,114 @@
     return rows
 
 
-def pack_kernel(x_ref, gain_ref, ids_ref, packed_ref, normed_ref, stacked):
+def pack_kernel(
+    expert_ref, x_ref, gain_ref, ids_ref, gate_ref, up_ref, packed_ref, normed_ref, piece_ref, *scratch
+):
+    stacked, made, held, sems, block_sems = scratch
     half = x_ref.shape[1] // 2
     tokens = x_ref.shape[0]
-    step = pl.program_id(0)
-    block = packed_ref.shape[0]
-
-    @pl.when(step == 0)
-    def _():
-        x = x_ref[...].astype(f32)
-        normed = rms_scale(x, gain_ref[...]).astype(bf16)
-        normed_ref[...] = normed
-        stacked[:tokens, :] = normed[:, :half]
-        stacked[tokens:, :] = normed[:, half:]
-
+    ins, outs = expert_copies(expert_ref[0], (gate_ref, up_ref), held, piece_ref, sems)
+    for c in ins:
+        c.start()
+    x = x_ref[...].astype(f32)
+    normed = rms_scale(x, gain_ref[...]).astype(bf16)
+    normed_ref[...] = normed
+    stacked[:tokens, :] = normed[:, :half]
+    stacked[tokens:, :] = normed[:, half:]
     rows = slot_rows(ids_ref[...].astype(f32), True)
-    r = iota((block, tokens), 0) + step * block
-    chosen = jnp.concatenate(
-        [
-            jnp.where((r == rows[0] + h * CAP) | (r == rows[1] + h * CAP), 1.0, 0.0).astype(bf16)
-            for h in range(2)
-        ],
-        axis=1,
-    )
-    packed_ref[...] = dot(chosen, stacked[...]).astype(bf16)
-
-
-def pack(x, gain, ids, slots):
+    size = made.shape[0] // block_sems.shape[0]
+    blocks = []
+    for i in range(block_sems.shape[0]):
+        at = pl.ds(i * size, size)
+        blocks.append(pltpu.make_async_copy(made.at[at], packed_ref.at[at], block_sems.at[i]))
+    for i, block in enumerate(blocks):
+        r = iota((size, tokens), 0) + i * size
+        chosen = jnp.concatenate(
+            [
+                jnp.where((r == rows[0] + h * CAP) | (r == rows[1] + h * CAP), 1.0, 0.0).astype(
+                    bf16
+                )
+                for h in range(2)
+            ],
+            axis=1,
+        )
+        made[i * size : (i + 1) * size, :] = dot(chosen, stacked[...]).astype(bf16)
+        block.start()
+        if i == 0:
+            for c, d in zip(ins, outs):
+                c.wait()
+                d.start()
+    for c in blocks + outs:
+        c.wait()
+
+
+def pack(expert, x, gain, ids, gate, up, slots):
     tokens, width = x.shape
+    rows = gate.shape[1]
     steps = 4
     total = 2 * slots
+    hbm = pl.BlockSpec(memory_space=ANY)
+    vmem = pl.BlockSpec(memory_space=VMEM)
     return pl.pallas_call(
         pack_kernel,
-        grid=(steps,),
-        in_specs=[
-            pl.BlockSpec((tokens, width), lambda i: (0, 0)),
-            pl.BlockSpec((1, width), lambda i: (0, 0)),
-            pl.BlockSpec((2, tokens), lambda i: (0, 0)),
-        ],
-        out_specs=[
-            pl.BlockSpec((total // steps, width // 2), lambda i: (i, 0)),
-            pl.BlockSpec((tokens, width), lambda i: (0, 0)),
-        ],
+        in_specs=[pl.BlockSpec(memory_space=pltpu.SMEM), vmem, vmem, vmem, hbm, hbm],
+        out_specs=[hbm, vmem, hbm],
         out_shape=[
             jax.ShapeDtypeStruct((total, width // 2), bf16),
             jax.ShapeDtypeStruct((tokens, width), bf16),
+            jax.ShapeDtypeStruct((2 * rows, width), bf16),
         ],
-        scratch_shapes=[VMEM((2 * tokens, width // 2), bf16)],
+        scratch_shapes=[
+            VMEM((2 * tokens, width // 2), bf16),
+            VMEM((total, width // 2), bf16),
+            VMEM((2 * rows, width), bf16),
+            pltpu.SemaphoreType.DMA((2, 2)),
+            pltpu.SemaphoreType.DMA((steps,)),
+        ],
+        compiler_params=pltpu.CompilerParams(vmem_limit_bytes=63 * MIB),
         cost_estimate=pl.CostEstimate(
             flops=2 * total * tokens * width, bytes_accessed=6 * tokens * width, transcendentals=0
         ),
         name="pack",
-    )(x, gain, ids)
-
-
-def pick_kernel(parity_ref, *refs):
-    arrays, outs, held, sems = refs[:-4], refs[-4:-2], refs[-2], refs[-1]
+    )(expert, x, gain, ids, gate, up)
+
+
+def expert_copies(j, arrays, held, out, sems):
     rows = arrays[0].shape[1]
-    steps = []
-    for p, out in enumerate(outs):
-        j = lax.rem(parity_ref[0] + p, 2)
-        for m, array in enumerate(arrays):
-            at = pl.ds(m * rows, rows)
-            steps.append(
-                (
-                    pltpu.make_async_copy(array.at[j], held.at[p, at], sems.at[0, p, m]),
-                    pltpu.make_async_copy(held.at[p, at], out.at[at], sems.at[1, p, m]),
-                )
-            )
-    for c, _ in steps:
+    ins, outs = [], []
+    for m, array in enumerate(arrays):
+        at = pl.ds(m * rows, rows)
+        ins.append(pltpu.make_async_copy(array.at[j], held.at[at], sems.at[0, m]))
+        outs.append(pltpu.make_async_copy(held.at[at], out.at[at], sems.at[1, m]))
+    return ins, outs
+
+
+def pick_kernel(expert_ref, *refs):
+    ins, outs = expert_copies(expert_ref[0], refs[:-3], refs[-2], refs[-3], refs[-1])
+    for c in ins:
         c.start()
-    for c, d in steps:
+    for c, d in zip(ins, outs):
         c.wait()
         d.start()
-    for _, d in steps:
+    for d in outs:
         d.wait()
 
 
-def pick(parity, arrays, limit):
+def pick(expert, arrays, limit):
     rows, width = arrays[0].shape[1:]
     count = len(arrays)
     return pl.pallas_call(
         pick_kernel,
         in_specs=[pl.BlockSpec(memory_space=pltpu.SMEM)] + [pl.BlockSpec(memory_space=ANY)] * count,
-        out_specs=[pl.BlockSpec(memory_space=ANY)] * 2,
-        out_shape=[jax.ShapeDtypeStruct((count * rows, width), bf16)] * 2,
-        scratch_shapes=[
-            VMEM((2, count * rows, width), bf16),
-            pltpu.SemaphoreType.DMA((2, 2, count)),
-        ],
+        out_specs=pl.BlockSpec(memory_space=ANY),
+        out_shape=jax.ShapeDtypeStruct((count * rows, width), bf16),
+        scratch_shapes=[VMEM((count * rows, width), bf16), pltpu.SemaphoreType.DMA((2, count))],
         compiler_params=pltpu.CompilerParams(vmem_limit_bytes=limit * MIB),
         cost_estimate=pl.CostEstimate(
-            flops=1000, bytes_accessed=8 * count * rows * width, transcendentals=0
+            flops=1000, bytes_accessed=4 * count * rows * width, transcendentals=0
         ),
         name="pick",
-    )(parity, *arrays)
+    )(expert, *arrays)
 
 
 def start_pieces(own_ref, own, other, copy, parts):
@@ -261,7 +274,6 @@
     out_ref, down, made, sems, out_sems = refs[8:]
     part = own[0].shape[0]
     half = out_ref.shape[1]
-    groups = out_ref.shape[0] // BLOCK
     count = half // BLOCK
 
     def copies(n, pieces):
@@ -283,20 +295,19 @@
                 for c in copies(n, pieces):
                     c.start()
 
-    a, b = iota((BLOCK, BLOCK), 0), iota((BLOCK, BLOCK), 1)
-    b, h = b % (BLOCK // 2), b // (BLOCK // 2)
-    back = jnp.where(a == (b // CAP) * (2 * CAP) + b % CAP + h * CAP, 1.0, 0.0).astype(bf16)
+    tiles = hidden.shape[0] // (2 * CAP)
+    low = iota((tiles, 2 * CAP, BLOCK), 1) < CAP
     for n in range(count):
         for c in copies(n, own):
             c.wait()
         at = n * BLOCK
         x = hidden[...]
-        left = dot(x, down[:, at : at + BLOCK]).astype(bf16)
-        right = dot(x, down[:, half + at : half + at + BLOCK]).astype(bf16)
-        for i in range(groups):
-            mine = slice(i * (BLOCK // 2), (i + 1) * (BLOCK // 2))
-            both = jnp.concatenate([left[mine], right[mine]], axis=0)
-            made[i * BLOCK : (i + 1) * BLOCK, at : at + BLOCK] = dot(back, both).astype(bf16)
+        left = dot(x, down[:, at : at + BLOCK]).reshape(tiles, 2 * CAP, BLOCK)
+        right = dot(x, down[:, half + at : half + at + BLOCK]).reshape(tiles, 2 * CAP, BLOCK)
+        one = jnp.where(low, left, pltpu.roll(right, CAP, 1))
+        two = jnp.where(low, pltpu.roll(left, CAP, 1), right)
+        both = jnp.stack([one, two], axis=1).reshape(out_ref.shape[0], BLOCK)
+        made[:, at : at + BLOCK] = both.astype(bf16)
         columns = pl.ds(at, BLOCK)
         pltpu.make_async_copy(made.at[:, columns], out_ref.at[:, columns], out_sems.at[n]).start()
     for n in range(count):
@@ -416,11 +427,18 @@
     )(part, ids, weights, normed, *parts)
 
 
-def combine_kernel(back_ref, shared_ref, columns_ref, gain_ref, out_ref, came, common, sems):
+def combine_kernel(
+    back_ref, shared_ref, columns_ref, gain_ref, out_ref, came, common, sem, back_sems
+):
     tokens, half = out_ref.shape[0], back_ref.shape[1]
-    back_in = pltpu.make_async_copy(back_ref, came, sems.at[0])
-    shared_in = pltpu.make_async_copy(shared_ref, common, sems.at[1])
-    back_in.start()
+    rows = [pl.ds(i * BLOCK, BLOCK) for i in range(back_ref.shape[0] // BLOCK)]
+    back_in = [
+        pltpu.make_async_copy(back_ref.at[at], came.at[at], back_sems.at[i])
+        for i, at in enumerate(rows)
+    ]
+    shared_in = pltpu.make_async_copy(shared_ref, common, sem)
+    for c in back_in:
+        c.start()
     shared_in.start()
     r = iota((tokens, back_ref.shape[0]), 1)
     first = [columns_ref[:, k : k + 1].astype(jnp.int32) for k in range(2)]
@@ -430,16 +448,16 @@
         spread = jnp.where(r == first[0] + h * CAP, weights[0], 0.0) + jnp.where(
             r == first[1] + h * CAP, weights[1], 0.0
         )
-        coarse = spread.astype(bf16)
-        fine = (spread - coarse.astype(f32)).astype(bf16)
-        spreads += [coarse, fine]
-    back_in.wait()
-    summed = dot(jnp.concatenate(spreads, axis=0), came[...])
+        spreads.append(spread.astype(bf16))
+    spread = jnp.concatenate(spreads, axis=0)
+    summed = jnp.zeros((2 * tokens, half), f32)
+    for i, c in enumerate(back_in):
+        c.wait()
+        at = slice(i * BLOCK, (i + 1) * BLOCK)
+        summed = summed + dot(spread[:, at], came[at, :])
     shared_in.wait()
     halves = [
-        summed[2 * h * tokens : (2 * h + 1) * tokens]
-        + summed[(2 * h + 1) * tokens : (2 * h + 2) * tokens]
-        + common[:, h * half : (h + 1) * half]
+        summed[h * tokens : (h + 1) * tokens] + common[:, h * half : (h + 1) * half]
         for h in range(2)
     ]
     square = sum(jnp.sum(v * v, axis=1, keepdims=True) for v in halves)
@@ -460,7 +478,8 @@
         scratch_shapes=[
             VMEM((slots, half), bf16),
             VMEM((tokens, 2 * half), f32),
-            pltpu.SemaphoreType.DMA((2,)),
+            pltpu.SemaphoreType.DMA,
+            pltpu.SemaphoreType.DMA((slots // BLOCK,)),
         ],
         compiler_params=pltpu.CompilerParams(vmem_limit_bytes=COMBINE_LIMIT * MIB),
         cost_estimate=pl.CostEstimate(
@@ -584,7 +603,8 @@
 
     gate_t, up_t = w_gate.transpose(0, 2, 1), w_up.transpose(0, 2, 1)
 
-    parity = (x % 2).astype(jnp.int32).reshape(1)
+    even_expert = (x % 2).astype(jnp.int32).reshape(1)
+    odd_expert = 1 - even_expert
 
     def moved(piece, route):
         return lax.ppermute(piece, CORE_TP, route)
@@ -597,18 +617,19 @@
             came_near,
         )
 
-    even, odd = pick(parity, (gate_t, up_t), 63)
-    near_in, far_in = moved(odd, near), moved(even, far)
-
+    near_in = moved(pick(odd_expert, (gate_t, up_t), 63), near)
     ids_t = expert_ids.T
-    packed, normed = pack(moe_in, pre_gain.reshape(1, -1), ids_t, 128 * CAP)
+    packed, normed, even = pack(
+        even_expert, moe_in, pre_gain.reshape(1, -1), ids_t, gate_t, up_t, 128 * CAP
+    )
+    far_in = moved(even, far)
     chips = packed.shape[0] // (2 * CAP)
     arrived = lax.all_to_all(
         packed.reshape(chips, 2 * CAP, -1), CHIPS, split_axis=0, concat_axis=0, tiled=True
     ).reshape(packed.shape)
 
-    even_out, odd_out = pick(parity, (w_down,), 8)
-    near_out, far_out = moved(odd_out, near), moved(even_out, far)
+    near_out = moved(pick(odd_expert, (w_down,), 8), near)
+    far_out = moved(pick(even_expert, (w_down,), 8), far)
     up_pieces = gathered(near_in, far_in, moved(near_in, swapped), moved(far_in, swapped))
     down_pieces = gathered(near_out, far_out, moved(near_out, swapped), moved(far_out, swapped))
 

time: 210 us -> 209 us (level)
    unnamed x36 -> x34, local copies, waits for them, and re-layouts: 11.8 us -> 11.2 us
  transfers between devices with their start and end apart: 17 -> 17, of which waited for: 6 -> 6; matrix products, arithmetic and copies ran while one was open for 1% -> 1% of each run, Pallas kernels for 13% -> 12%
where the time goes in v3:
time: 209 us; the launch traced here: 206 us
  waiting for transfers between devices  118 us (56%)
  starting transfers between devices  40.2 us (19%)
  Pallas kernels  34.2 us (16%)
  local copies, waits for them, and re-layouts  11.2 us (5%)
    ppermute x8, waiting for transfers between devices, moved(): return lax.ppermute(piece, CORE_TP, route)  75.5 us
    ppermute x1, waiting for transfers between devices, body(): quarters.append(lax.ppermute(quarters[0], ('y', 'c'), beside))  34 us
    all_to_all x1, starting transfers between devices, body(): lax.all_to_all(packed.reshape(chips, 2 * CAP, -1), CHIPS, split_axis=0, c...  15.8 us
    all_to_all x1, starting transfers between devices, body(): lax.all_to_all(out.reshape(chips, 2 * CAP, -1), CHIPS, split_axis=0, conc...  15.1 us
    unnamed x34, local copies, waits for them, and re-layouts  11.2 us
    ppermute x1, waiting for transfers between devices, from_behind(): return lax.ppermute(block, axis, route)  8.25 us
    pallas_call x1, Pallas kernels, expert_up(): pl.pallas_call(up_kernel, in_specs=[pl.BlockSpec(memory_space=pltpu.SMEM)...  6.87 us
    pallas_call x1, Pallas kernels, attention(): pl.pallas_call(attention_kernel, in_specs=[pl.BlockSpec(memory_space=pltp...  5.94 us
  transfers between devices with their start and end apart: 17, of which 6 were waited for; matrix products, arithmetic and copies ran while one was open for 1% of the time, Pallas kernels for 12%

profile of v3, /device:TPU:8, one launch (start us, length us, event | category | flops | bytes accessed | tf_op | source)
XLA Modules:
  0.0 206.0 jit_solution(16307945184229971546)
XLA Ops:
  0.6 4.8 %pack.1 = (bf16[1024,1024]{1,0:T(8,128)(2,1)}, bf16[128,2048]{1,0:T(8,128)(2,1)}, bf16[384,2048]{1,0:T(8,128)(2,1)}) custom-call(s32[1]{0:T(128)} %bitcast.5.expert_ref, bf16[128,2048]{1,0:T(8,128)(2,1)} %x_ref.1, f32[1,2048]{1,0:T(1,128)} %bitcast.31, s32[2,128]{1,0:T(2,128)} %bitcast.23, bf16[2,192,2048]{2,1,0:T(8,128)(2,1)} %bitcast.26, ...), custom_call_target="tpu_custom_call" | custom-call | flops 536870912 | bytes 1572864 | tf_op jit(solution)/shard_map/pack/pallas_call | solution.py:132
  5.4 15.8 %all-to-all-start = ((bf16[128,8,1024]{2,1,0:T(8,128)(2,1)}), bf16[128,8,1024]{2,1,0:T(8,128)(2,1)}, u32[]{:S(2)}, u32[]{:S(2)}) async-start(bf16[128,8,1024]{2,1,0:T(8,128)(2,1)} %bitcast.30), calls=%async_computation | async-start | bytes 4194304 | tf_op jit(solution)/shard_map/all_to_all | solution.py:627
  21.3 2.4 %pick.3 = bf16[384,2048]{1,0:T(8,128)(2,1)} custom-call(s32[1]{0:T(128)S(6)} %sub.15.expert_ref, bf16[2,192,2048]{2,1,0:T(8,128)(2,1)} %bitcast.27, bf16[2,192,2048]{2,1,0:T(8,128)(2,1)} %bitcast.29), custom_call_target="tpu_custom_call" | custom-call | flops 1000 | bytes 3145728 | tf_op jit(solution)/shard_map/pick/pallas_call | solution.py:180
  23.7 1.5 collective-permute-start.3
  25.3 52.9 %collective-permute-done.1.refs_2_.refs_4_ = bf16[384,2048]{1,0:T(8,128)(2,1)} collective-permute-done((bf16[384,2048]{1,0:T(8,128)(2,1)}, bf16[384,2048]{1,0:T(8,128)(2,1)}, u32[]{:S(2)}, u32[]{:S(2)}) %collective-permute-start.1) | collective-permute-done | bytes 1572896 | tf_op jit(solution)/shard_map/ppermute | solution.py:610
  78.1 1.3 collective-permute-done.3.refs_1_.refs_7_
  79.5 1.4 copy-done
  81.0 0.6 collective-permute-start.5
  82.0 20.0 %collective-permute-done.5.refs_2_.refs_4_ = bf16[192,2048]{1,0:T(8,128)(2,1)} collective-permute-done((bf16[192,2048]{1,0:T(8,128)(2,1)S(1)}, bf16[192,2048]{1,0:T(8,128)(2,1)}, u32[]{:S(2)}, u32[]{:S(2)}) %collective-permute-start.5) | collective-permute-done | bytes 786464 | tf_op jit(solution)/shard_map/ppermute | solution.py:610
  102.0 1.3 collective-permute-done.7.refs_1_.refs_7_
  103.4 1.0 copy-done.2
  104.4 1.0 copy-done.3
  105.5 1.0 copy-done.4
  106.5 0.6 shared_prep.1
  107.6 2.3 %collective-permute-start.10 = (bf16[1536,128]{1,0:T(8,128)(2,1)S(1)}, bf16[1536,128]{1,0:T(8,128)(2,1)}, u32[]{:S(2)}, u32[]{:S(2)}) collective-permute-start(bf16[1536,128]{1,0:T(8,128)(2,1)S(1)} %shared_prep.1), channel_id=1, source_target_pairs={{0,2},{1,3},{2,0},{3,1},{4,6},{5,7},{6,4},{7,5},{8,10},{9,11},{10,... | collective-permute-start | bytes 1179656 | tf_op jit(solution)/shard_map/ppermute | solution.py:664
  109.9 6.9 %expert_up.1.hidden = bf16[512,768]{1,0:T(8,128)(2,1)S(1)} custom-call(s32[1]{0:T(128)} %bitcast.4.own_ref, bf16[1024,1024]{1,0:T(8,128)(2,1)} %bitcast.11.recv, bf16[384,2048]{1,0:T(8,128)(2,1)S(1)} %collective-permute-done.2.refs_0_.refs_6_, bf16[384,2048]{1,0:T(8,128)(2,1)S(1)} %collective-permute-done.3.refs_1_.refs_7_, ...), custom_call_target="tpu_custom_call" | custom-call | flops 3221225472 | bytes 8388608 | tf_op jit(solution)/shard_map/expert_up/pallas_call | solution.py:249
  116.8 4.8 %expert_down.1 = bf16[1024,1024]{1,0:T(8,128)(2,1)} custom-call(s32[1]{0:T(128)} %bitcast.4.own_ref, bf16[512,768]{1,0:T(8,128)(2,1)S(1)} %expert_up.1.hidden, bf16[192,2048]{1,0:T(8,128)(2,1)} %collective-permute-done.6.refs_0_.refs_6_, bf16[192,2048]{1,0:T(8,128)(2,1)} %collective-permute-done.7.refs_1_.refs_7_, ...), custom_call_target="tpu_custom_call" | custom-call | flops 1610612736 | bytes 6029312 | tf_op jit(solution)/shard_map/expert_down/pallas_call | solution.py:322
  121.6 15.1 %all-to-all-start.1 = ((bf16[128,8,1024]{2,1,0:T(8,128)(2,1)}), bf16[128,8,1024]{2,1,0:T(8,128)(2,1)}, u32[]{:S(2)}, u32[]{:S(2)}) async-start(bf16[128,8,1024]{2,1,0:T(8,128)(2,1)} %bitcast.12), calls=%async_computation.1 | async-start | bytes 4194304 | tf_op jit(solution)/shard_map/all_to_all | solution.py:649
  136.7 1.4 pad_maximum_fusion.refs_0_
  138.1 1.1 collective-permute-start.12
  139.2 34.0 %collective-permute-done.12.refs_1_ = bf16[6144,128]{1,0:T(8,128)(2,1)S(1)} collective-permute-done((bf16[6144,128]{1,0:T(8,128)(2,1)S(1)}, bf16[6144,128]{1,0:T(8,128)(2,1)S(1)}, u32[]{:S(2)}, u32[]{:S(2)}) %collective-permute-start.12) | collective-permute-done | bytes 1572896 | tf_op jit(solution)/shard_map/ppermute | solution.py:669
  173.2 3.0 %collective-permute-start = (bf16[2,128,256]{2,1,0:T(8,128)(2,1)S(1)}, bf16[2,128,256]{2,1,0:T(8,128)(2,1)S(1)}, u32[]{:S(2)}, u32[]{:S(2)}) collective-permute-start(bf16[2,128,256]{2,1,0:T(8,128)(2,1)S(1)} %pad_maximum_fusion.1), channel_id=1, source_target_pairs={{0,1},{1,2},{2,3},{3,4},{4,5},{5,6},{6,7},{7,8},{8,9},{9,10},{10,1... | collective-permute-start | bytes 393224 | tf_op jit(solution)/shard_map/ppermute | solution.py:56
  176.3 8.2 %collective-permute-done.rim_ref = bf16[2,128,256]{2,1,0:T(8,128)(2,1)S(1)} collective-permute-done((bf16[2,128,256]{2,1,0:T(8,128)(2,1)S(1)}, bf16[2,128,256]{2,1,0:T(8,128)(2,1)S(1)}, u32[]{:S(2)}, u32[]{:S(2)}) %collective-permute-start) | collective-permute-done | bytes 131104 | tf_op jit(solution)/shard_map/ppermute | solution.py:56
  184.5 2.2 %copy-done.1 = bf16[1024,2048]{1,0:T(8,128)(2,1)S(1)} copy-done((bf16[1024,2048]{1,0:T(8,128)(2,1)S(1)}, bf16[1024,2048]{1,0:T(8,128)(2,1)}, u32[]{:S(2)}) %copy-start.1) | copy-done | bytes 4194328
  186.7 1.0 copy-done.5
  187.7 0.9 copy-done.8
  188.6 0.9 copy-done.10
  189.6 5.9 %attention.1 = bf16[256,2048]{1,0:T(8,128)(2,1)} custom-call(s32[1]{0:T(128)} %bitcast.first_ref, f32[16]{0:T(128)S(1)} %copy-done.14, bf16[256,1024]{1,0:T(8,128)(2,1)S(1)} %copy-done.5, bf16[256,256]{1,0:T(8,128)(2,1)S(1)} %copy-done.8, bf16[256,256]{1,0:T(8,128)(2,1)S(1)} %copy-done.10, bf16[2,128,256]{2,1,0:T(8,128)(2,1)S(1)} %collective-permute-done.rim_ref, ...), custom_call_target="tpu_custom_call" | custom-call | flops 1610612736 | bytes 6291456 | tf_op jit(solution)/shard_map/attention/pallas_call | solution.py:550
  195.5 4.7 %shared_expert.1 = (f32[128,2048]{1,0:T(8,128)S(1)}, f32[128,128]{1,0:T(8,128)S(1)}) custom-call(s32[4]{0:T(128)S(1)} %pad_add_fusion.part_ref, s32[2,128]{1,0:T(2,128)S(1)} %bitcast.24, f32[2,128]{1,0:T(2,128)S(1)} %bitcast.25, bf16[128,2048]{1,0:T(8,128)(2,1)S(1)} %copy-done.6, bf16[6144,128]{1,0:T(8,128)(2,1)S(1)} %pad_maximum_fusion.refs_0_, ...), custom_call_target="tpu_custom_call" | custom-call | flops 805306368 | bytes 6291456 | tf_op jit(solution)/shard_map/shared_expert/pallas_call | solution.py:411
  200.2 1.0 copy-done.15
  201.3 0.6 copy-done.16
  201.9 3.9 %combine.1 = bf16[128,2048]{1,0:T(8,128)(2,1)} custom-call(bf16[1024,1024]{1,0:T(8,128)(2,1)} %bitcast.13.back_ref, f32[128,2048]{1,0:T(8,128)} %copy-done.15, f32[128,128]{1,0:T(8,128)} %copy-done.16, f32[1,2048]{1,0:T(1,128)} %bitcast.32), custom_call_target="tpu_custom_call" | custom-call | flops 1073741824 | bytes 2097152 | tf_op jit(solution)/shard_map/combine/pallas_call | solution.py:473
  (49 shorter events, 1.3 us)
Async XLA Ops:
  5.4 104.5 %all-to-all-start = ((bf16[128,8,1024]{2,1,0:T(8,128)(2,1)}), bf16[128,8,1024]{2,1,0:T(8,128)(2,1)}, u32[]{:S(2)}, u32[]{:S(2)}) async-start(bf16[128,8,1024]{2,1,0:T(8,128)(2,1)} %bitcast.30), calls=%async_computation | async-start | bytes 4194304 | tf_op jit(solution)/shard_map/all_to_all | solution.py:627
  21.2 56.9 %collective-permute-start.1 = (bf16[384,2048]{1,0:T(8,128)(2,1)}, bf16[384,2048]{1,0:T(8,128)(2,1)}, u32[]{:S(2)}, u32[]{:S(2)}) collective-permute-start(bf16[384,2048]{1,0:T(8,128)(2,1)} %get-tuple-element.8), channel_id=1, source_target_pairs={{2,0},{0,4},{3,1},{1,5},{4,6},{6,2},{5,7},{7,3},{10,8},{8,12},{11,... | collective-permute-start | bytes 4718600 | tf_op jit(solution)/shard_map/ppermute | solution.py:610
  23.7 55.7 %collective-permute-start.3 = (bf16[384,2048]{1,0:T(8,128)(2,1)}, bf16[384,2048]{1,0:T(8,128)(2,1)S(1)}, u32[]{:S(2)}, u32[]{:S(2)}) collective-permute-start(bf16[384,2048]{1,0:T(8,128)(2,1)} %pick.3), channel_id=1, source_target_pairs={{3,0},{1,4},{0,1},{2,5},{5,6},{7,2},{6,7},{4,3},{11,8},{9,12},{8,9... | collective-permute-start | bytes 4718600 | tf_op jit(solution)/shard_map/ppermute | solution.py:610
  78.1 29.5 %collective-permute-start.2 = (bf16[384,2048]{1,0:T(8,128)(2,1)}, bf16[384,2048]{1,0:T(8,128)(2,1)S(1)}, u32[]{:S(2)}, u32[]{:S(2)}) collective-permute-start(bf16[384,2048]{1,0:T(8,128)(2,1)} %collective-permute-done.1.refs_2_.refs_4_), channel_id=1, source_target_pairs={{0,4},{1,5},{2,6},{3,7},{4,0},{5,1},{6,2},{7,3},{8,12},{9,13},{10,... | collective-permute-start | bytes 4718600 | tf_op jit(solution)/shard_map/ppermute | solution.py:610
  79.4 30.4 %collective-permute-start.4 = (bf16[384,2048]{1,0:T(8,128)(2,1)S(1)}, bf16[384,2048]{1,0:T(8,128)(2,1)}, u32[]{:S(2)}, u32[]{:S(2)}) collective-permute-start(bf16[384,2048]{1,0:T(8,128)(2,1)S(1)} %collective-permute-done.3.refs_1_.refs_7_), channel_id=1, source_target_pairs={{0,4},{1,5},{2,6},{3,7},{4,0},{5,1},{6,2},{7,3},{8,12},{9,13},{10,... | collective-permute-start | bytes 4718600 | tf_op jit(solution)/shard_map/ppermute | solution.py:610
  79.4 1.4 copy-start
  81.0 21.0 %collective-permute-start.5 = (bf16[192,2048]{1,0:T(8,128)(2,1)S(1)}, bf16[192,2048]{1,0:T(8,128)(2,1)}, u32[]{:S(2)}, u32[]{:S(2)}) collective-permute-start(bf16[192,2048]{1,0:T(8,128)(2,1)S(1)} %pick.4), channel_id=1, source_target_pairs={{2,0},{0,4},{3,1},{1,5},{4,6},{6,2},{5,7},{7,3},{10,8},{8,12},{11,... | collective-permute-start | bytes 2359304 | tf_op jit(solution)/shard_map/ppermute | solution.py:610
  81.7 21.6 %collective-permute-start.7 = (bf16[192,2048]{1,0:T(8,128)(2,1)S(1)}, bf16[192,2048]{1,0:T(8,128)(2,1)}, u32[]{:S(2)}, u32[]{:S(2)}) collective-permute-start(bf16[192,2048]{1,0:T(8,128)(2,1)S(1)} %pick.5), channel_id=1, source_target_pairs={{3,0},{1,4},{0,1},{2,5},{5,6},{7,2},{6,7},{4,3},{11,8},{9,12},{8,9... | collective-permute-start | bytes 2359304 | tf_op jit(solution)/shard_map/ppermute | solution.py:610
  102.0 14.8 %collective-permute-start.6 = (bf16[192,2048]{1,0:T(8,128)(2,1)}, bf16[192,2048]{1,0:T(8,128)(2,1)}, u32[]{:S(2)}, u32[]{:S(2)}) collective-permute-start(bf16[192,2048]{1,0:T(8,128)(2,1)} %collective-permute-done.5.refs_2_.refs_4_), channel_id=1, source_target_pairs={{0,4},{1,5},{2,6},{3,7},{4,0},{5,1},{6,2},{7,3},{8,12},{9,13},{10,... | collective-permute-start | bytes 2359304 | tf_op jit(solution)/shard_map/ppermute | solution.py:610
  103.3 13.5 %collective-permute-start.8 = (bf16[192,2048]{1,0:T(8,128)(2,1)}, bf16[192,2048]{1,0:T(8,128)(2,1)}, u32[]{:S(2)}, u32[]{:S(2)}) collective-permute-start(bf16[192,2048]{1,0:T(8,128)(2,1)} %collective-permute-done.7.refs_1_.refs_7_), channel_id=1, source_target_pairs={{0,4},{1,5},{2,6},{3,7},{4,0},{5,1},{6,2},{7,3},{8,12},{9,13},{10,... | collective-permute-start | bytes 2359304 | tf_op jit(solution)/shard_map/ppermute | solution.py:610
  103.4 1.0 copy-start.2
  104.4 1.0 copy-start.3
  105.5 1.0 copy-start.4
  107.1 29.5 %collective-permute-start.11 = (bf16[1536,128]{1,0:T(8,128)(2,1)S(1)}, bf16[1536,128]{1,0:T(8,128)(2,1)}, u32[]{:S(2)}, u32[]{:S(2)}) collective-permute-start(bf16[1536,128]{1,0:T(8,128)(2,1)S(1)} %shared_prep.1), channel_id=1, source_target_pairs={{0,3},{1,0},{2,1},{3,2},{4,7},{5,4},{6,5},{7,6},{8,11},{9,8},{10,9... | collective-permute-start | bytes 1179656 | tf_op jit(solution)/shard_map/ppermute | solution.py:664
  107.6 29.1 %collective-permute-start.10 = (bf16[1536,128]{1,0:T(8,128)(2,1)S(1)}, bf16[1536,128]{1,0:T(8,128)(2,1)}, u32[]{:S(2)}, u32[]{:S(2)}) collective-permute-start(bf16[1536,128]{1,0:T(8,128)(2,1)S(1)} %shared_prep.1), channel_id=1, source_target_pairs={{0,2},{1,3},{2,0},{3,1},{4,6},{5,7},{6,4},{7,5},{8,10},{9,11},{10,... | collective-permute-start | bytes 1179656 | tf_op jit(solution)/shard_map/ppermute | solution.py:664
  109.9 26.8 %collective-permute-start.9 = (bf16[1536,128]{1,0:T(8,128)(2,1)S(1)}, bf16[1536,128]{1,0:T(8,128)(2,1)}, u32[]{:S(2)}, u32[]{:S(2)}) collective-permute-start(bf16[1536,128]{1,0:T(8,128)(2,1)S(1)} %shared_prep.1), channel_id=1, source_target_pairs={{0,1},{1,2},{2,3},{3,0},{4,5},{5,6},{6,7},{7,4},{8,9},{9,10},{10,1... | collective-permute-start | bytes 1179656 | tf_op jit(solution)/shard_map/ppermute | solution.py:664
  121.6 80.3 %all-to-all-start.1 = ((bf16[128,8,1024]{2,1,0:T(8,128)(2,1)}), bf16[128,8,1024]{2,1,0:T(8,128)(2,1)}, u32[]{:S(2)}, u32[]{:S(2)}) async-start(bf16[128,8,1024]{2,1,0:T(8,128)(2,1)} %bitcast.12), calls=%async_computation.1 | async-start | bytes 4194304 | tf_op jit(solution)/shard_map/all_to_all | solution.py:649
  136.6 36.6 %copy-start.7 = (bf16[256,256]{1,0:T(8,128)(2,1)S(1)}, bf16[256,256]{1,0:T(8,128)(2,1)}, u32[]{:S(2)}) copy-start(bf16[256,256]{1,0:T(8,128)(2,1)} %k_ref.1) | copy-start | bytes 393220
  136.6 36.6 %copy-start.9 = (bf16[256,256]{1,0:T(8,128)(2,1)S(1)}, bf16[256,256]{1,0:T(8,128)(2,1)}, u32[]{:S(2)}) copy-start(bf16[256,256]{1,0:T(8,128)(2,1)} %v_ref.1) | copy-start | bytes 393220
  136.6 47.9 %copy-start.11 = (f32[2048]{0:T(1024)S(1)}, f32[2048]{0:T(1024)}, u32[]{:S(2)}) copy-start(f32[2048]{0:T(1024)} %param.22) | copy-start | bytes 24580
  136.7 47.9 %copy-start.14 = (f32[16]{0:T(128)S(1)}, f32[16]{0:T(128)}, u32[]{:S(2)}) copy-start(f32[16]{0:T(128)} %sink_ref.1) | copy-start | bytes 196
  138.1 35.1 %collective-permute-start.12 = (bf16[6144,128]{1,0:T(8,128)(2,1)S(1)}, bf16[6144,128]{1,0:T(8,128)(2,1)S(1)}, u32[]{:S(2)}, u32[]{:S(2)}) collective-permute-start(bf16[6144,128]{1,0:T(8,128)(2,1)S(1)} %pad_maximum_fusion.refs_0_), channel_id=1, source_target_pairs={{0,8},{4,28},{8,0},{12,20},{16,24},{20,12},{24,16},{28,4},{1,9},{5... | collective-permute-start | bytes 4718600 | tf_op jit(solution)/shard_map/ppermute | solution.py:669
  139.2 56.3 %collective-permute-start.13 = (bf16[6144,128]{1,0:T(8,128)(2,1)S(1)}, bf16[6144,128]{1,0:T(8,128)(2,1)}, u32[]{:S(2)}, u32[]{:S(2)}) collective-permute-start(bf16[6144,128]{1,0:T(8,128)(2,1)S(1)} %pad_maximum_fusion.refs_0_), channel_id=1, source_target_pairs={{0,4},{4,0},{1,5},{5,1},{2,6},{6,2},{3,7},{7,3},{8,12},{12,8},{9,1... | collective-permute-start | bytes 4718600 | tf_op jit(solution)/shard_map/ppermute | solution.py:670
  173.2 22.3 %collective-permute-start.14 = (bf16[6144,128]{1,0:T(8,128)(2,1)S(1)}, bf16[6144,128]{1,0:T(8,128)(2,1)}, u32[]{:S(2)}, u32[]{:S(2)}) collective-permute-start(bf16[6144,128]{1,0:T(8,128)(2,1)S(1)} %collective-permute-done.12.refs_1_), channel_id=1, source_target_pairs={{0,4},{4,0},{1,5},{5,1},{2,6},{6,2},{3,7},{7,3},{8,12},{12,8},{9,1... | collective-permute-start | bytes 4718600 | tf_op jit(solution)/shard_map/ppermute | solution.py:670
  173.2 11.3 %collective-permute-start = (bf16[2,128,256]{2,1,0:T(8,128)(2,1)S(1)}, bf16[2,128,256]{2,1,0:T(8,128)(2,1)S(1)}, u32[]{:S(2)}, u32[]{:S(2)}) collective-permute-start(bf16[2,128,256]{2,1,0:T(8,128)(2,1)S(1)} %pad_maximum_fusion.1), channel_id=1, source_target_pairs={{0,1},{1,2},{2,3},{3,4},{4,5},{5,6},{6,7},{7,8},{8,9},{9,10},{10,1... | collective-permute-start | bytes 393224 | tf_op jit(solution)/shard_map/ppermute | solution.py:56
  184.5 2.2 %copy-start.1 = (bf16[1024,2048]{1,0:T(8,128)(2,1)S(1)}, bf16[1024,2048]{1,0:T(8,128)(2,1)}, u32[]{:S(2)}) copy-start(bf16[1024,2048]{1,0:T(8,128)(2,1)} %weight_ref.1) | copy-start | bytes 12582916
  186.7 1.0 copy-start.5
  188.6 0.9 copy-start.10
  189.6 6.0 %copy-start.6 = (bf16[128,2048]{1,0:T(8,128)(2,1)S(1)}, bf16[128,2048]{1,0:T(8,128)(2,1)}, u32[]{:S(2)}) copy-start(bf16[128,2048]{1,0:T(8,128)(2,1)} %get-tuple-element.9.x_ref) | copy-start | bytes 1572868
  189.6 6.0 %copy-start.12 = (s32[128,2]{0,1:T(2,128)S(1)}, s32[128,2]{0,1:T(2,128)}, u32[]{:S(2)}) copy-start(s32[128,2]{0,1:T(2,128)} %param.25) | copy-start | bytes 3076
  189.6 6.0 %copy-start.13 = (f32[128,2]{0,1:T(2,128)S(1)}, f32[128,2]{0,1:T(2,128)}, u32[]{:S(2)}) copy-start(f32[128,2]{0,1:T(2,128)} %param.26) | copy-start | bytes 3076
  200.2 1.0 copy-start.15
  (2 other events, 1.5 us)

commit v4 on v3

--- a/solution.py
+++ b/solution.py
@@ -17,7 +17,7 @@
 BLOCK = 256
 MIB = 1 << 20
 PARTS = 4
-COMBINE_LIMIT = 62
+COMBINE_LIMIT = 16
 UP_LIMIT = 24
 DOWN_LIMIT = 16
 EP = ("z", "y", "c")
@@ -382,13 +382,14 @@
 
 
 def shared_kernel(part_ref, ids_ref, weight_ref, x_ref, *refs):
-    parts, (out_ref, columns_ref, into, down) = refs[:PARTS], refs[PARTS:]
+    most, last = refs[:PARTS], refs[PARTS : 2 * PARTS]
+    out_ref, columns_ref, into, down = refs[2 * PARTS :]
     depth = x_ref.shape[1] // PARTS
-    units = parts[0].shape[1]
-    for p, ref in enumerate(parts):
+    units = most[0].shape[1]
+    for p in range(PARTS):
         first = pl.multiple_of(part_ref[p] * depth, depth)
         for k in range(4):
-            base = 3 * k * depth
+            ref, base = (most[p], 3 * k * depth) if k < 3 else (last[p], 0)
             for m in range(2):
                 lane = (m * 4 + k) * units
                 into[pl.ds(first, depth), lane : lane + units] = ref[
@@ -405,12 +406,12 @@
     columns_ref[...] = slot_columns(ids_ref[...], weight_ref[...])
 
 
-def shared_expert(part, ids, weights, normed, parts):
+def shared_expert(part, ids, weights, normed, most, last):
     tokens, width = normed.shape
-    units = 4 * parts[0].shape[1]
+    units = 4 * most[0].shape[1]
     return pl.pallas_call(
         shared_kernel,
-        in_specs=[pl.BlockSpec(memory_space=pltpu.SMEM)] + in_vmem(3 + PARTS),
+        in_specs=[pl.BlockSpec(memory_space=pltpu.SMEM)] + in_vmem(3 + 2 * PARTS),
         out_specs=[pl.BlockSpec(memory_space=VMEM)] * 2,
         out_shape=[
             jax.ShapeDtypeStruct((tokens, width), f32),
@@ -424,22 +425,11 @@
             transcendentals=tokens * units,
         ),
         name="shared_expert",
-    )(part, ids, weights, normed, *parts)
-
-
-def combine_kernel(
-    back_ref, shared_ref, columns_ref, gain_ref, out_ref, came, common, sem, back_sems
-):
+    )(part, ids, weights, normed, *most, *last)
+
+
+def combine_kernel(back_ref, shared_ref, columns_ref, gain_ref, out_ref):
     tokens, half = out_ref.shape[0], back_ref.shape[1]
-    rows = [pl.ds(i * BLOCK, BLOCK) for i in range(back_ref.shape[0] // BLOCK)]
-    back_in = [
-        pltpu.make_async_copy(back_ref.at[at], came.at[at], back_sems.at[i])
-        for i, at in enumerate(rows)
-    ]
-    shared_in = pltpu.make_async_copy(shared_ref, common, sem)
-    for c in back_in:
-        c.start()
-    shared_in.start()
     r = iota((tokens, back_ref.shape[0]), 1)
     first = [columns_ref[:, k : k + 1].astype(jnp.int32) for k in range(2)]
     weights = [columns_ref[:, 2 + k : 3 + k] for k in range(2)]
@@ -450,14 +440,9 @@
         )
         spreads.append(spread.astype(bf16))
     spread = jnp.concatenate(spreads, axis=0)
-    summed = jnp.zeros((2 * tokens, half), f32)
-    for i, c in enumerate(back_in):
-        c.wait()
-        at = slice(i * BLOCK, (i + 1) * BLOCK)
-        summed = summed + dot(spread[:, at], came[at, :])
-    shared_in.wait()
+    summed = dot(spread, back_ref[...])
     halves = [
-        summed[h * tokens : (h + 1) * tokens] + common[:, h * half : (h + 1) * half]
+        summed[h * tokens : (h + 1) * tokens] + shared_ref[:, h * half : (h + 1) * half]
         for h in range(2)
     ]
     square = sum(jnp.sum(v * v, axis=1, keepdims=True) for v in halves)
@@ -472,15 +457,9 @@
     tokens = shared.shape[0]
     return pl.pallas_call(
         combine_kernel,
-        in_specs=[pl.BlockSpec(memory_space=ANY)] * 2 + in_vmem(2),
+        in_specs=in_vmem(4),
         out_specs=pl.BlockSpec(memory_space=VMEM),
         out_shape=jax.ShapeDtypeStruct((tokens, 2 * half), bf16),
-        scratch_shapes=[
-            VMEM((slots, half), bf16),
-            VMEM((tokens, 2 * half), f32),
-            pltpu.SemaphoreType.DMA,
-            pltpu.SemaphoreType.DMA((slots // BLOCK,)),
-        ],
         compiler_params=pltpu.CompilerParams(vmem_limit_bytes=COMBINE_LIMIT * MIB),
         cost_estimate=pl.CostEstimate(
             flops=8 * tokens * slots * half, bytes_accessed=2 * slots * half, transcendentals=0
@@ -659,17 +638,21 @@
         common_expert_up_weight,
         common_expert_down_weight,
     )
-    blocks = [prepared]
-    for k in range(1, tp):
-        blocks.append(lax.ppermute(prepared, "tp", [(i, (i + k) % tp) for i in range(tp)]))
-    quarters = [jnp.concatenate(blocks, axis=0)]
+    crossed = {}
+    for k in (1, 3, 2):
+        crossed[k] = lax.ppermute(prepared, "tp", [(i, (i + k) % tp) for i in range(tp)])
     beside = [
         (2 * i + c, 2 * ((i + 1 - 2 * ((i + c) % 2)) % ys) + c) for i in range(ys) for c in range(2)
     ]
-    quarters.append(lax.ppermute(quarters[0], ("y", "c"), beside))
-    quarters += [lax.ppermute(v, "c", [(0, 1), (1, 0)]) for v in quarters]
+
+    def spread_out(piece):
+        pair = [piece, lax.ppermute(piece, ("y", "c"), beside)]
+        return pair + [lax.ppermute(v, "c", [(0, 1), (1, 0)]) for v in pair]
+
+    most = spread_out(jnp.concatenate([prepared, crossed[1], crossed[3]], axis=0))
+    rest = spread_out(crossed[2])
     shared_sum, columns = shared_expert(
-        part, ids_t, routed_expert_weight.T, normed, quarters
+        part, ids_t, routed_expert_weight.T, normed, most, rest
     )
     experts_out = combine(returned, shared_sum, columns, moe_gain.reshape(1, -1))
     return (mixer_out, experts_out)

time: 209 us -> 217 us (1.038)
  the two profiles are of different devices: /device:TPU:8 before, /device:TPU:64 now
where the time goes in v4:
time: 217 us; the launch traced here: 216 us
  waiting for transfers between devices  135 us (62%)
  starting transfers between devices  38.4 us (18%)
  Pallas kernels  33.1 us (15%)
  local copies, waits for them, and re-layouts  7.94 us (4%)
    ppermute x8, waiting for transfers between devices, moved(): return lax.ppermute(piece, CORE_TP, route)  75.7 us
    ppermute x2, waiting for transfers between devices, spread_out(): pair = [piece, lax.ppermute(piece, ('y', 'c'), beside)]  32.2 us
    ppermute x3, waiting for transfers between devices, body(): lax.ppermute(prepared, 'tp', [(i, (i + k) % tp) for i in range(tp)])  18.8 us
    all_to_all x1, starting transfers between devices, body(): lax.all_to_all(packed.reshape(chips, 2 * CAP, -1), CHIPS, split_axis=0, c...  15.1 us
    all_to_all x1, starting transfers between devices, body(): lax.all_to_all(out.reshape(chips, 2 * CAP, -1), CHIPS, split_axis=0, conc...  12.1 us
    ppermute x1, waiting for transfers between devices, from_behind(): return lax.ppermute(block, axis, route)  8.51 us
    unnamed x32, local copies, waits for them, and re-layouts  7.94 us
    pallas_call x1, Pallas kernels, expert_up(): pl.pallas_call(up_kernel, in_specs=[pl.BlockSpec(memory_space=pltpu.SMEM)...  6.86 us
  transfers between devices with their start and end apart: 20, of which 9 were waited for; matrix products, arithmetic and copies ran while one was open for 0% of the time, Pallas kernels for 10%

profile of v4, /device:TPU:64, one launch (start us, length us, event | category | flops | bytes accessed | tf_op | source)
XLA Modules:
  0.0 216.5 jit_solution(3983624526161361590)
XLA Ops:
  0.6 4.8 %pack.1 = (bf16[1024,1024]{1,0:T(8,128)(2,1)}, bf16[128,2048]{1,0:T(8,128)(2,1)}, bf16[384,2048]{1,0:T(8,128)(2,1)}) custom-call(s32[1]{0:T(128)} %bitcast.5.expert_ref, bf16[128,2048]{1,0:T(8,128)(2,1)} %x_ref.1, f32[1,2048]{1,0:T(1,128)} %bitcast.33, s32[2,128]{1,0:T(2,128)} %bitcast.24, bf16[2,192,2048]{2,1,0:T(8,128)(2,1)} %bitcast.28, ...), custom_call_target="tpu_custom_call" | custom-call | flops 536870912 | bytes 1572864 | tf_op jit(solution)/shard_map/pack/pallas_call | solution.py:132
  5.4 15.1 %all-to-all-start = ((bf16[128,8,1024]{2,1,0:T(8,128)(2,1)}), bf16[128,8,1024]{2,1,0:T(8,128)(2,1)}, u32[]{:S(2)}, u32[]{:S(2)}) async-start(bf16[128,8,1024]{2,1,0:T(8,128)(2,1)} %bitcast.32), calls=%async_computation | async-start | bytes 4194304 | tf_op jit(solution)/shard_map/all_to_all | solution.py:606
  20.6 2.4 %pick.3 = bf16[384,2048]{1,0:T(8,128)(2,1)} custom-call(s32[1]{0:T(128)S(6)} %sub.15.expert_ref, bf16[2,192,2048]{2,1,0:T(8,128)(2,1)} %bitcast.29, bf16[2,192,2048]{2,1,0:T(8,128)(2,1)} %bitcast.31), custom_call_target="tpu_custom_call" | custom-call | flops 1000 | bytes 3145728 | tf_op jit(solution)/shard_map/pick/pallas_call | solution.py:180
  23.0 1.6 collective-permute-start.3
  24.6 53.2 %collective-permute-done.1.refs_2_.refs_4_ = bf16[384,2048]{1,0:T(8,128)(2,1)} collective-permute-done((bf16[384,2048]{1,0:T(8,128)(2,1)}, bf16[384,2048]{1,0:T(8,128)(2,1)}, u32[]{:S(2)}, u32[]{:S(2)}) %collective-permute-start.1) | collective-permute-done | bytes 1572896 | tf_op jit(solution)/shard_map/ppermute | solution.py:589
  77.8 1.0 collective-permute-done.3.refs_1_.refs_7_
  78.8 1.4 copy-done
  81.2 20.4 %collective-permute-done.5.refs_2_.refs_4_ = bf16[192,2048]{1,0:T(8,128)(2,1)} collective-permute-done((bf16[192,2048]{1,0:T(8,128)(2,1)S(1)}, bf16[192,2048]{1,0:T(8,128)(2,1)}, u32[]{:S(2)}, u32[]{:S(2)}) %collective-permute-start.5) | collective-permute-done | bytes 786464 | tf_op jit(solution)/shard_map/ppermute | solution.py:589
  101.5 1.1 collective-permute-done.7.refs_1_.refs_7_
  102.7 6.9 %expert_up.1.hidden = bf16[512,768]{1,0:T(8,128)(2,1)S(1)} custom-call(s32[1]{0:T(128)} %bitcast.4.own_ref, bf16[1024,1024]{1,0:T(8,128)(2,1)} %bitcast.11.recv, bf16[384,2048]{1,0:T(8,128)(2,1)S(1)} %collective-permute-done.2.refs_0_.refs_6_, bf16[384,2048]{1,0:T(8,128)(2,1)S(1)} %collective-permute-done.3.refs_1_.refs_7_, ...), custom_call_target="tpu_custom_call" | custom-call | flops 3221225472 | bytes 8388608 | tf_op jit(solution)/shard_map/expert_up/pallas_call | solution.py:249
  109.6 4.8 %expert_down.1 = bf16[1024,1024]{1,0:T(8,128)(2,1)} custom-call(s32[1]{0:T(128)} %bitcast.4.own_ref, bf16[512,768]{1,0:T(8,128)(2,1)S(1)} %expert_up.1.hidden, bf16[192,2048]{1,0:T(8,128)(2,1)} %collective-permute-done.6.refs_0_.refs_6_, bf16[192,2048]{1,0:T(8,128)(2,1)} %collective-permute-done.7.refs_1_.refs_7_, ...), custom_call_target="tpu_custom_call" | custom-call | flops 1610612736 | bytes 6029312 | tf_op jit(solution)/shard_map/expert_down/pallas_call | solution.py:322
  114.4 12.1 %all-to-all-start.1 = ((bf16[128,8,1024]{2,1,0:T(8,128)(2,1)}), bf16[128,8,1024]{2,1,0:T(8,128)(2,1)S(1)}, u32[]{:S(2)}, u32[]{:S(2)}) async-start(bf16[128,8,1024]{2,1,0:T(8,128)(2,1)} %bitcast.12), calls=%async_computation.1 | async-start | bytes 4194304 | tf_op jit(solution)/shard_map/all_to_all | solution.py:628
  126.5 1.0 copy-done.4
  127.6 0.6 shared_prep.1
  128.2 2.8 %collective-permute-start.10 = (bf16[1536,128]{1,0:T(8,128)(2,1)S(1)}, bf16[1536,128]{1,0:T(8,128)(2,1)S(1)}, u32[]{:S(2)}, u32[]{:S(2)}) collective-permute-start(bf16[1536,128]{1,0:T(8,128)(2,1)S(1)} %shared_prep.1), channel_id=1, source_target_pairs={{0,3},{1,0},{2,1},{3,2},{4,7},{5,4},{6,5},{7,6},{8,11},{9,8},{10,9... | collective-permute-start | bytes 1179656 | tf_op jit(solution)/shard_map/ppermute | solution.py:643
  131.0 16.9 %collective-permute-done.10 = bf16[1536,128]{1,0:T(8,128)(2,1)S(1)} collective-permute-done((bf16[1536,128]{1,0:T(8,128)(2,1)S(1)}, bf16[1536,128]{1,0:T(8,128)(2,1)S(1)}, u32[]{:S(2)}, u32[]{:S(2)}) %collective-permute-start.10) | collective-permute-done | bytes 393248 | tf_op jit(solution)/shard_map/ppermute | solution.py:643
  147.9 1.9 collective-permute-done.9
  149.9 1.1 collective-permute-start.11
  151.2 1.1 collective-permute-start.12
  152.3 25.0 %collective-permute-done.11.refs_1_ = bf16[4608,128]{1,0:T(8,128)(2,1)} collective-permute-done((bf16[4608,128]{1,0:T(8,128)(2,1)S(1)}, bf16[4608,128]{1,0:T(8,128)(2,1)}, u32[]{:S(2)}, u32[]{:S(2)}) %collective-permute-start.11) | collective-permute-done | bytes 1179680 | tf_op jit(solution)/shard_map/ppermute | solution.py:649
  177.3 0.9 collective-permute-start.16
  178.2 7.2 %collective-permute-done.15.refs_5_ = bf16[1536,128]{1,0:T(8,128)(2,1)} collective-permute-done((bf16[1536,128]{1,0:T(8,128)(2,1)}, bf16[1536,128]{1,0:T(8,128)(2,1)}, u32[]{:S(2)}, u32[]{:S(2)}) %collective-permute-start.15) | collective-permute-done | bytes 393248 | tf_op jit(solution)/shard_map/ppermute | solution.py:649
  186.0 0.7 pad_maximum_fusion.1
  186.6 2.3 %collective-permute-start = (bf16[2,128,256]{2,1,0:T(8,128)(2,1)}, bf16[2,128,256]{2,1,0:T(8,128)(2,1)}, u32[]{:S(2)}, u32[]{:S(2)}) collective-permute-start(bf16[2,128,256]{2,1,0:T(8,128)(2,1)} %pad_maximum_fusion.1), channel_id=1, source_target_pairs={{0,1},{1,2},{2,3},{3,4},{4,5},{5,6},{6,7},{7,8},{8,9},{9,10},{10,1... | collective-permute-start | bytes 393224 | tf_op jit(solution)/shard_map/ppermute | solution.py:56
  188.9 8.5 %collective-permute-done.rim_ref = bf16[2,128,256]{2,1,0:T(8,128)(2,1)} collective-permute-done((bf16[2,128,256]{2,1,0:T(8,128)(2,1)}, bf16[2,128,256]{2,1,0:T(8,128)(2,1)}, u32[]{:S(2)}, u32[]{:S(2)}) %collective-permute-start) | collective-permute-done | bytes 131104 | tf_op jit(solution)/shard_map/ppermute | solution.py:56
  197.5 2.2 %copy-done.1 = bf16[1024,2048]{1,0:T(8,128)(2,1)S(1)} copy-done((bf16[1024,2048]{1,0:T(8,128)(2,1)S(1)}, bf16[1024,2048]{1,0:T(8,128)(2,1)}, u32[]{:S(2)}) %copy-start.1) | copy-done | bytes 4194328
  199.6 1.0 copy-done.5
  200.7 6.4 %attention.1 = bf16[256,2048]{1,0:T(8,128)(2,1)} custom-call(s32[1]{0:T(128)} %bitcast.first_ref, f32[16]{0:T(128)S(1)} %copy-done.12, bf16[256,1024]{1,0:T(8,128)(2,1)S(1)} %copy-done.5, bf16[256,256]{1,0:T(8,128)(2,1)S(1)} %copy-done.7, bf16[256,256]{1,0:T(8,128)(2,1)S(1)} %copy-done.8, bf16[2,128,256]{2,1,0:T(8,128)(2,1)} %collective-permute-done.rim_ref, ...), custom_call_target="tpu_custom_call" | custom-call | flops 1610612736 | bytes 6291456 | tf_op jit(solution)/shard_map/attention/pallas_call | solution.py:529
  207.2 5.2 %shared_expert.1 = (f32[128,2048]{1,0:T(8,128)S(1)}, f32[128,128]{1,0:T(8,128)S(1)}) custom-call(s32[4]{0:T(128)S(1)} %pad_add_fusion.part_ref, s32[2,128]{1,0:T(2,128)S(1)} %bitcast.25, f32[2,128]{1,0:T(2,128)S(1)} %bitcast.26, bf16[128,2048]{1,0:T(8,128)(2,1)S(1)} %copy-done.6, bf16[4608,128]{1,0:T(8,128)(2,1)S(1)} %pad_maximum_fusion.refs_0_, ...), custom_call_target="tpu_custom_call" | custom-call | flops 805306368 | bytes 6291456 | tf_op jit(solution)/shard_map/shared_expert/pallas_call | solution.py:412
  212.5 1.0 copy-done.13
  213.4 1.2 copy-done.14
  214.7 1.8 combine.1
  (53 shorter events, 2.1 us)
Async XLA Ops:
  5.4 97.3 %all-to-all-start = ((bf16[128,8,1024]{2,1,0:T(8,128)(2,1)}), bf16[128,8,1024]{2,1,0:T(8,128)(2,1)}, u32[]{:S(2)}, u32[]{:S(2)}) async-start(bf16[128,8,1024]{2,1,0:T(8,128)(2,1)} %bitcast.32), calls=%async_computation | async-start | bytes 4194304 | tf_op jit(solution)/shard_map/all_to_all | solution.py:606
  20.5 57.2 %collective-permute-start.1 = (bf16[384,2048]{1,0:T(8,128)(2,1)}, bf16[384,2048]{1,0:T(8,128)(2,1)}, u32[]{:S(2)}, u32[]{:S(2)}) collective-permute-start(bf16[384,2048]{1,0:T(8,128)(2,1)} %get-tuple-element.8), channel_id=1, source_target_pairs={{2,0},{0,4},{3,1},{1,5},{4,6},{6,2},{5,7},{7,3},{10,8},{8,12},{11,... | collective-permute-start | bytes 4718600 | tf_op jit(solution)/shard_map/ppermute | solution.py:589
  23.0 55.8 %collective-permute-start.3 = (bf16[384,2048]{1,0:T(8,128)(2,1)}, bf16[384,2048]{1,0:T(8,128)(2,1)S(1)}, u32[]{:S(2)}, u32[]{:S(2)}) collective-permute-start(bf16[384,2048]{1,0:T(8,128)(2,1)} %pick.3), channel_id=1, source_target_pairs={{3,0},{1,4},{0,1},{2,5},{5,6},{7,2},{6,7},{4,3},{11,8},{9,12},{8,9... | collective-permute-start | bytes 4718600 | tf_op jit(solution)/shard_map/ppermute | solution.py:589
  77.8 24.9 %collective-permute-start.2 = (bf16[384,2048]{1,0:T(8,128)(2,1)}, bf16[384,2048]{1,0:T(8,128)(2,1)S(1)}, u32[]{:S(2)}, u32[]{:S(2)}) collective-permute-start(bf16[384,2048]{1,0:T(8,128)(2,1)} %collective-permute-done.1.refs_2_.refs_4_), channel_id=1, source_target_pairs={{0,4},{1,5},{2,6},{3,7},{4,0},{5,1},{6,2},{7,3},{8,12},{9,13},{10,... | collective-permute-start | bytes 4718600 | tf_op jit(solution)/shard_map/ppermute | solution.py:589
  78.8 23.9 %collective-permute-start.4 = (bf16[384,2048]{1,0:T(8,128)(2,1)S(1)}, bf16[384,2048]{1,0:T(8,128)(2,1)}, u32[]{:S(2)}, u32[]{:S(2)}) collective-permute-start(bf16[384,2048]{1,0:T(8,128)(2,1)S(1)} %collective-permute-done.3.refs_1_.refs_7_), channel_id=1, source_target_pairs={{0,4},{1,5},{2,6},{3,7},{4,0},{5,1},{6,2},{7,3},{8,12},{9,13},{10,... | collective-permute-start | bytes 4718600 | tf_op jit(solution)/shard_map/ppermute | solution.py:589
  78.8 1.4 copy-start
  80.3 21.2 %collective-permute-start.5 = (bf16[192,2048]{1,0:T(8,128)(2,1)S(1)}, bf16[192,2048]{1,0:T(8,128)(2,1)}, u32[]{:S(2)}, u32[]{:S(2)}) collective-permute-start(bf16[192,2048]{1,0:T(8,128)(2,1)S(1)} %pick.4), channel_id=1, source_target_pairs={{2,0},{0,4},{3,1},{1,5},{4,6},{6,2},{5,7},{7,3},{10,8},{8,12},{11,... | collective-permute-start | bytes 2359304 | tf_op jit(solution)/shard_map/ppermute | solution.py:589
  81.1 21.6 %collective-permute-start.7 = (bf16[192,2048]{1,0:T(8,128)(2,1)S(1)}, bf16[192,2048]{1,0:T(8,128)(2,1)}, u32[]{:S(2)}, u32[]{:S(2)}) collective-permute-start(bf16[192,2048]{1,0:T(8,128)(2,1)S(1)} %pick.5), channel_id=1, source_target_pairs={{3,0},{1,4},{0,1},{2,5},{5,6},{7,2},{6,7},{4,3},{11,8},{9,12},{8,9... | collective-permute-start | bytes 2359304 | tf_op jit(solution)/shard_map/ppermute | solution.py:589
  101.5 8.0 %collective-permute-start.6 = (bf16[192,2048]{1,0:T(8,128)(2,1)}, bf16[192,2048]{1,0:T(8,128)(2,1)}, u32[]{:S(2)}, u32[]{:S(2)}) collective-permute-start(bf16[192,2048]{1,0:T(8,128)(2,1)} %collective-permute-done.5.refs_2_.refs_4_), channel_id=1, source_target_pairs={{0,4},{1,5},{2,6},{3,7},{4,0},{5,1},{6,2},{7,3},{8,12},{9,13},{10,... | collective-permute-start | bytes 2359304 | tf_op jit(solution)/shard_map/ppermute | solution.py:589
  102.7 6.9 %collective-permute-start.8 = (bf16[192,2048]{1,0:T(8,128)(2,1)}, bf16[192,2048]{1,0:T(8,128)(2,1)}, u32[]{:S(2)}, u32[]{:S(2)}) collective-permute-start(bf16[192,2048]{1,0:T(8,128)(2,1)} %collective-permute-done.7.refs_1_.refs_7_), channel_id=1, source_target_pairs={{0,4},{1,5},{2,6},{3,7},{4,0},{5,1},{6,2},{7,3},{8,12},{9,13},{10,... | collective-permute-start | bytes 2359304 | tf_op jit(solution)/shard_map/ppermute | solution.py:589
  114.4 12.2 %copy-start.2 = (bf16[2048,128]{1,0:T(8,128)(2,1)S(1)}, bf16[2048,128]{1,0:T(8,128)(2,1)}, u32[]{:S(2)}) copy-start(bf16[2048,128]{1,0:T(8,128)(2,1)} %gate_ref.1) | copy-start | bytes 1572868
  114.4 12.2 %copy-start.3 = (bf16[2048,128]{1,0:T(8,128)(2,1)S(1)}, bf16[2048,128]{1,0:T(8,128)(2,1)}, u32[]{:S(2)}) copy-start(bf16[2048,128]{1,0:T(8,128)(2,1)} %up_ref.1) | copy-start | bytes 1572868
  114.4 99.1 %all-to-all-start.1 = ((bf16[128,8,1024]{2,1,0:T(8,128)(2,1)}), bf16[128,8,1024]{2,1,0:T(8,128)(2,1)S(1)}, u32[]{:S(2)}, u32[]{:S(2)}) async-start(bf16[128,8,1024]{2,1,0:T(8,128)(2,1)} %bitcast.12), calls=%async_computation.1 | async-start | bytes 4194304 | tf_op jit(solution)/shard_map/all_to_all | solution.py:628
  128.2 57.8 %copy-start.7 = (bf16[256,256]{1,0:T(8,128)(2,1)S(1)}, bf16[256,256]{1,0:T(8,128)(2,1)}, u32[]{:S(2)}) copy-start(bf16[256,256]{1,0:T(8,128)(2,1)} %k_ref.1) | copy-start | bytes 393220
  128.2 57.8 %copy-start.8 = (bf16[256,256]{1,0:T(8,128)(2,1)S(1)}, bf16[256,256]{1,0:T(8,128)(2,1)}, u32[]{:S(2)}) copy-start(bf16[256,256]{1,0:T(8,128)(2,1)} %v_ref.1) | copy-start | bytes 393220
  128.2 69.2 %copy-start.9 = (f32[2048]{0:T(1024)S(1)}, f32[2048]{0:T(1024)}, u32[]{:S(2)}) copy-start(f32[2048]{0:T(1024)} %param.22) | copy-start | bytes 24580
  128.2 69.2 %copy-start.12 = (f32[16]{0:T(128)S(1)}, f32[16]{0:T(128)}, u32[]{:S(2)}) copy-start(f32[16]{0:T(128)} %sink_ref.1) | copy-start | bytes 196
  128.2 19.7 %collective-permute-start.10 = (bf16[1536,128]{1,0:T(8,128)(2,1)S(1)}, bf16[1536,128]{1,0:T(8,128)(2,1)S(1)}, u32[]{:S(2)}, u32[]{:S(2)}) collective-permute-start(bf16[1536,128]{1,0:T(8,128)(2,1)S(1)} %shared_prep.1), channel_id=1, source_target_pairs={{0,3},{1,0},{2,1},{3,2},{4,7},{5,4},{6,5},{7,6},{8,11},{9,8},{10,9... | collective-permute-start | bytes 1179656 | tf_op jit(solution)/shard_map/ppermute | solution.py:643
  131.0 18.8 %collective-permute-start.9 = (bf16[1536,128]{1,0:T(8,128)(2,1)S(1)}, bf16[1536,128]{1,0:T(8,128)(2,1)S(1)}, u32[]{:S(2)}, u32[]{:S(2)}) collective-permute-start(bf16[1536,128]{1,0:T(8,128)(2,1)S(1)} %shared_prep.1), channel_id=1, source_target_pairs={{0,1},{1,2},{2,3},{3,0},{4,5},{5,6},{6,7},{7,4},{8,9},{9,10},{10,1... | collective-permute-start | bytes 1179656 | tf_op jit(solution)/shard_map/ppermute | solution.py:643
  149.9 27.4 %collective-permute-start.11 = (bf16[4608,128]{1,0:T(8,128)(2,1)S(1)}, bf16[4608,128]{1,0:T(8,128)(2,1)}, u32[]{:S(2)}, u32[]{:S(2)}) collective-permute-start(bf16[4608,128]{1,0:T(8,128)(2,1)S(1)} %pad_maximum_fusion.refs_0_), channel_id=1, source_target_pairs={{0,8},{4,28},{8,0},{12,20},{16,24},{20,12},{24,16},{28,4},{1,9},{5... | collective-permute-start | bytes 3538952 | tf_op jit(solution)/shard_map/ppermute | solution.py:649
  151.0 26.3 %collective-permute-start.14 = (bf16[1536,128]{1,0:T(8,128)(2,1)S(1)}, bf16[1536,128]{1,0:T(8,128)(2,1)}, u32[]{:S(2)}, u32[]{:S(2)}) collective-permute-start(bf16[1536,128]{1,0:T(8,128)(2,1)S(1)} %shared_prep.1), channel_id=1, source_target_pairs={{0,2},{1,3},{2,0},{3,1},{4,6},{5,7},{6,4},{7,5},{8,10},{9,11},{10,... | collective-permute-start | bytes 1179656 | tf_op jit(solution)/shard_map/ppermute | solution.py:643
  151.2 56.0 %collective-permute-start.12 = (bf16[4608,128]{1,0:T(8,128)(2,1)S(1)}, bf16[4608,128]{1,0:T(8,128)(2,1)}, u32[]{:S(2)}, u32[]{:S(2)}) collective-permute-start(bf16[4608,128]{1,0:T(8,128)(2,1)S(1)} %pad_maximum_fusion.refs_0_), channel_id=1, source_target_pairs={{0,4},{4,0},{1,5},{5,1},{2,6},{6,2},{3,7},{7,3},{8,12},{12,8},{9,1... | collective-permute-start | bytes 3538952 | tf_op jit(solution)/shard_map/ppermute | solution.py:650
  177.3 29.9 %collective-permute-start.13 = (bf16[4608,128]{1,0:T(8,128)(2,1)}, bf16[4608,128]{1,0:T(8,128)(2,1)}, u32[]{:S(2)}, u32[]{:S(2)}) collective-permute-start(bf16[4608,128]{1,0:T(8,128)(2,1)} %collective-permute-done.11.refs_1_), channel_id=1, source_target_pairs={{0,4},{4,0},{1,5},{5,1},{2,6},{6,2},{3,7},{7,3},{8,12},{12,8},{9,1... | collective-permute-start | bytes 3538952 | tf_op jit(solution)/shard_map/ppermute | solution.py:650
  177.3 8.1 %collective-permute-start.15 = (bf16[1536,128]{1,0:T(8,128)(2,1)}, bf16[1536,128]{1,0:T(8,128)(2,1)}, u32[]{:S(2)}, u32[]{:S(2)}) collective-permute-start(bf16[1536,128]{1,0:T(8,128)(2,1)} %collective-permute-done.14.refs_4_), channel_id=1, source_target_pairs={{0,8},{4,28},{8,0},{12,20},{16,24},{20,12},{24,16},{28,4},{1,9},{5... | collective-permute-start | bytes 1179656 | tf_op jit(solution)/shard_map/ppermute | solution.py:649
  177.3 29.8 %collective-permute-start.16 = (bf16[1536,128]{1,0:T(8,128)(2,1)}, bf16[1536,128]{1,0:T(8,128)(2,1)}, u32[]{:S(2)}, u32[]{:S(2)}) collective-permute-start(bf16[1536,128]{1,0:T(8,128)(2,1)} %collective-permute-done.14.refs_4_), channel_id=1, source_target_pairs={{0,4},{4,0},{1,5},{5,1},{2,6},{6,2},{3,7},{7,3},{8,12},{12,8},{9,1... | collective-permute-start | bytes 1179656 | tf_op jit(solution)/shard_map/ppermute | solution.py:650
  185.4 21.7 %collective-permute-start.17 = (bf16[1536,128]{1,0:T(8,128)(2,1)}, bf16[1536,128]{1,0:T(8,128)(2,1)}, u32[]{:S(2)}, u32[]{:S(2)}) collective-permute-start(bf16[1536,128]{1,0:T(8,128)(2,1)} %collective-permute-done.15.refs_5_), channel_id=1, source_target_pairs={{0,4},{4,0},{1,5},{5,1},{2,6},{6,2},{3,7},{7,3},{8,12},{12,8},{9,1... | collective-permute-start | bytes 1179656 | tf_op jit(solution)/shard_map/ppermute | solution.py:650
  186.6 10.8 %collective-permute-start = (bf16[2,128,256]{2,1,0:T(8,128)(2,1)}, bf16[2,128,256]{2,1,0:T(8,128)(2,1)}, u32[]{:S(2)}, u32[]{:S(2)}) collective-permute-start(bf16[2,128,256]{2,1,0:T(8,128)(2,1)} %pad_maximum_fusion.1), channel_id=1, source_target_pairs={{0,1},{1,2},{2,3},{3,4},{4,5},{5,6},{6,7},{7,8},{8,9},{9,10},{10,1... | collective-permute-start | bytes 393224 | tf_op jit(solution)/shard_map/ppermute | solution.py:56
  197.5 2.2 %copy-start.1 = (bf16[1024,2048]{1,0:T(8,128)(2,1)S(1)}, bf16[1024,2048]{1,0:T(8,128)(2,1)}, u32[]{:S(2)}) copy-start(bf16[1024,2048]{1,0:T(8,128)(2,1)} %weight_ref.1) | copy-start | bytes 12582916
  200.7 6.5 %copy-start.6 = (bf16[128,2048]{1,0:T(8,128)(2,1)S(1)}, bf16[128,2048]{1,0:T(8,128)(2,1)}, u32[]{:S(2)}) copy-start(bf16[128,2048]{1,0:T(8,128)(2,1)} %get-tuple-element.9.x_ref) | copy-start | bytes 1572868
  200.7 6.5 %copy-start.10 = (s32[128,2]{0,1:T(2,128)S(1)}, s32[128,2]{0,1:T(2,128)}, u32[]{:S(2)}) copy-start(s32[128,2]{0,1:T(2,128)} %param.25) | copy-start | bytes 3076
  200.7 6.5 %copy-start.11 = (f32[128,2]{0,1:T(2,128)S(1)}, f32[128,2]{0,1:T(2,128)}, u32[]{:S(2)}) copy-start(f32[128,2]{0,1:T(2,128)} %param.26) | copy-start | bytes 3076
  207.2 6.2 %copy-start.15 = (f32[2048]{0:T(1024)S(1)}, f32[2048]{0:T(1024)}, u32[]{:S(2)}) copy-start(f32[2048]{0:T(1024)} %param.33) | copy-start | bytes 24580
  (4 other events, 4.3 us)

commit v5 on v4

--- a/solution.py
+++ b/solution.py
@@ -22,7 +22,7 @@
 DOWN_LIMIT = 16
 EP = ("z", "y", "c")
 EP_TP = ("z", "y", "c", "tp")
-CHIPS = ("z", "y", "tp")
+CHIPS = ("tp", "z", "y")
 CORE_TP = ("c", "tp")
 EPS = 1e-06
 NEGATIVE = -1e30
@@ -59,6 +59,10 @@
 def rms_scale(inputs, gain_vec):
     mean_sq = jnp.mean(inputs * inputs, axis=-1, keepdims=True)
     return inputs * lax.rsqrt(mean_sq + EPS) * gain_vec
+
+
+def chip_index(ids):
+    return (ids & 3) * 32 + (ids >> 4) * 4 + ((ids >> 2) & 3)
 
 
 def slot_rows(ids, lanes):
@@ -95,7 +99,7 @@
     normed_ref[...] = normed
     stacked[:tokens, :] = normed[:, :half]
     stacked[tokens:, :] = normed[:, half:]
-    rows = slot_rows(ids_ref[...].astype(f32), True)
+    rows = slot_rows(chip_index(ids_ref[...]).astype(f32), True)
     size = made.shape[0] // block_sems.shape[0]
     blocks = []
     for i in range(block_sems.shape[0]):
@@ -370,7 +374,7 @@
 
 def slot_columns(ids, weights):
     tokens = ids.shape[1]
-    first = slot_rows(ids.astype(f32), False)
+    first = slot_rows(chip_index(ids).astype(f32), False)
     eye = iota((tokens, tokens), 0) == iota((tokens, tokens), 1)
     lane = iota((tokens, 128), 1)
     out = jnp.zeros((tokens, 128), f32)

time: 217 us -> 217 us (level)
  the two profiles are of different devices: /device:TPU:64 before, /device:TPU:8 now
where the time goes in v5:
time: 217 us; the launch traced here: 213 us
  waiting for transfers between devices  131 us (60%)
  starting transfers between devices  39.8 us (18%)
  Pallas kernels  33.1 us (15%)
  local copies, waits for them, and re-layouts  7.94 us (4%)
    ppermute x8, waiting for transfers between devices, moved(): return lax.ppermute(piece, CORE_TP, route)  75.8 us
    ppermute x2, waiting for transfers between devices, spread_out(): pair = [piece, lax.ppermute(piece, ('y', 'c'), beside)]  29.7 us
    ppermute x3, waiting for transfers between devices, body(): lax.ppermute(prepared, 'tp', [(i, (i + k) % tp) for i in range(tp)])  17.7 us
    all_to_all x1, starting transfers between devices, body(): lax.all_to_all(packed.reshape(chips, 2 * CAP, -1), CHIPS, split_axis=0, c...  15.8 us
    all_to_all x1, starting transfers between devices, body(): lax.all_to_all(out.reshape(chips, 2 * CAP, -1), CHIPS, split_axis=0, conc...  11.9 us
    unnamed x32, local copies, waits for them, and re-layouts  7.94 us
    ppermute x1, waiting for transfers between devices, from_behind(): return lax.ppermute(block, axis, route)  7.54 us
    pallas_call x1, Pallas kernels, expert_up(): pl.pallas_call(up_kernel, in_specs=[pl.BlockSpec(memory_space=pltpu.SMEM)...  6.86 us
  transfers between devices with their start and end apart: 20, of which 9 were waited for; matrix products, arithmetic and copies ran while one was open for 0% of the time, Pallas kernels for 10%

profile of v5, /device:TPU:8, one launch (start us, length us, event | category | flops | bytes accessed | tf_op | source)
XLA Modules:
  0.0 213.4 jit_solution(15023220393591877966)
XLA Ops:
  0.6 4.8 %pack.1 = (bf16[1024,1024]{1,0:T(8,128)(2,1)}, bf16[128,2048]{1,0:T(8,128)(2,1)}, bf16[384,2048]{1,0:T(8,128)(2,1)}) custom-call(s32[1]{0:T(128)} %bitcast.5.expert_ref, bf16[128,2048]{1,0:T(8,128)(2,1)} %x_ref.1, f32[1,2048]{1,0:T(1,128)} %bitcast.33, s32[2,128]{1,0:T(2,128)} %bitcast.24, bf16[2,192,2048]{2,1,0:T(8,128)(2,1)} %bitcast.28, ...), custom_call_target="tpu_custom_call" | custom-call | flops 536870912 | bytes 1572864 | tf_op jit(solution)/shard_map/pack/pallas_call | solution.py:136
  5.4 15.8 %all-to-all-start = ((bf16[128,8,1024]{2,1,0:T(8,128)(2,1)}), bf16[128,8,1024]{2,1,0:T(8,128)(2,1)}, u32[]{:S(2)}, u32[]{:S(2)}) async-start(bf16[128,8,1024]{2,1,0:T(8,128)(2,1)} %bitcast.32), calls=%async_computation | async-start | bytes 4194304 | tf_op jit(solution)/shard_map/all_to_all | solution.py:610
  21.3 2.4 %pick.3 = bf16[384,2048]{1,0:T(8,128)(2,1)} custom-call(s32[1]{0:T(128)S(6)} %sub.15.expert_ref, bf16[2,192,2048]{2,1,0:T(8,128)(2,1)} %bitcast.29, bf16[2,192,2048]{2,1,0:T(8,128)(2,1)} %bitcast.31), custom_call_target="tpu_custom_call" | custom-call | flops 1000 | bytes 3145728 | tf_op jit(solution)/shard_map/pick/pallas_call | solution.py:184
  23.7 1.7 collective-permute-start.3
  25.4 53.0 %collective-permute-done.1.refs_2_.refs_4_ = bf16[384,2048]{1,0:T(8,128)(2,1)} collective-permute-done((bf16[384,2048]{1,0:T(8,128)(2,1)}, bf16[384,2048]{1,0:T(8,128)(2,1)}, u32[]{:S(2)}, u32[]{:S(2)}) %collective-permute-start.1) | collective-permute-done | bytes 1572896 | tf_op jit(solution)/shard_map/ppermute | solution.py:593
  78.4 1.4 collective-permute-done.3.refs_1_.refs_7_
  79.8 1.4 copy-done
  82.2 19.9 %collective-permute-done.5.refs_2_.refs_4_ = bf16[192,2048]{1,0:T(8,128)(2,1)} collective-permute-done((bf16[192,2048]{1,0:T(8,128)(2,1)S(1)}, bf16[192,2048]{1,0:T(8,128)(2,1)}, u32[]{:S(2)}, u32[]{:S(2)}) %collective-permute-start.5) | collective-permute-done | bytes 786464 | tf_op jit(solution)/shard_map/ppermute | solution.py:593
  102.2 1.4 collective-permute-done.7.refs_1_.refs_7_
  103.7 6.9 %expert_up.1.hidden = bf16[512,768]{1,0:T(8,128)(2,1)S(1)} custom-call(s32[1]{0:T(128)} %bitcast.4.own_ref, bf16[1024,1024]{1,0:T(8,128)(2,1)} %bitcast.11.recv, bf16[384,2048]{1,0:T(8,128)(2,1)S(1)} %collective-permute-done.2.refs_0_.refs_6_, bf16[384,2048]{1,0:T(8,128)(2,1)S(1)} %collective-permute-done.3.refs_1_.refs_7_, ...), custom_call_target="tpu_custom_call" | custom-call | flops 3221225472 | bytes 8388608 | tf_op jit(solution)/shard_map/expert_up/pallas_call | solution.py:253
  110.6 4.8 %expert_down.1 = bf16[1024,1024]{1,0:T(8,128)(2,1)} custom-call(s32[1]{0:T(128)} %bitcast.4.own_ref, bf16[512,768]{1,0:T(8,128)(2,1)S(1)} %expert_up.1.hidden, bf16[192,2048]{1,0:T(8,128)(2,1)} %collective-permute-done.6.refs_0_.refs_6_, bf16[192,2048]{1,0:T(8,128)(2,1)} %collective-permute-done.7.refs_1_.refs_7_, ...), custom_call_target="tpu_custom_call" | custom-call | flops 1610612736 | bytes 6029312 | tf_op jit(solution)/shard_map/expert_down/pallas_call | solution.py:326
  115.4 11.9 %all-to-all-start.1 = ((bf16[128,8,1024]{2,1,0:T(8,128)(2,1)}), bf16[128,8,1024]{2,1,0:T(8,128)(2,1)S(1)}, u32[]{:S(2)}, u32[]{:S(2)}) async-start(bf16[128,8,1024]{2,1,0:T(8,128)(2,1)} %bitcast.12), calls=%async_computation.1 | async-start | bytes 4194304 | tf_op jit(solution)/shard_map/all_to_all | solution.py:632
  127.4 1.0 copy-done.4
  129.1 3.3 %collective-permute-start.10 = (bf16[1536,128]{1,0:T(8,128)(2,1)S(1)}, bf16[1536,128]{1,0:T(8,128)(2,1)S(1)}, u32[]{:S(2)}, u32[]{:S(2)}) collective-permute-start(bf16[1536,128]{1,0:T(8,128)(2,1)S(1)} %shared_prep.1), channel_id=1, source_target_pairs={{0,3},{1,0},{2,1},{3,2},{4,7},{5,4},{6,5},{7,6},{8,11},{9,8},{10,9... | collective-permute-start | bytes 1179656 | tf_op jit(solution)/shard_map/ppermute | solution.py:647
  132.4 15.3 %collective-permute-done.10 = bf16[1536,128]{1,0:T(8,128)(2,1)S(1)} collective-permute-done((bf16[1536,128]{1,0:T(8,128)(2,1)S(1)}, bf16[1536,128]{1,0:T(8,128)(2,1)S(1)}, u32[]{:S(2)}, u32[]{:S(2)}) %collective-permute-start.10) | collective-permute-done | bytes 393248 | tf_op jit(solution)/shard_map/ppermute | solution.py:647
  147.7 2.4 %collective-permute-done.9 = bf16[1536,128]{1,0:T(8,128)(2,1)S(1)} collective-permute-done((bf16[1536,128]{1,0:T(8,128)(2,1)S(1)}, bf16[1536,128]{1,0:T(8,128)(2,1)S(1)}, u32[]{:S(2)}, u32[]{:S(2)}) %collective-permute-start.9) | collective-permute-done | bytes 393248 | tf_op jit(solution)/shard_map/ppermute | solution.py:647
  150.2 1.1 collective-permute-start.11
  151.2 0.8 collective-permute-start.14
  152.1 23.9 %collective-permute-done.11.refs_1_ = bf16[4608,128]{1,0:T(8,128)(2,1)} collective-permute-done((bf16[4608,128]{1,0:T(8,128)(2,1)S(1)}, bf16[4608,128]{1,0:T(8,128)(2,1)}, u32[]{:S(2)}, u32[]{:S(2)}) %collective-permute-start.11) | collective-permute-done | bytes 1179680 | tf_op jit(solution)/shard_map/ppermute | solution.py:653
  176.0 1.0 collective-permute-start.15
  177.0 1.2 collective-permute-start.16
  178.2 5.9 %collective-permute-done.15.refs_5_ = bf16[1536,128]{1,0:T(8,128)(2,1)} collective-permute-done((bf16[1536,128]{1,0:T(8,128)(2,1)}, bf16[1536,128]{1,0:T(8,128)(2,1)}, u32[]{:S(2)}, u32[]{:S(2)}) %collective-permute-start.15) | collective-permute-done | bytes 393248 | tf_op jit(solution)/shard_map/ppermute | solution.py:653
  184.1 0.7 pad_maximum_fusion.1
  184.7 2.1 collective-permute-start
  186.9 7.5 %collective-permute-done.rim_ref = bf16[2,128,256]{2,1,0:T(8,128)(2,1)} collective-permute-done((bf16[2,128,256]{2,1,0:T(8,128)(2,1)}, bf16[2,128,256]{2,1,0:T(8,128)(2,1)}, u32[]{:S(2)}, u32[]{:S(2)}) %collective-permute-start) | collective-permute-done | bytes 131104 | tf_op jit(solution)/shard_map/ppermute | solution.py:56
  194.4 2.2 %copy-done.1 = bf16[1024,2048]{1,0:T(8,128)(2,1)S(1)} copy-done((bf16[1024,2048]{1,0:T(8,128)(2,1)S(1)}, bf16[1024,2048]{1,0:T(8,128)(2,1)}, u32[]{:S(2)}) %copy-start.1) | copy-done | bytes 4194328
  196.6 1.0 copy-done.5
  197.7 6.4 %attention.1 = bf16[256,2048]{1,0:T(8,128)(2,1)} custom-call(s32[1]{0:T(128)} %bitcast.first_ref, f32[16]{0:T(128)S(1)} %copy-done.12, bf16[256,1024]{1,0:T(8,128)(2,1)S(1)} %copy-done.5, bf16[256,256]{1,0:T(8,128)(2,1)S(1)} %copy-done.7, bf16[256,256]{1,0:T(8,128)(2,1)S(1)} %copy-done.8, bf16[2,128,256]{2,1,0:T(8,128)(2,1)} %collective-permute-done.rim_ref, ...), custom_call_target="tpu_custom_call" | custom-call | flops 1610612736 | bytes 6291456 | tf_op jit(solution)/shard_map/attention/pallas_call | solution.py:533
  204.2 5.2 %shared_expert.1 = (f32[128,2048]{1,0:T(8,128)S(1)}, f32[128,128]{1,0:T(8,128)S(1)}) custom-call(s32[4]{0:T(128)S(1)} %pad_add_fusion.part_ref, s32[2,128]{1,0:T(2,128)S(1)} %bitcast.25, f32[2,128]{1,0:T(2,128)S(1)} %bitcast.26, bf16[128,2048]{1,0:T(8,128)(2,1)S(1)} %copy-done.6, bf16[4608,128]{1,0:T(8,128)(2,1)S(1)} %pad_maximum_fusion.refs_0_, ...), custom_call_target="tpu_custom_call" | custom-call | flops 805306368 | bytes 6291456 | tf_op jit(solution)/shard_map/shared_expert/pallas_call | solution.py:416
  209.4 1.0 copy-done.13
  210.4 1.2 copy-done.14
  211.6 1.8 combine.1
  (53 shorter events, 2.0 us)
Async XLA Ops:
  5.4 98.2 %all-to-all-start = ((bf16[128,8,1024]{2,1,0:T(8,128)(2,1)}), bf16[128,8,1024]{2,1,0:T(8,128)(2,1)}, u32[]{:S(2)}, u32[]{:S(2)}) async-start(bf16[128,8,1024]{2,1,0:T(8,128)(2,1)} %bitcast.32), calls=%async_computation | async-start | bytes 4194304 | tf_op jit(solution)/shard_map/all_to_all | solution.py:610
  21.2 57.2 %collective-permute-start.1 = (bf16[384,2048]{1,0:T(8,128)(2,1)}, bf16[384,2048]{1,0:T(8,128)(2,1)}, u32[]{:S(2)}, u32[]{:S(2)}) collective-permute-start(bf16[384,2048]{1,0:T(8,128)(2,1)} %get-tuple-element.8), channel_id=1, source_target_pairs={{2,0},{0,4},{3,1},{1,5},{4,6},{6,2},{5,7},{7,3},{10,8},{8,12},{11,... | collective-permute-start | bytes 4718600 | tf_op jit(solution)/shard_map/ppermute | solution.py:593
  23.7 56.0 %collective-permute-start.3 = (bf16[384,2048]{1,0:T(8,128)(2,1)}, bf16[384,2048]{1,0:T(8,128)(2,1)S(1)}, u32[]{:S(2)}, u32[]{:S(2)}) collective-permute-start(bf16[384,2048]{1,0:T(8,128)(2,1)} %pick.3), channel_id=1, source_target_pairs={{3,0},{1,4},{0,1},{2,5},{5,6},{7,2},{6,7},{4,3},{11,8},{9,12},{8,9... | collective-permute-start | bytes 4718600 | tf_op jit(solution)/shard_map/ppermute | solution.py:593
  78.4 25.2 %collective-permute-start.2 = (bf16[384,2048]{1,0:T(8,128)(2,1)}, bf16[384,2048]{1,0:T(8,128)(2,1)S(1)}, u32[]{:S(2)}, u32[]{:S(2)}) collective-permute-start(bf16[384,2048]{1,0:T(8,128)(2,1)} %collective-permute-done.1.refs_2_.refs_4_), channel_id=1, source_target_pairs={{0,4},{1,5},{2,6},{3,7},{4,0},{5,1},{6,2},{7,3},{8,12},{9,13},{10,... | collective-permute-start | bytes 4718600 | tf_op jit(solution)/shard_map/ppermute | solution.py:593
  79.8 23.9 %collective-permute-start.4 = (bf16[384,2048]{1,0:T(8,128)(2,1)S(1)}, bf16[384,2048]{1,0:T(8,128)(2,1)}, u32[]{:S(2)}, u32[]{:S(2)}) collective-permute-start(bf16[384,2048]{1,0:T(8,128)(2,1)S(1)} %collective-permute-done.3.refs_1_.refs_7_), channel_id=1, source_target_pairs={{0,4},{1,5},{2,6},{3,7},{4,0},{5,1},{6,2},{7,3},{8,12},{9,13},{10,... | collective-permute-start | bytes 4718600 | tf_op jit(solution)/shard_map/ppermute | solution.py:593
  79.8 1.4 copy-start
  81.3 20.9 %collective-permute-start.5 = (bf16[192,2048]{1,0:T(8,128)(2,1)S(1)}, bf16[192,2048]{1,0:T(8,128)(2,1)}, u32[]{:S(2)}, u32[]{:S(2)}) collective-permute-start(bf16[192,2048]{1,0:T(8,128)(2,1)S(1)} %pick.4), channel_id=1, source_target_pairs={{2,0},{0,4},{3,1},{1,5},{4,6},{6,2},{5,7},{7,3},{10,8},{8,12},{11,... | collective-permute-start | bytes 2359304 | tf_op jit(solution)/shard_map/ppermute | solution.py:593
  82.0 21.6 %collective-permute-start.7 = (bf16[192,2048]{1,0:T(8,128)(2,1)S(1)}, bf16[192,2048]{1,0:T(8,128)(2,1)}, u32[]{:S(2)}, u32[]{:S(2)}) collective-permute-start(bf16[192,2048]{1,0:T(8,128)(2,1)S(1)} %pick.5), channel_id=1, source_target_pairs={{3,0},{1,4},{0,1},{2,5},{5,6},{7,2},{6,7},{4,3},{11,8},{9,12},{8,9... | collective-permute-start | bytes 2359304 | tf_op jit(solution)/shard_map/ppermute | solution.py:593
  102.2 8.4 %collective-permute-start.6 = (bf16[192,2048]{1,0:T(8,128)(2,1)}, bf16[192,2048]{1,0:T(8,128)(2,1)}, u32[]{:S(2)}, u32[]{:S(2)}) collective-permute-start(bf16[192,2048]{1,0:T(8,128)(2,1)} %collective-permute-done.5.refs_2_.refs_4_), channel_id=1, source_target_pairs={{0,4},{1,5},{2,6},{3,7},{4,0},{5,1},{6,2},{7,3},{8,12},{9,13},{10,... | collective-permute-start | bytes 2359304 | tf_op jit(solution)/shard_map/ppermute | solution.py:593
  103.6 6.9 %collective-permute-start.8 = (bf16[192,2048]{1,0:T(8,128)(2,1)}, bf16[192,2048]{1,0:T(8,128)(2,1)}, u32[]{:S(2)}, u32[]{:S(2)}) collective-permute-start(bf16[192,2048]{1,0:T(8,128)(2,1)} %collective-permute-done.7.refs_1_.refs_7_), channel_id=1, source_target_pairs={{0,4},{1,5},{2,6},{3,7},{4,0},{5,1},{6,2},{7,3},{8,12},{9,13},{10,... | collective-permute-start | bytes 2359304 | tf_op jit(solution)/shard_map/ppermute | solution.py:593
  115.3 12.1 %copy-start.2 = (bf16[2048,128]{1,0:T(8,128)(2,1)S(1)}, bf16[2048,128]{1,0:T(8,128)(2,1)}, u32[]{:S(2)}) copy-start(bf16[2048,128]{1,0:T(8,128)(2,1)} %gate_ref.1) | copy-start | bytes 1572868
  115.3 12.0 %copy-start.3 = (bf16[2048,128]{1,0:T(8,128)(2,1)S(1)}, bf16[2048,128]{1,0:T(8,128)(2,1)}, u32[]{:S(2)}) copy-start(bf16[2048,128]{1,0:T(8,128)(2,1)} %up_ref.1) | copy-start | bytes 1572868
  115.4 95.0 %all-to-all-start.1 = ((bf16[128,8,1024]{2,1,0:T(8,128)(2,1)}), bf16[128,8,1024]{2,1,0:T(8,128)(2,1)S(1)}, u32[]{:S(2)}, u32[]{:S(2)}) async-start(bf16[128,8,1024]{2,1,0:T(8,128)(2,1)} %bitcast.12), calls=%async_computation.1 | async-start | bytes 4194304 | tf_op jit(solution)/shard_map/all_to_all | solution.py:632
  129.0 55.0 %copy-start.7 = (bf16[256,256]{1,0:T(8,128)(2,1)S(1)}, bf16[256,256]{1,0:T(8,128)(2,1)}, u32[]{:S(2)}) copy-start(bf16[256,256]{1,0:T(8,128)(2,1)} %k_ref.1) | copy-start | bytes 393220
  129.0 55.0 %copy-start.8 = (bf16[256,256]{1,0:T(8,128)(2,1)S(1)}, bf16[256,256]{1,0:T(8,128)(2,1)}, u32[]{:S(2)}) copy-start(bf16[256,256]{1,0:T(8,128)(2,1)} %v_ref.1) | copy-start | bytes 393220
  129.1 65.4 %copy-start.9 = (f32[2048]{0:T(1024)S(1)}, f32[2048]{0:T(1024)}, u32[]{:S(2)}) copy-start(f32[2048]{0:T(1024)} %param.22) | copy-start | bytes 24580
  129.1 65.4 %copy-start.12 = (f32[16]{0:T(128)S(1)}, f32[16]{0:T(128)}, u32[]{:S(2)}) copy-start(f32[16]{0:T(128)} %sink_ref.1) | copy-start | bytes 196
  129.1 18.6 %collective-permute-start.10 = (bf16[1536,128]{1,0:T(8,128)(2,1)S(1)}, bf16[1536,128]{1,0:T(8,128)(2,1)S(1)}, u32[]{:S(2)}, u32[]{:S(2)}) collective-permute-start(bf16[1536,128]{1,0:T(8,128)(2,1)S(1)} %shared_prep.1), channel_id=1, source_target_pairs={{0,3},{1,0},{2,1},{3,2},{4,7},{5,4},{6,5},{7,6},{8,11},{9,8},{10,9... | collective-permute-start | bytes 1179656 | tf_op jit(solution)/shard_map/ppermute | solution.py:647
  132.4 17.7 %collective-permute-start.9 = (bf16[1536,128]{1,0:T(8,128)(2,1)S(1)}, bf16[1536,128]{1,0:T(8,128)(2,1)S(1)}, u32[]{:S(2)}, u32[]{:S(2)}) collective-permute-start(bf16[1536,128]{1,0:T(8,128)(2,1)S(1)} %shared_prep.1), channel_id=1, source_target_pairs={{0,1},{1,2},{2,3},{3,0},{4,5},{5,6},{6,7},{7,4},{8,9},{9,10},{10,1... | collective-permute-start | bytes 1179656 | tf_op jit(solution)/shard_map/ppermute | solution.py:647
  150.2 25.8 %collective-permute-start.11 = (bf16[4608,128]{1,0:T(8,128)(2,1)S(1)}, bf16[4608,128]{1,0:T(8,128)(2,1)}, u32[]{:S(2)}, u32[]{:S(2)}) collective-permute-start(bf16[4608,128]{1,0:T(8,128)(2,1)S(1)} %pad_maximum_fusion.refs_0_), channel_id=1, source_target_pairs={{0,8},{4,28},{8,0},{12,20},{16,24},{20,12},{24,16},{28,4},{1,9},{5... | collective-permute-start | bytes 3538952 | tf_op jit(solution)/shard_map/ppermute | solution.py:653
  151.2 24.7 %collective-permute-start.14 = (bf16[1536,128]{1,0:T(8,128)(2,1)S(1)}, bf16[1536,128]{1,0:T(8,128)(2,1)}, u32[]{:S(2)}, u32[]{:S(2)}) collective-permute-start(bf16[1536,128]{1,0:T(8,128)(2,1)S(1)} %shared_prep.1), channel_id=1, source_target_pairs={{0,2},{1,3},{2,0},{3,1},{4,6},{5,7},{6,4},{7,5},{8,10},{9,11},{10,... | collective-permute-start | bytes 1179656 | tf_op jit(solution)/shard_map/ppermute | solution.py:647
  152.1 52.0 %collective-permute-start.12 = (bf16[4608,128]{1,0:T(8,128)(2,1)S(1)}, bf16[4608,128]{1,0:T(8,128)(2,1)}, u32[]{:S(2)}, u32[]{:S(2)}) collective-permute-start(bf16[4608,128]{1,0:T(8,128)(2,1)S(1)} %pad_maximum_fusion.refs_0_), channel_id=1, source_target_pairs={{0,4},{4,0},{1,5},{5,1},{2,6},{6,2},{3,7},{7,3},{8,12},{12,8},{9,1... | collective-permute-start | bytes 3538952 | tf_op jit(solution)/shard_map/ppermute | solution.py:654
  175.9 28.2 %collective-permute-start.13 = (bf16[4608,128]{1,0:T(8,128)(2,1)}, bf16[4608,128]{1,0:T(8,128)(2,1)}, u32[]{:S(2)}, u32[]{:S(2)}) collective-permute-start(bf16[4608,128]{1,0:T(8,128)(2,1)} %collective-permute-done.11.refs_1_), channel_id=1, source_target_pairs={{0,4},{4,0},{1,5},{5,1},{2,6},{6,2},{3,7},{7,3},{8,12},{12,8},{9,1... | collective-permute-start | bytes 3538952 | tf_op jit(solution)/shard_map/ppermute | solution.py:654
  176.0 8.1 %collective-permute-start.15 = (bf16[1536,128]{1,0:T(8,128)(2,1)}, bf16[1536,128]{1,0:T(8,128)(2,1)}, u32[]{:S(2)}, u32[]{:S(2)}) collective-permute-start(bf16[1536,128]{1,0:T(8,128)(2,1)} %collective-permute-done.14.refs_4_), channel_id=1, source_target_pairs={{0,8},{4,28},{8,0},{12,20},{16,24},{20,12},{24,16},{28,4},{1,9},{5... | collective-permute-start | bytes 1179656 | tf_op jit(solution)/shard_map/ppermute | solution.py:653
  177.0 27.1 %collective-permute-start.16 = (bf16[1536,128]{1,0:T(8,128)(2,1)}, bf16[1536,128]{1,0:T(8,128)(2,1)}, u32[]{:S(2)}, u32[]{:S(2)}) collective-permute-start(bf16[1536,128]{1,0:T(8,128)(2,1)} %collective-permute-done.14.refs_4_), channel_id=1, source_target_pairs={{0,4},{4,0},{1,5},{5,1},{2,6},{6,2},{3,7},{7,3},{8,12},{12,8},{9,1... | collective-permute-start | bytes 1179656 | tf_op jit(solution)/shard_map/ppermute | solution.py:654
  184.1 20.1 %collective-permute-start.17 = (bf16[1536,128]{1,0:T(8,128)(2,1)}, bf16[1536,128]{1,0:T(8,128)(2,1)}, u32[]{:S(2)}, u32[]{:S(2)}) collective-permute-start(bf16[1536,128]{1,0:T(8,128)(2,1)} %collective-permute-done.15.refs_5_), channel_id=1, source_target_pairs={{0,4},{4,0},{1,5},{5,1},{2,6},{6,2},{3,7},{7,3},{8,12},{12,8},{9,1... | collective-permute-start | bytes 1179656 | tf_op jit(solution)/shard_map/ppermute | solution.py:654
  184.7 9.7 %collective-permute-start = (bf16[2,128,256]{2,1,0:T(8,128)(2,1)}, bf16[2,128,256]{2,1,0:T(8,128)(2,1)}, u32[]{:S(2)}, u32[]{:S(2)}) collective-permute-start(bf16[2,128,256]{2,1,0:T(8,128)(2,1)} %pad_maximum_fusion.1), channel_id=1, source_target_pairs={{0,1},{1,2},{2,3},{3,4},{4,5},{5,6},{6,7},{7,8},{8,9},{9,10},{10,1... | collective-permute-start | bytes 393224 | tf_op jit(solution)/shard_map/ppermute | solution.py:56
  194.4 2.2 %copy-start.1 = (bf16[1024,2048]{1,0:T(8,128)(2,1)S(1)}, bf16[1024,2048]{1,0:T(8,128)(2,1)}, u32[]{:S(2)}) copy-start(bf16[1024,2048]{1,0:T(8,128)(2,1)} %weight_ref.1) | copy-start | bytes 12582916
  197.7 6.5 %copy-start.6 = (bf16[128,2048]{1,0:T(8,128)(2,1)S(1)}, bf16[128,2048]{1,0:T(8,128)(2,1)}, u32[]{:S(2)}) copy-start(bf16[128,2048]{1,0:T(8,128)(2,1)} %get-tuple-element.9.x_ref) | copy-start | bytes 1572868
  197.7 6.5 %copy-start.10 = (s32[128,2]{0,1:T(2,128)S(1)}, s32[128,2]{0,1:T(2,128)}, u32[]{:S(2)}) copy-start(s32[128,2]{0,1:T(2,128)} %param.25) | copy-start | bytes 3076
  197.7 6.5 %copy-start.11 = (f32[128,2]{0,1:T(2,128)S(1)}, f32[128,2]{0,1:T(2,128)}, u32[]{:S(2)}) copy-start(f32[128,2]{0,1:T(2,128)} %param.26) | copy-start | bytes 3076
  204.2 6.2 %copy-start.15 = (f32[2048]{0:T(1024)S(1)}, f32[2048]{0:T(1024)}, u32[]{:S(2)}) copy-start(f32[2048]{0:T(1024)} %param.33) | copy-start | bytes 24580
  (4 other events, 4.3 us)

commit v6 on v5

--- a/solution.py
+++ b/solution.py
@@ -15,6 +15,7 @@
 WINDOW = 128
 CAP = 4
 BLOCK = 256
+WIDE = 512
 MIB = 1 << 20
 PARTS = 4
 COMBINE_LIMIT = 16
@@ -278,13 +279,13 @@
     out_ref, down, made, sems, out_sems = refs[8:]
     part = own[0].shape[0]
     half = out_ref.shape[1]
-    count = half // BLOCK
+    count = half // WIDE
 
     def copies(n, pieces):
         return [
             pltpu.make_async_copy(
-                piece.at[:, pl.ds(h * half + n * BLOCK, BLOCK)],
-                down.at[pl.ds(k * part, part), pl.ds(h * half + n * BLOCK, BLOCK)],
+                piece.at[:, pl.ds(h * half + n * WIDE, WIDE)],
+                down.at[pl.ds(k * part, part), pl.ds(h * half + n * WIDE, WIDE)],
                 sems.at[n, h, k],
             )
             for h in range(2)
@@ -300,29 +301,29 @@
                     c.start()
 
     tiles = hidden.shape[0] // (2 * CAP)
-    low = iota((tiles, 2 * CAP, BLOCK), 1) < CAP
+    low = iota((tiles, 2 * CAP, WIDE), 1) < CAP
     for n in range(count):
         for c in copies(n, own):
             c.wait()
-        at = n * BLOCK
+        at = n * WIDE
         x = hidden[...]
-        left = dot(x, down[:, at : at + BLOCK]).reshape(tiles, 2 * CAP, BLOCK)
-        right = dot(x, down[:, half + at : half + at + BLOCK]).reshape(tiles, 2 * CAP, BLOCK)
+        left = dot(x, down[:, at : at + WIDE]).reshape(tiles, 2 * CAP, WIDE)
+        right = dot(x, down[:, half + at : half + at + WIDE]).reshape(tiles, 2 * CAP, WIDE)
         one = jnp.where(low, left, pltpu.roll(right, CAP, 1))
         two = jnp.where(low, pltpu.roll(left, CAP, 1), right)
-        both = jnp.stack([one, two], axis=1).reshape(out_ref.shape[0], BLOCK)
-        made[:, at : at + BLOCK] = both.astype(bf16)
-        columns = pl.ds(at, BLOCK)
+        both = jnp.stack([one, two], axis=1).reshape(out_ref.shape[0], WIDE)
+        made[:, at : at + WIDE] = both.astype(bf16)
+        columns = pl.ds(at, WIDE)
         pltpu.make_async_copy(made.at[:, columns], out_ref.at[:, columns], out_sems.at[n]).start()
     for n in range(count):
-        columns = pl.ds(n * BLOCK, BLOCK)
+        columns = pl.ds(n * WIDE, WIDE)
         pltpu.make_async_copy(made.at[:, columns], out_ref.at[:, columns], out_sems.at[n]).wait()
 
 
 def expert_down(own, hidden, mine, others):
     rows, units = hidden.shape
     width = mine[0].shape[1]
-    count = width // 2 // BLOCK
+    count = width // 2 // WIDE
     return pl.pallas_call(
         down_kernel,
         in_specs=[pl.BlockSpec(memory_space=pltpu.SMEM)]

time: 217 us -> 217 us (level)
  no operation moved by 1% of the time
where the time goes in v6:
time: 217 us; the launch traced here: 214 us
  waiting for transfers between devices  131 us (60%)
  starting transfers between devices  40 us (18%)
  Pallas kernels  33.1 us (15%)
  local copies, waits for them, and re-layouts  7.94 us (4%)
    ppermute x8, waiting for transfers between devices, moved(): return lax.ppermute(piece, CORE_TP, route)  75.8 us
    ppermute x2, waiting for transfers between devices, spread_out(): pair = [piece, lax.ppermute(piece, ('y', 'c'), beside)]  29.7 us
    ppermute x3, waiting for transfers between devices, body(): lax.ppermute(prepared, 'tp', [(i, (i + k) % tp) for i in range(tp)])  17.7 us
    all_to_all x1, starting transfers between devices, body(): lax.all_to_all(packed.reshape(chips, 2 * CAP, -1), CHIPS, split_axis=0, c...  15.8 us
    all_to_all x1, starting transfers between devices, body(): lax.all_to_all(out.reshape(chips, 2 * CAP, -1), CHIPS, split_axis=0, conc...  12.1 us
    unnamed x32, local copies, waits for them, and re-layouts  7.94 us
    ppermute x1, waiting for transfers between devices, from_behind(): return lax.ppermute(block, axis, route)  7.54 us
    pallas_call x1, Pallas kernels, expert_up(): pl.pallas_call(up_kernel, in_specs=[pl.BlockSpec(memory_space=pltpu.SMEM)...  6.86 us
  transfers between devices with their start and end apart: 20, of which 9 were waited for; matrix products, arithmetic and copies ran while one was open for 0% of the time, Pallas kernels for 10%

profile of v6, /device:TPU:8, one launch (start us, length us, event | category | flops | bytes accessed | tf_op | source)
XLA Modules:
  0.0 213.6 jit_solution(924632482757640358)
XLA Ops:
  0.6 4.8 %pack.1 = (bf16[1024,1024]{1,0:T(8,128)(2,1)}, bf16[128,2048]{1,0:T(8,128)(2,1)}, bf16[384,2048]{1,0:T(8,128)(2,1)}) custom-call(s32[1]{0:T(128)} %bitcast.5.expert_ref, bf16[128,2048]{1,0:T(8,128)(2,1)} %x_ref.1, f32[1,2048]{1,0:T(1,128)} %bitcast.33, s32[2,128]{1,0:T(2,128)} %bitcast.24, bf16[2,192,2048]{2,1,0:T(8,128)(2,1)} %bitcast.28, ...), custom_call_target="tpu_custom_call" | custom-call | flops 536870912 | bytes 1572864 | tf_op jit(solution)/shard_map/pack/pallas_call | solution.py:137
  5.4 15.8 %all-to-all-start = ((bf16[128,8,1024]{2,1,0:T(8,128)(2,1)}), bf16[128,8,1024]{2,1,0:T(8,128)(2,1)}, u32[]{:S(2)}, u32[]{:S(2)}) async-start(bf16[128,8,1024]{2,1,0:T(8,128)(2,1)} %bitcast.32), calls=%async_computation | async-start | bytes 4194304 | tf_op jit(solution)/shard_map/all_to_all | solution.py:611
  21.3 2.4 %pick.3 = bf16[384,2048]{1,0:T(8,128)(2,1)} custom-call(s32[1]{0:T(128)S(6)} %sub.15.expert_ref, bf16[2,192,2048]{2,1,0:T(8,128)(2,1)} %bitcast.29, bf16[2,192,2048]{2,1,0:T(8,128)(2,1)} %bitcast.31), custom_call_target="tpu_custom_call" | custom-call | flops 1000 | bytes 3145728 | tf_op jit(solution)/shard_map/pick/pallas_call | solution.py:185
  23.7 1.7 collective-permute-start.3
  25.4 53.0 %collective-permute-done.1.refs_2_.refs_4_ = bf16[384,2048]{1,0:T(8,128)(2,1)} collective-permute-done((bf16[384,2048]{1,0:T(8,128)(2,1)}, bf16[384,2048]{1,0:T(8,128)(2,1)}, u32[]{:S(2)}, u32[]{:S(2)}) %collective-permute-start.1) | collective-permute-done | bytes 1572896 | tf_op jit(solution)/shard_map/ppermute | solution.py:594
  78.4 1.4 collective-permute-done.3.refs_1_.refs_7_
  79.8 1.4 copy-done
  82.2 19.9 %collective-permute-done.5.refs_2_.refs_4_ = bf16[192,2048]{1,0:T(8,128)(2,1)} collective-permute-done((bf16[192,2048]{1,0:T(8,128)(2,1)S(1)}, bf16[192,2048]{1,0:T(8,128)(2,1)}, u32[]{:S(2)}, u32[]{:S(2)}) %collective-permute-start.5) | collective-permute-done | bytes 786464 | tf_op jit(solution)/shard_map/ppermute | solution.py:594
  102.2 1.4 collective-permute-done.7.refs_1_.refs_7_
  103.7 6.9 %expert_up.1.hidden = bf16[512,768]{1,0:T(8,128)(2,1)S(1)} custom-call(s32[1]{0:T(128)} %bitcast.4.own_ref, bf16[1024,1024]{1,0:T(8,128)(2,1)} %bitcast.11.recv, bf16[384,2048]{1,0:T(8,128)(2,1)S(1)} %collective-permute-done.2.refs_0_.refs_6_, bf16[384,2048]{1,0:T(8,128)(2,1)S(1)} %collective-permute-done.3.refs_1_.refs_7_, ...), custom_call_target="tpu_custom_call" | custom-call | flops 3221225472 | bytes 8388608 | tf_op jit(solution)/shard_map/expert_up/pallas_call | solution.py:254
  110.6 4.8 %expert_down.1 = bf16[1024,1024]{1,0:T(8,128)(2,1)} custom-call(s32[1]{0:T(128)} %bitcast.4.own_ref, bf16[512,768]{1,0:T(8,128)(2,1)S(1)} %expert_up.1.hidden, bf16[192,2048]{1,0:T(8,128)(2,1)} %collective-permute-done.6.refs_0_.refs_6_, bf16[192,2048]{1,0:T(8,128)(2,1)} %collective-permute-done.7.refs_1_.refs_7_, ...), custom_call_target="tpu_custom_call" | custom-call | flops 1610612736 | bytes 6029312 | tf_op jit(solution)/shard_map/expert_down/pallas_call | solution.py:327
  115.3 12.1 %all-to-all-start.1 = ((bf16[128,8,1024]{2,1,0:T(8,128)(2,1)}), bf16[128,8,1024]{2,1,0:T(8,128)(2,1)S(1)}, u32[]{:S(2)}, u32[]{:S(2)}) async-start(bf16[128,8,1024]{2,1,0:T(8,128)(2,1)} %bitcast.12), calls=%async_computation.1 | async-start | bytes 4194304 | tf_op jit(solution)/shard_map/all_to_all | solution.py:633
  127.6 1.0 copy-done.4
  129.3 3.3 %collective-permute-start.10 = (bf16[1536,128]{1,0:T(8,128)(2,1)S(1)}, bf16[1536,128]{1,0:T(8,128)(2,1)S(1)}, u32[]{:S(2)}, u32[]{:S(2)}) collective-permute-start(bf16[1536,128]{1,0:T(8,128)(2,1)S(1)} %shared_prep.1), channel_id=1, source_target_pairs={{0,3},{1,0},{2,1},{3,2},{4,7},{5,4},{6,5},{7,6},{8,11},{9,8},{10,9... | collective-permute-start | bytes 1179656 | tf_op jit(solution)/shard_map/ppermute | solution.py:648
  132.6 15.3 %collective-permute-done.10 = bf16[1536,128]{1,0:T(8,128)(2,1)S(1)} collective-permute-done((bf16[1536,128]{1,0:T(8,128)(2,1)S(1)}, bf16[1536,128]{1,0:T(8,128)(2,1)S(1)}, u32[]{:S(2)}, u32[]{:S(2)}) %collective-permute-start.10) | collective-permute-done | bytes 393248 | tf_op jit(solution)/shard_map/ppermute | solution.py:648
  147.8 2.4 %collective-permute-done.9 = bf16[1536,128]{1,0:T(8,128)(2,1)S(1)} collective-permute-done((bf16[1536,128]{1,0:T(8,128)(2,1)S(1)}, bf16[1536,128]{1,0:T(8,128)(2,1)S(1)}, u32[]{:S(2)}, u32[]{:S(2)}) %collective-permute-start.9) | collective-permute-done | bytes 393248 | tf_op jit(solution)/shard_map/ppermute | solution.py:648
  150.3 1.1 collective-permute-start.11
  151.4 0.8 collective-permute-start.14
  152.3 23.9 %collective-permute-done.11.refs_1_ = bf16[4608,128]{1,0:T(8,128)(2,1)} collective-permute-done((bf16[4608,128]{1,0:T(8,128)(2,1)S(1)}, bf16[4608,128]{1,0:T(8,128)(2,1)}, u32[]{:S(2)}, u32[]{:S(2)}) %collective-permute-start.11) | collective-permute-done | bytes 1179680 | tf_op jit(solution)/shard_map/ppermute | solution.py:654
  176.1 1.0 collective-permute-start.15
  177.1 1.2 collective-permute-start.16
  178.4 5.9 %collective-permute-done.15.refs_5_ = bf16[1536,128]{1,0:T(8,128)(2,1)} collective-permute-done((bf16[1536,128]{1,0:T(8,128)(2,1)}, bf16[1536,128]{1,0:T(8,128)(2,1)}, u32[]{:S(2)}, u32[]{:S(2)}) %collective-permute-start.15) | collective-permute-done | bytes 393248 | tf_op jit(solution)/shard_map/ppermute | solution.py:654
  184.2 0.7 pad_maximum_fusion.1
  184.9 2.1 collective-permute-start
  187.1 7.5 %collective-permute-done.rim_ref = bf16[2,128,256]{2,1,0:T(8,128)(2,1)} collective-permute-done((bf16[2,128,256]{2,1,0:T(8,128)(2,1)}, bf16[2,128,256]{2,1,0:T(8,128)(2,1)}, u32[]{:S(2)}, u32[]{:S(2)}) %collective-permute-start) | collective-permute-done | bytes 131104 | tf_op jit(solution)/shard_map/ppermute | solution.py:57
  194.6 2.2 %copy-done.1 = bf16[1024,2048]{1,0:T(8,128)(2,1)S(1)} copy-done((bf16[1024,2048]{1,0:T(8,128)(2,1)S(1)}, bf16[1024,2048]{1,0:T(8,128)(2,1)}, u32[]{:S(2)}) %copy-start.1) | copy-done | bytes 4194328
  196.8 1.0 copy-done.5
  197.8 6.4 %attention.1 = bf16[256,2048]{1,0:T(8,128)(2,1)} custom-call(s32[1]{0:T(128)} %bitcast.first_ref, f32[16]{0:T(128)S(1)} %copy-done.12, bf16[256,1024]{1,0:T(8,128)(2,1)S(1)} %copy-done.5, bf16[256,256]{1,0:T(8,128)(2,1)S(1)} %copy-done.7, bf16[256,256]{1,0:T(8,128)(2,1)S(1)} %copy-done.8, bf16[2,128,256]{2,1,0:T(8,128)(2,1)} %collective-permute-done.rim_ref, ...), custom_call_target="tpu_custom_call" | custom-call | flops 1610612736 | bytes 6291456 | tf_op jit(solution)/shard_map/attention/pallas_call | solution.py:534
  204.3 5.2 %shared_expert.1 = (f32[128,2048]{1,0:T(8,128)S(1)}, f32[128,128]{1,0:T(8,128)S(1)}) custom-call(s32[4]{0:T(128)S(1)} %pad_add_fusion.part_ref, s32[2,128]{1,0:T(2,128)S(1)} %bitcast.25, f32[2,128]{1,0:T(2,128)S(1)} %bitcast.26, bf16[128,2048]{1,0:T(8,128)(2,1)S(1)} %copy-done.6, bf16[4608,128]{1,0:T(8,128)(2,1)S(1)} %pad_maximum_fusion.refs_0_, ...), custom_call_target="tpu_custom_call" | custom-call | flops 805306368 | bytes 6291456 | tf_op jit(solution)/shard_map/shared_expert/pallas_call | solution.py:417
  209.6 1.0 copy-done.13
  210.6 1.2 copy-done.14
  211.8 1.8 combine.1
  (53 shorter events, 2.0 us)
Async XLA Ops:
  5.4 98.2 %all-to-all-start = ((bf16[128,8,1024]{2,1,0:T(8,128)(2,1)}), bf16[128,8,1024]{2,1,0:T(8,128)(2,1)}, u32[]{:S(2)}, u32[]{:S(2)}) async-start(bf16[128,8,1024]{2,1,0:T(8,128)(2,1)} %bitcast.32), calls=%async_computation | async-start | bytes 4194304 | tf_op jit(solution)/shard_map/all_to_all | solution.py:611
  21.2 57.2 %collective-permute-start.1 = (bf16[384,2048]{1,0:T(8,128)(2,1)}, bf16[384,2048]{1,0:T(8,128)(2,1)}, u32[]{:S(2)}, u32[]{:S(2)}) collective-permute-start(bf16[384,2048]{1,0:T(8,128)(2,1)} %get-tuple-element.8), channel_id=1, source_target_pairs={{2,0},{0,4},{3,1},{1,5},{4,6},{6,2},{5,7},{7,3},{10,8},{8,12},{11,... | collective-permute-start | bytes 4718600 | tf_op jit(solution)/shard_map/ppermute | solution.py:594
  23.7 56.0 %collective-permute-start.3 = (bf16[384,2048]{1,0:T(8,128)(2,1)}, bf16[384,2048]{1,0:T(8,128)(2,1)S(1)}, u32[]{:S(2)}, u32[]{:S(2)}) collective-permute-start(bf16[384,2048]{1,0:T(8,128)(2,1)} %pick.3), channel_id=1, source_target_pairs={{3,0},{1,4},{0,1},{2,5},{5,6},{7,2},{6,7},{4,3},{11,8},{9,12},{8,9... | collective-permute-start | bytes 4718600 | tf_op jit(solution)/shard_map/ppermute | solution.py:594
  78.4 25.2 %collective-permute-start.2 = (bf16[384,2048]{1,0:T(8,128)(2,1)}, bf16[384,2048]{1,0:T(8,128)(2,1)S(1)}, u32[]{:S(2)}, u32[]{:S(2)}) collective-permute-start(bf16[384,2048]{1,0:T(8,128)(2,1)} %collective-permute-done.1.refs_2_.refs_4_), channel_id=1, source_target_pairs={{0,4},{1,5},{2,6},{3,7},{4,0},{5,1},{6,2},{7,3},{8,12},{9,13},{10,... | collective-permute-start | bytes 4718600 | tf_op jit(solution)/shard_map/ppermute | solution.py:594
  79.8 23.9 %collective-permute-start.4 = (bf16[384,2048]{1,0:T(8,128)(2,1)S(1)}, bf16[384,2048]{1,0:T(8,128)(2,1)}, u32[]{:S(2)}, u32[]{:S(2)}) collective-permute-start(bf16[384,2048]{1,0:T(8,128)(2,1)S(1)} %collective-permute-done.3.refs_1_.refs_7_), channel_id=1, source_target_pairs={{0,4},{1,5},{2,6},{3,7},{4,0},{5,1},{6,2},{7,3},{8,12},{9,13},{10,... | collective-permute-start | bytes 4718600 | tf_op jit(solution)/shard_map/ppermute | solution.py:594
  79.8 1.4 copy-start
  81.3 20.9 %collective-permute-start.5 = (bf16[192,2048]{1,0:T(8,128)(2,1)S(1)}, bf16[192,2048]{1,0:T(8,128)(2,1)}, u32[]{:S(2)}, u32[]{:S(2)}) collective-permute-start(bf16[192,2048]{1,0:T(8,128)(2,1)S(1)} %pick.4), channel_id=1, source_target_pairs={{2,0},{0,4},{3,1},{1,5},{4,6},{6,2},{5,7},{7,3},{10,8},{8,12},{11,... | collective-permute-start | bytes 2359304 | tf_op jit(solution)/shard_map/ppermute | solution.py:594
  82.0 21.6 %collective-permute-start.7 = (bf16[192,2048]{1,0:T(8,128)(2,1)S(1)}, bf16[192,2048]{1,0:T(8,128)(2,1)}, u32[]{:S(2)}, u32[]{:S(2)}) collective-permute-start(bf16[192,2048]{1,0:T(8,128)(2,1)S(1)} %pick.5), channel_id=1, source_target_pairs={{3,0},{1,4},{0,1},{2,5},{5,6},{7,2},{6,7},{4,3},{11,8},{9,12},{8,9... | collective-permute-start | bytes 2359304 | tf_op jit(solution)/shard_map/ppermute | solution.py:594
  102.2 8.4 %collective-permute-start.6 = (bf16[192,2048]{1,0:T(8,128)(2,1)}, bf16[192,2048]{1,0:T(8,128)(2,1)}, u32[]{:S(2)}, u32[]{:S(2)}) collective-permute-start(bf16[192,2048]{1,0:T(8,128)(2,1)} %collective-permute-done.5.refs_2_.refs_4_), channel_id=1, source_target_pairs={{0,4},{1,5},{2,6},{3,7},{4,0},{5,1},{6,2},{7,3},{8,12},{9,13},{10,... | collective-permute-start | bytes 2359304 | tf_op jit(solution)/shard_map/ppermute | solution.py:594
  103.6 6.9 %collective-permute-start.8 = (bf16[192,2048]{1,0:T(8,128)(2,1)}, bf16[192,2048]{1,0:T(8,128)(2,1)}, u32[]{:S(2)}, u32[]{:S(2)}) collective-permute-start(bf16[192,2048]{1,0:T(8,128)(2,1)} %collective-permute-done.7.refs_1_.refs_7_), channel_id=1, source_target_pairs={{0,4},{1,5},{2,6},{3,7},{4,0},{5,1},{6,2},{7,3},{8,12},{9,13},{10,... | collective-permute-start | bytes 2359304 | tf_op jit(solution)/shard_map/ppermute | solution.py:594
  115.3 12.2 %copy-start.2 = (bf16[2048,128]{1,0:T(8,128)(2,1)S(1)}, bf16[2048,128]{1,0:T(8,128)(2,1)}, u32[]{:S(2)}) copy-start(bf16[2048,128]{1,0:T(8,128)(2,1)} %gate_ref.1) | copy-start | bytes 1572868
  115.3 12.2 %copy-start.3 = (bf16[2048,128]{1,0:T(8,128)(2,1)S(1)}, bf16[2048,128]{1,0:T(8,128)(2,1)}, u32[]{:S(2)}) copy-start(bf16[2048,128]{1,0:T(8,128)(2,1)} %up_ref.1) | copy-start | bytes 1572868
  115.3 95.2 %all-to-all-start.1 = ((bf16[128,8,1024]{2,1,0:T(8,128)(2,1)}), bf16[128,8,1024]{2,1,0:T(8,128)(2,1)S(1)}, u32[]{:S(2)}, u32[]{:S(2)}) async-start(bf16[128,8,1024]{2,1,0:T(8,128)(2,1)} %bitcast.12), calls=%async_computation.1 | async-start | bytes 4194304 | tf_op jit(solution)/shard_map/all_to_all | solution.py:633
  129.2 55.0 %copy-start.7 = (bf16[256,256]{1,0:T(8,128)(2,1)S(1)}, bf16[256,256]{1,0:T(8,128)(2,1)}, u32[]{:S(2)}) copy-start(bf16[256,256]{1,0:T(8,128)(2,1)} %k_ref.1) | copy-start | bytes 393220
  129.2 55.0 %copy-start.8 = (bf16[256,256]{1,0:T(8,128)(2,1)S(1)}, bf16[256,256]{1,0:T(8,128)(2,1)}, u32[]{:S(2)}) copy-start(bf16[256,256]{1,0:T(8,128)(2,1)} %v_ref.1) | copy-start | bytes 393220
  129.2 65.4 %copy-start.9 = (f32[2048]{0:T(1024)S(1)}, f32[2048]{0:T(1024)}, u32[]{:S(2)}) copy-start(f32[2048]{0:T(1024)} %param.22) | copy-start | bytes 24580
  129.2 65.4 %copy-start.12 = (f32[16]{0:T(128)S(1)}, f32[16]{0:T(128)}, u32[]{:S(2)}) copy-start(f32[16]{0:T(128)} %sink_ref.1) | copy-start | bytes 196
  129.3 18.6 %collective-permute-start.10 = (bf16[1536,128]{1,0:T(8,128)(2,1)S(1)}, bf16[1536,128]{1,0:T(8,128)(2,1)S(1)}, u32[]{:S(2)}, u32[]{:S(2)}) collective-permute-start(bf16[1536,128]{1,0:T(8,128)(2,1)S(1)} %shared_prep.1), channel_id=1, source_target_pairs={{0,3},{1,0},{2,1},{3,2},{4,7},{5,4},{6,5},{7,6},{8,11},{9,8},{10,9... | collective-permute-start | bytes 1179656 | tf_op jit(solution)/shard_map/ppermute | solution.py:648
  132.6 17.7 %collective-permute-start.9 = (bf16[1536,128]{1,0:T(8,128)(2,1)S(1)}, bf16[1536,128]{1,0:T(8,128)(2,1)S(1)}, u32[]{:S(2)}, u32[]{:S(2)}) collective-permute-start(bf16[1536,128]{1,0:T(8,128)(2,1)S(1)} %shared_prep.1), channel_id=1, source_target_pairs={{0,1},{1,2},{2,3},{3,0},{4,5},{5,6},{6,7},{7,4},{8,9},{9,10},{10,1... | collective-permute-start | bytes 1179656 | tf_op jit(solution)/shard_map/ppermute | solution.py:648
  150.3 25.8 %collective-permute-start.11 = (bf16[4608,128]{1,0:T(8,128)(2,1)S(1)}, bf16[4608,128]{1,0:T(8,128)(2,1)}, u32[]{:S(2)}, u32[]{:S(2)}) collective-permute-start(bf16[4608,128]{1,0:T(8,128)(2,1)S(1)} %pad_maximum_fusion.refs_0_), channel_id=1, source_target_pairs={{0,8},{4,28},{8,0},{12,20},{16,24},{20,12},{24,16},{28,4},{1,9},{5... | collective-permute-start | bytes 3538952 | tf_op jit(solution)/shard_map/ppermute | solution.py:654
  151.4 24.7 %collective-permute-start.14 = (bf16[1536,128]{1,0:T(8,128)(2,1)S(1)}, bf16[1536,128]{1,0:T(8,128)(2,1)}, u32[]{:S(2)}, u32[]{:S(2)}) collective-permute-start(bf16[1536,128]{1,0:T(8,128)(2,1)S(1)} %shared_prep.1), channel_id=1, source_target_pairs={{0,2},{1,3},{2,0},{3,1},{4,6},{5,7},{6,4},{7,5},{8,10},{9,11},{10,... | collective-permute-start | bytes 1179656 | tf_op jit(solution)/shard_map/ppermute | solution.py:648
  152.2 52.0 %collective-permute-start.12 = (bf16[4608,128]{1,0:T(8,128)(2,1)S(1)}, bf16[4608,128]{1,0:T(8,128)(2,1)}, u32[]{:S(2)}, u32[]{:S(2)}) collective-permute-start(bf16[4608,128]{1,0:T(8,128)(2,1)S(1)} %pad_maximum_fusion.refs_0_), channel_id=1, source_target_pairs={{0,4},{4,0},{1,5},{5,1},{2,6},{6,2},{3,7},{7,3},{8,12},{12,8},{9,1... | collective-permute-start | bytes 3538952 | tf_op jit(solution)/shard_map/ppermute | solution.py:655
  176.1 28.2 %collective-permute-start.13 = (bf16[4608,128]{1,0:T(8,128)(2,1)}, bf16[4608,128]{1,0:T(8,128)(2,1)}, u32[]{:S(2)}, u32[]{:S(2)}) collective-permute-start(bf16[4608,128]{1,0:T(8,128)(2,1)} %collective-permute-done.11.refs_1_), channel_id=1, source_target_pairs={{0,4},{4,0},{1,5},{5,1},{2,6},{6,2},{3,7},{7,3},{8,12},{12,8},{9,1... | collective-permute-start | bytes 3538952 | tf_op jit(solution)/shard_map/ppermute | solution.py:655
  176.1 8.1 %collective-permute-start.15 = (bf16[1536,128]{1,0:T(8,128)(2,1)}, bf16[1536,128]{1,0:T(8,128)(2,1)}, u32[]{:S(2)}, u32[]{:S(2)}) collective-permute-start(bf16[1536,128]{1,0:T(8,128)(2,1)} %collective-permute-done.14.refs_4_), channel_id=1, source_target_pairs={{0,8},{4,28},{8,0},{12,20},{16,24},{20,12},{24,16},{28,4},{1,9},{5... | collective-permute-start | bytes 1179656 | tf_op jit(solution)/shard_map/ppermute | solution.py:654
  177.1 27.1 %collective-permute-start.16 = (bf16[1536,128]{1,0:T(8,128)(2,1)}, bf16[1536,128]{1,0:T(8,128)(2,1)}, u32[]{:S(2)}, u32[]{:S(2)}) collective-permute-start(bf16[1536,128]{1,0:T(8,128)(2,1)} %collective-permute-done.14.refs_4_), channel_id=1, source_target_pairs={{0,4},{4,0},{1,5},{5,1},{2,6},{6,2},{3,7},{7,3},{8,12},{12,8},{9,1... | collective-permute-start | bytes 1179656 | tf_op jit(solution)/shard_map/ppermute | solution.py:655
  184.2 20.1 %collective-permute-start.17 = (bf16[1536,128]{1,0:T(8,128)(2,1)}, bf16[1536,128]{1,0:T(8,128)(2,1)}, u32[]{:S(2)}, u32[]{:S(2)}) collective-permute-start(bf16[1536,128]{1,0:T(8,128)(2,1)} %collective-permute-done.15.refs_5_), channel_id=1, source_target_pairs={{0,4},{4,0},{1,5},{5,1},{2,6},{6,2},{3,7},{7,3},{8,12},{12,8},{9,1... | collective-permute-start | bytes 1179656 | tf_op jit(solution)/shard_map/ppermute | solution.py:655
  184.9 9.7 %collective-permute-start = (bf16[2,128,256]{2,1,0:T(8,128)(2,1)}, bf16[2,128,256]{2,1,0:T(8,128)(2,1)}, u32[]{:S(2)}, u32[]{:S(2)}) collective-permute-start(bf16[2,128,256]{2,1,0:T(8,128)(2,1)} %pad_maximum_fusion.1), channel_id=1, source_target_pairs={{0,1},{1,2},{2,3},{3,4},{4,5},{5,6},{6,7},{7,8},{8,9},{9,10},{10,1... | collective-permute-start | bytes 393224 | tf_op jit(solution)/shard_map/ppermute | solution.py:57
  194.6 2.2 %copy-start.1 = (bf16[1024,2048]{1,0:T(8,128)(2,1)S(1)}, bf16[1024,2048]{1,0:T(8,128)(2,1)}, u32[]{:S(2)}) copy-start(bf16[1024,2048]{1,0:T(8,128)(2,1)} %weight_ref.1) | copy-start | bytes 12582916
  197.8 6.5 %copy-start.6 = (bf16[128,2048]{1,0:T(8,128)(2,1)S(1)}, bf16[128,2048]{1,0:T(8,128)(2,1)}, u32[]{:S(2)}) copy-start(bf16[128,2048]{1,0:T(8,128)(2,1)} %get-tuple-element.9.x_ref) | copy-start | bytes 1572868
  197.8 6.5 %copy-start.10 = (s32[128,2]{0,1:T(2,128)S(1)}, s32[128,2]{0,1:T(2,128)}, u32[]{:S(2)}) copy-start(s32[128,2]{0,1:T(2,128)} %param.25) | copy-start | bytes 3076
  197.8 6.5 %copy-start.11 = (f32[128,2]{0,1:T(2,128)S(1)}, f32[128,2]{0,1:T(2,128)}, u32[]{:S(2)}) copy-start(f32[128,2]{0,1:T(2,128)} %param.26) | copy-start | bytes 3076
  204.3 6.2 %copy-start.15 = (f32[2048]{0:T(1024)S(1)}, f32[2048]{0:T(1024)}, u32[]{:S(2)}) copy-start(f32[2048]{0:T(1024)} %param.33) | copy-start | bytes 24580
  (4 other events, 4.3 us)
